TPU v7x, 512 devices: a whole 4x8x8 slice. The times are simulated.
512 devices in a mesh: sp: 64 (over z, y), fs: 4 (over x), tp: 2 (over core).
Axes of the slice: x: 4, y: 8, z: 8, core: 2. Of those that a mesh axis runs over, the one named last changes fastest.
Arguments:
- tokens: bfloat16 [4, 24576, 2048], P('fs', ('sp', 'tp')), may hold values from -6 to 6
- norm_gain: float32 [2048], replicated, may hold values from 0.1 to 1.9
- conv_gate_w: bfloat16 [2048, 1024], P('sp', 'tp'), may hold values from -0.125 to 0.125
- conv_in_w: bfloat16 [2048, 1024], P('sp', 'tp'), may hold values from -0.125 to 0.125
- query_w: bfloat16 [2048, 1024], P('sp', 'tp'), may hold values from -0.125 to 0.125
- forget_w: bfloat16 [2048, 1024], P('sp', 'tp'), may hold values from -0.125 to 0.125
- value_w: bfloat16 [2048, 1024], P('sp', 'tp'), may hold values from -0.125 to 0.125
- conv_taps: float32 [3, 1024], P(None, 'tp'), may hold values from -3.5 to 3.5
- floor_gate: float32 [1024], P('tp'), may hold values from 0.93 to 1
- leak: float32 [4, 24576, 8], P('fs', 'sp', 'tp'), may hold values from -1.4 to 0
- head_gain: float32 [128], replicated, may hold values from 0.1 to 1.9
- conv_out_w: bfloat16 [1024, 2048], P('tp', 'fs'), may hold values from -0.125 to 0.125
- chain_out_w: bfloat16 [1024, 2048], P('tp', 'fs'), may hold values from -0.125 to 0.125
Outputs:
- mixed: bfloat16 [4, 24576, 2048], P('fs', ('sp', 'tp'))
All inputs are finite; a program needn't handle non-finite values.
Results may differ from a plain program's by a relative error of at most 0.013.
Values may be sent and summed in bfloat16 or wider, within the bound.
No kernel may reach another device: no remote copies, remote signals or barrier semaphores. Data moves between devices by JAX's collectives and lax.ppermute only.
A program may use at most 128 MiB of HBM per device.

v0:
```python
import jax
import jax.numpy as jnp
from jax import lax
from jax.experimental import pallas as pl
from jax.experimental.pallas import tpu as pltpu
from jax.sharding import Mesh
from jax.sharding import PartitionSpec as P

SP = ("sp_0", "sp_1")
SP_TP = ("sp_0", "sp_1", "tp")
F32 = jnp.float32
BF16 = jnp.bfloat16
LANES = 128
SLOT_SHIFT = (0, 3, 1, 2)


def struct(shape, dtype):
    return jax.ShapeDtypeStruct(shape, dtype)


def vmem(count):
    return [pl.BlockSpec(memory_space=pltpu.VMEM) for _ in range(count)]


def split3(values):
    high = values.astype(BF16)
    rest = values - high.astype(F32)
    middle = rest.astype(BF16)
    low = (rest - middle.astype(F32)).astype(BF16)
    return high, middle, low


def dot(a, b, dims=((1,), (0,))):
    return lax.dot_general(a, b, (dims, ((), ())), preferred_element_type=F32)


def norm_kernel(x_ref, gain_ref, o_ref):
    values = x_ref[...].astype(F32)
    center = values - jnp.mean(values, axis=-1, keepdims=True)
    spread = jnp.mean(center * center, axis=-1, keepdims=True)
    o_ref[...] = (center * lax.rsqrt(spread + 1e-05) * gain_ref[...]).astype(BF16)


def norm_rows(tokens, gain):
    return pl.pallas_call(
        norm_kernel,
        out_shape=struct(tokens.shape, BF16),
        in_specs=vmem(2),
        out_specs=vmem(1)[0],
        name="norm",
    )(tokens, gain[None])


def slab_kernel(*refs):
    ins, o_ref = refs[:-1], refs[-1]
    start = pl.multiple_of(lax.axis_index("fs") * LANES, LANES)
    for i, w_ref in enumerate(ins):
        part = w_ref[:, pl.ds(start, LANES)]
        for k in range(o_ref.shape[0]):
            o_ref[k, :, i * LANES : (i + 1) * LANES] = part


def weight_slabs(weights, copies):
    rows = weights[0].shape[0]
    return pl.pallas_call(
        slab_kernel,
        out_shape=struct((copies, rows, len(weights) * LANES), BF16),
        in_specs=vmem(len(weights)),
        out_specs=vmem(1)[0],
        name="slab",
    )(*weights)


def copy_kernel(in_ref, o_ref):
    o_ref[...] = in_ref[...]


def passed_on(array):
    return pl.pallas_call(
        copy_kernel,
        out_shape=struct(array.shape, array.dtype),
        in_specs=vmem(1),
        out_specs=vmem(1)[0],
    )(array)


def place_rows(scratch, slot, direct, other, w):
    core = lax.axis_index("tp")
    half = direct.shape[0]
    first = pl.multiple_of(core * half, half)
    second = pl.multiple_of((1 - core) * half, half)
    scratch[slot, pl.ds(first, half), :] = dot(direct[...], w).astype(BF16)
    scratch[slot, pl.ds(second, half), :] = dot(other[...], w).astype(BF16)


def lower_triangle(n):
    row = lax.broadcasted_iota(jnp.int32, (n, n), 0)
    col = lax.broadcasted_iota(jnp.int32, (n, n), 1)
    return row >= col


def running_sum(tri, values):
    width = values.shape[1]
    parts = dot(tri, jnp.concatenate(split3(values), axis=1))
    return parts[:, :width] + parts[:, width : 2 * width] + parts[:, 2 * width :]


def state_kernel(*refs):
    toks, (w_ref, floor_ref, *rest) = refs[:8], refs[8:]
    leaks, rest = rest[:4], rest[4:]
    state_ref, run_ref, leak_ref, keys_ref, value_ref, raw = rest
    length = run_ref.shape[1]
    tri = lower_triangle(length).astype(F32).astype(BF16)
    x = lax.axis_index("fs")
    leak_rows = jnp.concatenate(
        [ref[pl.ds(x, 1), :] for ref in leaks] + [jnp.zeros((4, length), F32)], axis=0
    )
    padded = jnp.concatenate([leak_rows, jnp.zeros((LANES - 8, length), F32)], axis=0)
    leak_run = running_sum(tri, padded.T)
    leak_ref[...] = leak_run
    gap = 1.0 - floor_ref[...]
    lane = lax.broadcasted_iota(jnp.int32, (LANES, LANES), 1)
    w = w_ref[...]
    for r in range(4):
        place_rows(raw, r, toks[2 * r], toks[2 * r + 1], w)
        both = raw[r]
        keys = gap * jax.nn.sigmoid(-both[:, :LANES].astype(F32))
        values = both[:, LANES:]
        running = running_sum(tri, jnp.log1p(-keys))
        total = running + leak_run[:, r : r + 1]
        last = total[length - 1 :, :]
        fading = (keys * jnp.exp(last - total)).astype(BF16)
        state = dot(fading, values, ((0,), (0,)))
        spread = jnp.broadcast_to(last, (LANES, LANES)).T
        high = spread.astype(BF16).astype(F32)
        coded = jnp.where(lane < LANES // 2, high, spread - high)
        packed = jnp.concatenate(
            [state.reshape(LANES // 8, 8, LANES), coded.reshape(LANES // 8, 8, LANES)], axis=1
        )
        state_ref[r * 16 : (r + 1) * 16] = packed.astype(BF16)
        run_ref[r] = running
        keys_ref[r] = keys
        value_ref[r] = values


def local_states(toks, w, floor, leaks):
    length = 2 * toks[0].shape[0]
    block = (4, length, LANES)
    return pl.pallas_call(
        state_kernel,
        out_shape=(
            struct((64, 16, LANES), BF16),
            struct(block, F32),
            struct((length, LANES), F32),
            struct(block, F32),
            struct(block, BF16),
        ),
        in_specs=[
            *vmem(8),
            pl.BlockSpec((w.shape[0], 2 * LANES), lambda i: (0, 0)),
            *vmem(5),
        ],
        out_specs=tuple(vmem(5)),
        grid=(1,),
        scratch_shapes=[pltpu.VMEM((4, length, 2 * LANES), BF16)],
        name="states",
    )(*toks, w, floor, *leaks)


def scan_kernel(in_ref, o_ref):
    carry = jnp.zeros((8, LANES), F32)
    for k in range(in_ref.shape[0]):
        both = in_ref[k].astype(F32)
        o_ref[k] = carry.astype(BF16)
        coded = both[8:]
        decay = jnp.exp(coded + pltpu.roll(coded, LANES // 2, 1))
        carry = decay * carry + both[:8]


def scan_blocks(states):
    return pl.pallas_call(
        scan_kernel,
        out_shape=struct((states.shape[0], 8, LANES), BF16),
        in_specs=vmem(1),
        out_specs=vmem(1)[0],
        name="scan",
    )(states)


def inside_kernel(*refs):
    toks, (w_ref, run_ref, leak_ref, keys_ref, value_ref, *rest) = refs[:8], refs[8:]
    inside_ref, reach_ref, gate_ref, signal_ref, raw = rest
    length = run_ref.shape[1]
    causal = lower_triangle(length)
    w = w_ref[:, 2 * LANES :]
    leak_run = leak_ref[...]
    leak_rows = leak_run.T
    for r in range(4):
        place_rows(raw, r, toks[2 * r], toks[2 * r + 1], w)
        gate_ref[r] = raw[r, :, LANES : 2 * LANES]
        signal_ref[r] = raw[r, :, 2 * LANES :]
        running = run_ref[r]
        logits = raw[r, :, :LANES].astype(F32)
        query = logits * jax.nn.sigmoid(logits)
        middle = 0.5 * running[length - 1 :, :]
        ahead = (query * jnp.exp(running - middle)).astype(BF16)
        behind = (keys_ref[r] * jnp.exp(middle - running)).astype(BF16)
        column = leak_run[:, r : r + 1]
        fade = jnp.exp(jnp.where(causal, column - leak_rows[r : r + 1, :], -jnp.inf))
        scores = dot(ahead, behind, ((1,), (1,))) * fade
        inside_ref[r] = dot(scores.astype(BF16), value_ref[r])
        reach_ref[r] = (query * jnp.exp(running + column)).astype(BF16)


def inside_blocks(toks, w, running, leak_run, keys, values):
    length = running.shape[1]
    block = (4, length, LANES)
    return pl.pallas_call(
        inside_kernel,
        out_shape=(struct(block, F32), struct(block, BF16), struct(block, BF16), struct(block, BF16)),
        in_specs=vmem(13),
        out_specs=tuple(vmem(4)),
        scratch_shapes=[pltpu.VMEM((4, length, 3 * LANES), BF16)],
        name="inside",
    )(*toks, w, running, leak_run, keys, values)


def mix_kernel(
    inside_ref, reach_ref, state_ref, gate_ref, signal_ref, rim_ref, taps_ref, gain_ref, o_ref, padded
):
    length = inside_ref.shape[1]
    half = length // 2
    x = lax.axis_index("fs")
    start = pl.multiple_of(x * LANES, LANES)
    taps = taps_ref[:, pl.ds(start, LANES)]
    for r in range(4):
        sequence = (x + SLOT_SHIFT[r]) % 4
        padded[0:8, :] = rim_ref[r, 8:, :].astype(F32)
        padded[8:, :] = signal_ref[r].astype(F32)
        filtered = taps[0:1] * padded[6 : 6 + length, :]
        filtered = filtered + taps[1:2] * padded[7 : 7 + length, :]
        filtered = filtered + taps[2:3] * padded[8 : 8 + length, :]
        conv = (gate_ref[r].astype(F32) * filtered).astype(BF16)
        chain = inside_ref[r] + dot(reach_ref[r], state_ref[r])
        scale = lax.rsqrt(jnp.mean(chain * chain, axis=-1, keepdims=True) + 1e-06)
        chain = (chain * scale * gain_ref[...]).astype(BF16)
        for h in range(2):
            rows = slice(h * half, (h + 1) * half)
            o_ref[2 * sequence + h, :, :LANES] = conv[rows]
            o_ref[2 * sequence + h, :, LANES:] = chain[rows]


def mix_blocks(inside, reach, state, gate, signal, rim, taps, gain):
    length = inside.shape[1]
    return pl.pallas_call(
        mix_kernel,
        out_shape=struct((8, length // 2, 2 * LANES), BF16),
        in_specs=vmem(8),
        out_specs=vmem(1)[0],
        scratch_shapes=[pltpu.VMEM((length + 8, LANES), F32)],
        name="mix",
    )(inside, reach, state, gate, signal, rim, taps, gain)


def out_kernel(mix_ref, near_ref, far_ref, o_ref):
    core = lax.axis_index("tp")
    total = jnp.zeros(o_ref.shape, F32)
    for c, w_ref in ((core, near_ref), (1 - core, far_ref)):
        pieces = [mix_ref[2 * x + c] for x in range(4)]
        lhs = jnp.concatenate(
            [piece[:, :LANES] for piece in pieces] + [piece[:, LANES:] for piece in pieces], axis=1
        )
        total = total + dot(lhs, w_ref[0])
    o_ref[...] = total.astype(BF16)


def out_rows(mix, near, far):
    rows = mix.shape[1]
    pieces, deep, wide = near.shape
    return pl.pallas_call(
        out_kernel,
        out_shape=struct((rows, pieces * wide), BF16),
        grid=(pieces,),
        in_specs=[
            pl.BlockSpec(mix.shape, lambda j: (0, 0, 0)),
            pl.BlockSpec((1, deep, wide), lambda j: (j, 0, 0)),
            pl.BlockSpec((1, deep, wide), lambda j: (j, 0, 0)),
        ],
        out_specs=pl.BlockSpec((rows, wide), lambda j: (0, j)),
        name="out",
    )(mix, near, far)


def ring(array, axis, by):
    count = lax.axis_size(axis)
    return lax.ppermute(array, axis, [(i, (i + by) % count) for i in range(count)])


def exchanged(array, axis):
    return lax.all_to_all(array, axis, split_axis=0, concat_axis=0, tiled=True)


def layer(
    tokens,
    norm_gain,
    conv_gate_w,
    conv_in_w,
    query_w,
    forget_w,
    value_w,
    conv_taps,
    floor_gate,
    leak,
    head_gain,
    conv_out_w,
    chain_out_w,
):
    x = lax.axis_index("fs")
    slabs = weight_slabs((forget_w, value_w, query_w, conv_gate_w, conv_in_w), 8)
    y_rows = exchanged(slabs, "sp_1").reshape(-1, slabs.shape[2])
    y_rows = passed_on(y_rows)
    weights = lax.all_gather(y_rows, "sp_0", axis=0, tiled=True)

    own = norm_rows(tokens[0], norm_gain)
    own_leak = leak[0].T
    direct, leaks = [own], [own_leak]
    for by in (1, 3, 2):
        direct.append(ring(own, "fs", by))
        leaks.append(ring(own_leak, "fs", by))
    other = []
    for part in direct:
        other.append(ring(part, "tp", 1))
    toks = [part for pair in zip(direct, other) for part in pair]

    out_w = jnp.concatenate([conv_out_w, chain_out_w], axis=0)
    out_w, y_rows = lax.optimization_barrier((out_w, y_rows))
    near = lax.all_gather(out_w, "fs", axis=0)

    floor = lax.dynamic_slice_in_dim(floor_gate, x * LANES, LANES, 0)[None]
    states, running, leak_run, keys, values = local_states(toks, weights, floor, leaks)
    arrived = exchanged(states, SP)
    before = exchanged(scan_blocks(arrived), SP)
    before = before.reshape(4, LANES, LANES)

    inside, reach, gate, signal = inside_blocks(toks, weights, running, leak_run, keys, values)
    count = 64
    tail = signal[:, -16:, :]
    rim = lax.ppermute(tail, SP, [(i, i + 1) for i in range(count - 1)])
    mix = mix_blocks(inside, reach, before, gate, signal, rim, conv_taps, head_gain[None])
    near, mix = lax.optimization_barrier((near, mix))
    mix = exchanged(mix, ("fs", "tp"))
    far = ring(near, "tp", 1)
    return out_rows(mix, near, far)[None]


def solution(mesh):
    split = Mesh(
        mesh.devices.reshape(8, 8, mesh.shape["fs"], mesh.shape["tp"]), ("sp_0", "sp_1", "fs", "tp")
    )
    in_specs = (
        P("fs", SP_TP, None),
        P(),
        P(SP, "tp"),
        P(SP, "tp"),
        P(SP, "tp"),
        P(SP, "tp"),
        P(SP, "tp"),
        P(None, "tp"),
        P("tp"),
        P("fs", SP, "tp"),
        P(),
        P("tp", "fs"),
        P("tp", "fs"),
    )
    out_specs = P("fs", SP_TP, None)
    return jax.shard_map(layer, mesh=split, in_specs=in_specs, out_specs=out_specs, check_vma=False)
```

profile of v0, /device:TPU:1, one launch (start us, length us, event | category | flops | bytes accessed | tf_op | source)
XLA Modules:
  0.0 194.0 jit_solution(608778836774871991)
XLA Ops:
  8.1 17.8 %all_to_all.20 = bf16[8,32,640]{2,1,0:T(8,128)(2,1)} all-to-all(bf16[8,32,640]{2,1,0:T(8,128)(2,1)} %slab.1), channel_id=1, replica_groups=mesh['sp_0'=8,'sp_1'=8,'fs'=4,'tp'=2] {'sp_1'}, dimensions={0} | all-to-all | bytes 655360 | tf_op jit(solution)/shard_map/all_to_all | solution.py:300
  27.7 2.3 %pad_maximum_fusion = bf16[1024,512]{1,0:T(8,128)(2,1)} fusion(bf16[512,512]{1,0:T(8,128)(2,1)} %param.25, bf16[512,512]{1,0:T(8,128)(2,1)} %param.24), kind=kLoop, calls=%fused_computation | loop fusion | flops 2097152 | bytes 2097152 | tf_op jit(solution)/shard_map/concatenate | solution.py:335
  30.0 2.5 %norm.1.refs_0_ = bf16[192,2048]{1,0:T(8,128)(2,1)} custom-call(bf16[192,2048]{1,0:T(8,128)(2,1)} %bitcast.15, f32[1,2048]{1,0:T(1,128)} %bitcast.17), custom_call_target="tpu_custom_call" | custom-call | tf_op jit(solution)/shard_map/norm/pallas_call | solution.py:45
  32.5 4.8 %collective-permute-start.1 = (bf16[192,2048]{1,0:T(8,128)(2,1)}, bf16[192,2048]{1,0:T(8,128)(2,1)S(1)}, u32[]{:S(2)}, u32[]{:S(2)}) collective-permute-start(bf16[192,2048]{1,0:T(8,128)(2,1)} %norm.1.refs_0_), channel_id=1, source_target_pairs={{0,2},{2,4},{4,6},{6,0},{1,3},{3,5},{5,7},{7,1},{8,10},{10,12},{12... | collective-permute-start | bytes 2359304 | tf_op jit(solution)/shard_map/ppermute | solution.py:296
  37.4 3.2 %collective-permute-start.3 = (bf16[192,2048]{1,0:T(8,128)(2,1)}, bf16[192,2048]{1,0:T(8,128)(2,1)S(1)}, u32[]{:S(2)}, u32[]{:S(2)}) collective-permute-start(bf16[192,2048]{1,0:T(8,128)(2,1)} %norm.1.refs_0_), channel_id=1, source_target_pairs={{0,6},{2,0},{4,2},{6,4},{1,7},{3,1},{5,3},{7,5},{8,14},{10,8},{12,... | collective-permute-start | bytes 2359304 | tf_op jit(solution)/shard_map/ppermute | solution.py:296
  40.5 3.6 %collective-permute-start.5 = (bf16[192,2048]{1,0:T(8,128)(2,1)}, bf16[192,2048]{1,0:T(8,128)(2,1)S(1)}, u32[]{:S(2)}, u32[]{:S(2)}) collective-permute-start(bf16[192,2048]{1,0:T(8,128)(2,1)} %norm.1.refs_0_), channel_id=1, source_target_pairs={{0,4},{2,6},{4,0},{6,2},{1,5},{3,7},{5,1},{7,3},{8,12},{10,14},{12... | collective-permute-start | bytes 2359304 | tf_op jit(solution)/shard_map/ppermute | solution.py:296
  44.2 5.2 %collective-permute-start = (bf16[192,2048]{1,0:T(8,128)(2,1)}, bf16[192,2048]{1,0:T(8,128)(2,1)S(1)}, u32[]{:S(2)}, u32[]{:S(2)}) collective-permute-start(bf16[192,2048]{1,0:T(8,128)(2,1)} %norm.1.refs_0_), channel_id=1, source_target_pairs={{0,1},{1,0},{2,3},{3,2},{4,5},{5,4},{6,7},{7,6},{8,9},{9,8},{10,11... | collective-permute-start | bytes 2359304 | tf_op jit(solution)/shard_map/ppermute | solution.py:296
  49.4 4.3 %collective-permute-done.1.refs_2_ = bf16[192,2048]{1,0:T(8,128)(2,1)S(1)} collective-permute-done((bf16[192,2048]{1,0:T(8,128)(2,1)}, bf16[192,2048]{1,0:T(8,128)(2,1)S(1)}, u32[]{:S(2)}, u32[]{:S(2)}) %collective-permute-start.1) | collective-permute-done | bytes 786464 | tf_op jit(solution)/shard_map/ppermute | solution.py:296
  53.7 7.3 %collective-permute-start.2 = (bf16[192,2048]{1,0:T(8,128)(2,1)S(1)}, bf16[192,2048]{1,0:T(8,128)(2,1)}, u32[]{:S(2)}, u32[]{:S(2)}) collective-permute-start(bf16[192,2048]{1,0:T(8,128)(2,1)S(1)} %collective-permute-done.1.refs_2_), channel_id=1, source_target_pairs={{0,1},{1,0},{2,3},{3,2},{4,5},{5,4},{6,7},{7,6},{8,9},{9,8},{10,11... | collective-permute-start | bytes 2359304 | tf_op jit(solution)/shard_map/ppermute | solution.py:296
  61.0 3.5 %collective-permute-start.4 = (bf16[192,2048]{1,0:T(8,128)(2,1)S(1)}, bf16[192,2048]{1,0:T(8,128)(2,1)}, u32[]{:S(2)}, u32[]{:S(2)}) collective-permute-start(bf16[192,2048]{1,0:T(8,128)(2,1)S(1)} %collective-permute-done.3.refs_4_), channel_id=1, source_target_pairs={{0,1},{1,0},{2,3},{3,2},{4,5},{5,4},{6,7},{7,6},{8,9},{9,8},{10,11... | collective-permute-start | bytes 2359304 | tf_op jit(solution)/shard_map/ppermute | solution.py:296
  64.5 7.5 %collective-permute-done.5.refs_6_ = bf16[192,2048]{1,0:T(8,128)(2,1)S(1)} collective-permute-done((bf16[192,2048]{1,0:T(8,128)(2,1)}, bf16[192,2048]{1,0:T(8,128)(2,1)S(1)}, u32[]{:S(2)}, u32[]{:S(2)}) %collective-permute-start.5) | collective-permute-done | bytes 786464 | tf_op jit(solution)/shard_map/ppermute | solution.py:296
  72.0 5.2 %collective-permute-start.6 = (bf16[192,2048]{1,0:T(8,128)(2,1)S(1)}, bf16[192,2048]{1,0:T(8,128)(2,1)}, u32[]{:S(2)}, u32[]{:S(2)}) collective-permute-start(bf16[192,2048]{1,0:T(8,128)(2,1)S(1)} %collective-permute-done.5.refs_6_), channel_id=1, source_target_pairs={{0,1},{1,0},{2,3},{3,2},{4,5},{5,4},{6,7},{7,6},{8,9},{9,8},{10,11... | collective-permute-start | bytes 2359304 | tf_op jit(solution)/shard_map/ppermute | solution.py:296
  77.3 4.7 %collective-permute-start.7 = (f32[4,384]{1,0:T(4,128)S(1)}, f32[4,384]{1,0:T(4,128)S(1)}, u32[]{:S(2)}, u32[]{:S(2)}) collective-permute-start(f32[4,384]{1,0:T(4,128)S(1)} %bitcast.19), channel_id=1, source_target_pairs={{0,2},{2,4},{4,6},{6,0},{1,3},{3,5},{5,7},{7,1},{8,10},{10,12},{12... | collective-permute-start | bytes 18440 | tf_op jit(solution)/shard_map/ppermute | solution.py:296
  83.6 3.4 %collective-permute-start.8 = (f32[4,384]{1,0:T(4,128)S(1)}, f32[4,384]{1,0:T(4,128)S(1)}, u32[]{:S(2)}, u32[]{:S(2)}) collective-permute-start(f32[4,384]{1,0:T(4,128)S(1)} %bitcast.20), channel_id=1, source_target_pairs={{0,6},{2,0},{4,2},{6,4},{1,7},{3,1},{5,3},{7,5},{8,14},{10,8},{12,... | collective-permute-start | bytes 18440 | tf_op jit(solution)/shard_map/ppermute | solution.py:296
  88.0 3.1 %collective-permute-start.9 = (f32[4,384]{1,0:T(4,128)S(1)}, f32[4,384]{1,0:T(4,128)S(1)}, u32[]{:S(2)}, u32[]{:S(2)}) collective-permute-start(f32[4,384]{1,0:T(4,128)S(1)} %bitcast.21), channel_id=1, source_target_pairs={{0,4},{2,6},{4,0},{6,2},{1,5},{3,7},{5,1},{7,3},{8,12},{10,14},{12... | collective-permute-start | bytes 18440 | tf_op jit(solution)/shard_map/ppermute | solution.py:296
  94.8 8.9 %states.1 = (bf16[64,16,128]{2,1,0:T(8,128)(2,1)}, f32[4,384,128]{2,1,0:T(8,128)}, f32[384,128]{1,0:T(8,128)}, f32[4,384,128]{2,1,0:T(8,128)}, bf16[4,384,128]{2,1,0:T(8,128)(2,1)}) custom-call(bf16[192,2048]{1,0:T(8,128)(2,1)} %norm.1.refs_0_, bf16[192,2048]{1,0:T(8,128)(2,1)} %copy-done.4, bf16[192,2048]{1,0:T(8,128)(2,1)} %copy-done.1, ...), custom_call_target="tpu_custom_call" | custom-call | tf_op jit(solution)/shard_map/states/pallas_call | solution.py:149
  103.6 27.6 %all_to_all.21.in_ref = bf16[64,16,128]{2,1,0:T(8,128)(2,1)} all-to-all(bf16[64,16,128]{2,1,0:T(8,128)(2,1)} %get-tuple-element.24), channel_id=1, replica_groups=mesh['sp_0'=8,'sp_1'=8,'fs'=4,'tp'=2] {'sp_0','sp_1'}, dimensions={0} | all-to-all | bytes 524288 | tf_op jit(solution)/shard_map/all_to_all | solution.py:300
  133.1 4.8 %all-to-all-start.2 = ((bf16[64,8,128]{2,1,0:T(8,128)(2,1)}), bf16[64,8,128]{2,1,0:T(8,128)(2,1)S(1)}, u32[]{:S(2)}, u32[]{:S(2)}) async-start(bf16[64,8,128]{2,1,0:T(8,128)(2,1)} %scan.1), calls=%async_computation.2 | async-start | bytes 262144 | tf_op jit(solution)/shard_map/all_to_all | solution.py:300
  137.9 10.2 %inside.1 = (f32[4,384,128]{2,1,0:T(8,128)}, bf16[4,384,128]{2,1,0:T(8,128)(2,1)}, bf16[4,384,128]{2,1,0:T(8,128)(2,1)}, bf16[4,384,128]{2,1,0:T(8,128)(2,1)}) custom-call(bf16[192,2048]{1,0:T(8,128)(2,1)} %norm.1.refs_0_, bf16[192,2048]{1,0:T(8,128)(2,1)} %copy-done.4, bf16[192,2048]{1,0:T(8,128)(2,1)} %copy-done.1, ...), custom_call_target="tpu_custom_call" | custom-call | tf_op jit(solution)/shard_map/inside/pallas_call | solution.py:218
  148.8 2.6 %collective-permute-start.10 = (bf16[4,16,128]{2,1,0:T(8,128)(2,1)S(1)}, bf16[4,16,128]{2,1,0:T(8,128)(2,1)S(1)}, u32[]{:S(2)}, u32[]{:S(2)}) collective-permute-start(bf16[4,16,128]{2,1,0:T(8,128)(2,1)S(1)} %slice.3), channel_id=1, source_target_pairs={{0,8},{8,16},{16,24},{24,32},{32,40},{40,48},{48,56},{56,64},{64,7... | collective-permute-start | bytes 49160 | tf_op jit(solution)/shard_map/ppermute | solution.py:348
  153.0 3.2 %mix.1 = bf16[8,192,256]{2,1,0:T(8,128)(2,1)} custom-call(f32[4,384,128]{2,1,0:T(8,128)} %get-tuple-element.22.inside_ref, bf16[4,384,128]{2,1,0:T(8,128)(2,1)} %get-tuple-element.23.reach_ref, bf16[4,128,128]{2,1,0:T(8,128)(2,1)} %bitcast.16, bf16[4,384,128]{2,1,0:T(8,128)(2,1)} %get-tuple-element.25.gate_ref, ...), custom_call_target="tpu_custom_call" | custom-call | tf_op jit(solution)/shard_map/mix/pallas_call | solution.py:255
  156.2 8.0 %collective-permute-start.11 = (bf16[4,1024,512]{2,1,0:T(8,128)(2,1)}, bf16[4,1024,512]{2,1,0:T(8,128)(2,1)}, u32[]{:S(2)}, u32[]{:S(2)}) collective-permute-start(bf16[4,1024,512]{2,1,0:T(8,128)(2,1)} %bitcast.12), channel_id=1, source_target_pairs={{0,1},{1,0},{2,3},{3,2},{4,5},{5,4},{6,7},{7,6},{8,9},{9,8},{10,11... | collective-permute-start | bytes 12582920 | tf_op jit(solution)/shard_map/ppermute | solution.py:296
  164.2 16.9 %all_to_all.22.mix_ref = bf16[8,192,256]{2,1,0:T(8,128)(2,1)} all-to-all(bf16[8,192,256]{2,1,0:T(8,128)(2,1)} %mix.1), channel_id=1, replica_groups=mesh['sp_0'=8,'sp_1'=8,'fs'=4,'tp'=2] {'fs','tp'}, dimensions={0} | all-to-all | bytes 1572864 | tf_op jit(solution)/shard_map/all_to_all | solution.py:300
  181.1 6.1 %out.1 = bf16[192,2048]{1,0:T(8,128)(2,1)} custom-call(bf16[8,192,256]{2,1,0:T(8,128)(2,1)} %all_to_all.22.mix_ref, bf16[4,1024,512]{2,1,0:T(8,128)(2,1)} %bitcast.13, bf16[4,1024,512]{2,1,0:T(8,128)(2,1)} %collective-permute-done.11.far_ref), custom_call_target="tpu_custom_call" | custom-call | tf_op jit(solution)/shard_map/out/pallas_call | solution.py:280
  (44 shorter events, 13.7 us)
Async XLA Ops:
  6.5 84.5 %copy-start = (f32[512]{0:T(512)S(1)}, f32[512]{0:T(512)}, u32[]{:S(2)}) copy-start(f32[512]{0:T(512)} %param.21) | copy-start | bytes 6148
  6.5 87.3 %all-gather.4.cloned.1.call-start = ((), (), s32[]{:S(2)}) async-start(), calls=%async_computation.4 | async-start | bytes 2949120 | tf_op jit(solution)/shard_map/all_gather | solution.py:322
  27.6 49.6 %copy-start.7 = (f32[1,384,4]{1,2,0:T(4,128)S(1)}, f32[1,384,4]{1,2,0:T(4,128)}, u32[]{:S(2)}) copy-start(f32[1,384,4]{1,2,0:T(4,128)} %param.22) | copy-start | bytes 18436
  27.7 128.5 %all-gather.6.cloned.1.call-start = ((), (), s32[]{:S(2)}) async-start(), calls=%async_computation.5 | async-start | bytes 5242880 | tf_op jit(solution)/shard_map/all_gather | solution.py:337
  32.5 21.2 %collective-permute-start.1 = (bf16[192,2048]{1,0:T(8,128)(2,1)}, bf16[192,2048]{1,0:T(8,128)(2,1)S(1)}, u32[]{:S(2)}, u32[]{:S(2)}) collective-permute-start(bf16[192,2048]{1,0:T(8,128)(2,1)} %norm.1.refs_0_), channel_id=1, source_target_pairs={{0,2},{2,4},{4,6},{6,0},{1,3},{3,5},{5,7},{7,1},{8,10},{10,12},{12... | collective-permute-start | bytes 2359304 | tf_op jit(solution)/shard_map/ppermute | solution.py:296
  37.4 23.6 %collective-permute-start.3 = (bf16[192,2048]{1,0:T(8,128)(2,1)}, bf16[192,2048]{1,0:T(8,128)(2,1)S(1)}, u32[]{:S(2)}, u32[]{:S(2)}) collective-permute-start(bf16[192,2048]{1,0:T(8,128)(2,1)} %norm.1.refs_0_), channel_id=1, source_target_pairs={{0,6},{2,0},{4,2},{6,4},{1,7},{3,1},{5,3},{7,5},{8,14},{10,8},{12,... | collective-permute-start | bytes 2359304 | tf_op jit(solution)/shard_map/ppermute | solution.py:296
  40.5 31.4 %collective-permute-start.5 = (bf16[192,2048]{1,0:T(8,128)(2,1)}, bf16[192,2048]{1,0:T(8,128)(2,1)S(1)}, u32[]{:S(2)}, u32[]{:S(2)}) collective-permute-start(bf16[192,2048]{1,0:T(8,128)(2,1)} %norm.1.refs_0_), channel_id=1, source_target_pairs={{0,4},{2,6},{4,0},{6,2},{1,5},{3,7},{5,1},{7,3},{8,12},{10,14},{12... | collective-permute-start | bytes 2359304 | tf_op jit(solution)/shard_map/ppermute | solution.py:296
  44.2 49.7 %collective-permute-start = (bf16[192,2048]{1,0:T(8,128)(2,1)}, bf16[192,2048]{1,0:T(8,128)(2,1)S(1)}, u32[]{:S(2)}, u32[]{:S(2)}) collective-permute-start(bf16[192,2048]{1,0:T(8,128)(2,1)} %norm.1.refs_0_), channel_id=1, source_target_pairs={{0,1},{1,0},{2,3},{3,2},{4,5},{5,4},{6,7},{7,6},{8,9},{9,8},{10,11... | collective-permute-start | bytes 2359304 | tf_op jit(solution)/shard_map/ppermute | solution.py:296
  53.7 40.2 %copy-start.1 = (bf16[192,2048]{1,0:T(8,128)(2,1)}, bf16[192,2048]{1,0:T(8,128)(2,1)S(1)}, u32[]{:S(2)}) copy-start(bf16[192,2048]{1,0:T(8,128)(2,1)S(1)} %collective-permute-done.1.refs_2_) | copy-start | bytes 2359300
  53.7 40.1 %collective-permute-start.2 = (bf16[192,2048]{1,0:T(8,128)(2,1)S(1)}, bf16[192,2048]{1,0:T(8,128)(2,1)}, u32[]{:S(2)}, u32[]{:S(2)}) collective-permute-start(bf16[192,2048]{1,0:T(8,128)(2,1)S(1)} %collective-permute-done.1.refs_2_), channel_id=1, source_target_pairs={{0,1},{1,0},{2,3},{3,2},{4,5},{5,4},{6,7},{7,6},{8,9},{9,8},{10,11... | collective-permute-start | bytes 2359304 | tf_op jit(solution)/shard_map/ppermute | solution.py:296
  61.0 32.9 %copy-start.2 = (bf16[192,2048]{1,0:T(8,128)(2,1)}, bf16[192,2048]{1,0:T(8,128)(2,1)S(1)}, u32[]{:S(2)}) copy-start(bf16[192,2048]{1,0:T(8,128)(2,1)S(1)} %collective-permute-done.3.refs_4_) | copy-start | bytes 2359300
  61.0 32.8 %collective-permute-start.4 = (bf16[192,2048]{1,0:T(8,128)(2,1)S(1)}, bf16[192,2048]{1,0:T(8,128)(2,1)}, u32[]{:S(2)}, u32[]{:S(2)}) collective-permute-start(bf16[192,2048]{1,0:T(8,128)(2,1)S(1)} %collective-permute-done.3.refs_4_), channel_id=1, source_target_pairs={{0,1},{1,0},{2,3},{3,2},{4,5},{5,4},{6,7},{7,6},{8,9},{9,8},{10,11... | collective-permute-start | bytes 2359304 | tf_op jit(solution)/shard_map/ppermute | solution.py:296
  72.0 21.9 %copy-start.3 = (bf16[192,2048]{1,0:T(8,128)(2,1)}, bf16[192,2048]{1,0:T(8,128)(2,1)S(1)}, u32[]{:S(2)}) copy-start(bf16[192,2048]{1,0:T(8,128)(2,1)S(1)} %collective-permute-done.5.refs_6_) | copy-start | bytes 2359300
  72.0 21.9 %collective-permute-start.6 = (bf16[192,2048]{1,0:T(8,128)(2,1)S(1)}, bf16[192,2048]{1,0:T(8,128)(2,1)}, u32[]{:S(2)}, u32[]{:S(2)}) collective-permute-start(bf16[192,2048]{1,0:T(8,128)(2,1)S(1)} %collective-permute-done.5.refs_6_), channel_id=1, source_target_pairs={{0,1},{1,0},{2,3},{3,2},{4,5},{5,4},{6,7},{7,6},{8,9},{9,8},{10,11... | collective-permute-start | bytes 2359304 | tf_op jit(solution)/shard_map/ppermute | solution.py:296
  77.3 6.3 %collective-permute-start.7 = (f32[4,384]{1,0:T(4,128)S(1)}, f32[4,384]{1,0:T(4,128)S(1)}, u32[]{:S(2)}, u32[]{:S(2)}) collective-permute-start(f32[4,384]{1,0:T(4,128)S(1)} %bitcast.19), channel_id=1, source_target_pairs={{0,2},{2,4},{4,6},{6,0},{1,3},{3,5},{5,7},{7,1},{8,10},{10,12},{12... | collective-permute-start | bytes 18440 | tf_op jit(solution)/shard_map/ppermute | solution.py:296
  83.6 10.3 %copy-start.8 = (f32[4,384]{1,0:T(4,128)}, f32[4,384]{1,0:T(4,128)S(1)}, u32[]{:S(2)}) copy-start(f32[4,384]{1,0:T(4,128)S(1)} %collective-permute-done.7.refs_11_) | copy-start | bytes 18436
  83.6 4.4 %collective-permute-start.8 = (f32[4,384]{1,0:T(4,128)S(1)}, f32[4,384]{1,0:T(4,128)S(1)}, u32[]{:S(2)}, u32[]{:S(2)}) collective-permute-start(f32[4,384]{1,0:T(4,128)S(1)} %bitcast.20), channel_id=1, source_target_pairs={{0,6},{2,0},{4,2},{6,4},{1,7},{3,1},{5,3},{7,5},{8,14},{10,8},{12,... | collective-permute-start | bytes 18440 | tf_op jit(solution)/shard_map/ppermute | solution.py:296
  88.0 6.0 %copy-start.9 = (f32[4,384]{1,0:T(4,128)}, f32[4,384]{1,0:T(4,128)S(1)}, u32[]{:S(2)}) copy-start(f32[4,384]{1,0:T(4,128)S(1)} %collective-permute-done.8.refs_12_) | copy-start | bytes 18436
  88.0 5.9 %collective-permute-start.9 = (f32[4,384]{1,0:T(4,128)S(1)}, f32[4,384]{1,0:T(4,128)S(1)}, u32[]{:S(2)}, u32[]{:S(2)}) collective-permute-start(f32[4,384]{1,0:T(4,128)S(1)} %bitcast.21), channel_id=1, source_target_pairs={{0,4},{2,6},{4,0},{6,2},{1,5},{3,7},{5,1},{7,3},{8,12},{10,14},{12... | collective-permute-start | bytes 18440 | tf_op jit(solution)/shard_map/ppermute | solution.py:296
  93.8 0.9 copy-start.4
  133.1 19.2 %all-to-all-start.2 = ((bf16[64,8,128]{2,1,0:T(8,128)(2,1)}), bf16[64,8,128]{2,1,0:T(8,128)(2,1)S(1)}, u32[]{:S(2)}, u32[]{:S(2)}) async-start(bf16[64,8,128]{2,1,0:T(8,128)(2,1)} %scan.1), calls=%async_computation.2 | async-start | bytes 262144 | tf_op jit(solution)/shard_map/all_to_all | solution.py:300
  148.8 3.5 %collective-permute-start.10 = (bf16[4,16,128]{2,1,0:T(8,128)(2,1)S(1)}, bf16[4,16,128]{2,1,0:T(8,128)(2,1)S(1)}, u32[]{:S(2)}, u32[]{:S(2)}) collective-permute-start(bf16[4,16,128]{2,1,0:T(8,128)(2,1)S(1)} %slice.3), channel_id=1, source_target_pairs={{0,8},{8,16},{16,24},{24,32},{32,40},{40,48},{48,56},{56,64},{64,7... | collective-permute-start | bytes 49160 | tf_op jit(solution)/shard_map/ppermute | solution.py:348
  152.3 0.6 copy-start.5
  156.2 24.9 %collective-permute-start.11 = (bf16[4,1024,512]{2,1,0:T(8,128)(2,1)}, bf16[4,1024,512]{2,1,0:T(8,128)(2,1)}, u32[]{:S(2)}, u32[]{:S(2)}) collective-permute-start(bf16[4,1024,512]{2,1,0:T(8,128)(2,1)} %bitcast.12), channel_id=1, source_target_pairs={{0,1},{1,0},{2,3},{3,2},{4,5},{5,4},{6,7},{7,6},{8,9},{9,8},{10,11... | collective-permute-start | bytes 12582920 | tf_op jit(solution)/shard_map/ppermute | solution.py:296
  (2 other events, 1.2 us)
Sparse Core Ops, SparseCore 0:
  27.8 45.2 all-gather.3
  75.1 54.7 all-gather.5
where the time goes:
time: 197 us; the launch traced here: 194 us
  blocking collectives  62.3 us (32%)
  starting transfers between devices  59.5 us (30%)
  Pallas kernels  36 us (18%)
  waiting for transfers between devices  17.4 us (9%)
  between operations  13.6 us (7%)
  local copies, waits for them, and re-layouts  2.88 us (1%)
  other arithmetic  2.26 us (1%)
    all_to_all x3, blocking collectives, exchanged(): return lax.all_to_all(array, axis, split_axis=0, concat_axis=0, tiled=True)  62.3 us
    ppermute x11, starting transfers between devices, ring(): lax.ppermute(array, axis, [(i, (i + by) % count) for i in range(count)])  52 us
    ppermute x11, waiting for transfers between devices, ring(): lax.ppermute(array, axis, [(i, (i + by) % count) for i in range(count)])  16.5 us
    pallas_call x1, Pallas kernels, inside_blocks(): pl.pallas_call(inside_kernel, out_shape=(struct(block, F32), struct(block...  10.2 us
    pallas_call x1, Pallas kernels, local_states(): pl.pallas_call(state_kernel, out_shape=(struct((64, 16, LANES), BF16), st...  8.88 us
    pallas_call x1, Pallas kernels, out_rows(): pl.pallas_call(out_kernel, out_shape=struct((rows, pieces * wide), BF16),...  6.06 us
    all_to_all x1, starting transfers between devices, exchanged(): return lax.all_to_all(array, axis, split_axis=0, concat_axis=0, tiled=True)  4.79 us
  transfers between devices with their start and end apart: 15, of which 6 were waited for; matrix products, arithmetic and copies ran while one was open for 2% of the time, Pallas kernels for 14%

commit v1 on v0

v1 whole, which is shorter than its diff:
```python
import jax
import jax.numpy as jnp
from jax import lax
from jax.experimental import pallas as pl
from jax.experimental.pallas import tpu as pltpu
from jax.sharding import Mesh
from jax.sharding import PartitionSpec as P

SP = ("sp_0", "sp_1")
SP_TP = ("sp_0", "sp_1", "tp")
F32 = jnp.float32
BF16 = jnp.bfloat16
LANES = 128


def struct(shape, dtype):
    return jax.ShapeDtypeStruct(shape, dtype)


def vmem(count):
    return [pl.BlockSpec(memory_space=pltpu.VMEM) for _ in range(count)]


def split3(values):
    high = values.astype(BF16)
    rest = values - high.astype(F32)
    middle = rest.astype(BF16)
    low = (rest - middle.astype(F32)).astype(BF16)
    return high, middle, low


def dot(a, b, dims=((1,), (0,))):
    return lax.dot_general(a, b, (dims, ((), ())), preferred_element_type=F32)


def norm_kernel(x_ref, gain_ref, leak_ref, o_ref):
    rows = x_ref.shape[0]
    values = x_ref[...].astype(F32)
    center = values - jnp.mean(values, axis=-1, keepdims=True)
    spread = jnp.mean(center * center, axis=-1, keepdims=True)
    o_ref[:rows, :] = (center * lax.rsqrt(spread + 1e-05) * gain_ref[...]).astype(BF16)
    leaks = jnp.concatenate([leak_ref[h : h + 1, :] for h in range(leak_ref.shape[0])], axis=1)
    parts = [part.astype(F32) for part in split3(leaks)]
    tail = jnp.concatenate([*parts, jnp.zeros((8 - len(parts), leaks.shape[1]), F32)], axis=0)
    unused = jnp.zeros((8, o_ref.shape[1] - leaks.shape[1]), F32)
    o_ref[rows:, :] = jnp.concatenate([tail, unused], axis=1).astype(BF16)


def norm_rows(tokens, gain, leaks):
    return pl.pallas_call(
        norm_kernel,
        out_shape=struct((tokens.shape[0] + 8, tokens.shape[1]), BF16),
        in_specs=vmem(3),
        out_specs=vmem(1)[0],
        name="norm",
    )(tokens, gain[None], leaks)


def slab_kernel(*refs):
    ins, o_ref = refs[:-1], refs[-1]
    start = pl.multiple_of(lax.axis_index("fs") * LANES, LANES)
    both = jnp.concatenate([w_ref[:, pl.ds(start, LANES)] for w_ref in ins], axis=1)
    for k in range(o_ref.shape[0]):
        o_ref[k] = both


def weight_slabs(weights, copies):
    rows = weights[0].shape[0]
    return pl.pallas_call(
        slab_kernel,
        out_shape=struct((copies, rows, len(weights) * LANES), BF16),
        in_specs=vmem(len(weights)),
        out_specs=vmem(1)[0],
        name="slab",
    )(*weights)


def relay_kernel(in_ref, early_ref, late_ref):
    early = in_ref[:, : 2 * LANES]
    for k in range(early_ref.shape[0]):
        early_ref[k] = early
    late_ref[...] = in_ref[:, 2 * LANES :]


def split_columns(rows, copies):
    deep, wide = rows.shape
    return pl.pallas_call(
        relay_kernel,
        out_shape=(
            struct((copies, deep, 2 * LANES), BF16),
            struct((deep, wide - 2 * LANES), BF16),
        ),
        in_specs=vmem(1),
        out_specs=tuple(vmem(2)),
        name="relay",
    )(rows)


def place_rows(scratch, toks, r, w):
    core = lax.axis_index("tp")
    half = scratch.shape[0] // 2
    for part, place in ((2 * r, core), (2 * r + 1, 1 - core)):
        start = pl.multiple_of(place * half, half)
        scratch[pl.ds(start, half), :] = dot(toks[part, :half, :], w).astype(BF16)


def fetches(refs, toks, sems):
    return [pltpu.make_async_copy(ref, toks.at[k], sems.at[k]) for k, ref in enumerate(refs)]


def lower_triangle(n):
    row = lax.broadcasted_iota(jnp.int32, (n, n), 0)
    col = lax.broadcasted_iota(jnp.int32, (n, n), 1)
    return row >= col


def running_sum(tri, values):
    width = values.shape[1]
    parts = dot(tri, jnp.concatenate(split3(values), axis=1))
    return parts[:, :width] + parts[:, width : 2 * width] + parts[:, 2 * width :]


def state_kernel(*refs):
    tok_refs, rest = refs[:8], refs[8:]
    w_ref, floor_ref, state_ref, run_ref, leak_ref, keys_ref, value_ref, raw, toks, sems = rest
    copies = fetches(tok_refs, toks, sems)
    for copy in copies:
        copy.start()
    length = run_ref.shape[1]
    half = length // 2
    tri = lower_triangle(length).astype(F32).astype(BF16)
    gap = 1.0 - floor_ref[...]
    lane = lax.broadcasted_iota(jnp.int32, (LANES, LANES), 1)
    first = pl.multiple_of(lax.axis_index("fs") * length, LANES)
    w = w_ref[...]
    for r in range(4):
        copies[2 * r].wait()
        copies[2 * r + 1].wait()
        coded = toks[2 * r, half:, pl.ds(first, length)].astype(F32)
        leaks = jnp.sum(coded, axis=0, keepdims=True)
        leak_rows = jnp.broadcast_to(leaks, (LANES, length))
        place_rows(raw, toks, r, w)
        keys = gap * jax.nn.sigmoid(-raw[:, :LANES].astype(F32))
        values = raw[:, LANES:]
        both = running_sum(tri, jnp.concatenate([jnp.log1p(-keys), leak_rows.T], axis=1))
        running, leak_run = both[:, :LANES], both[:, LANES:]
        total = running + leak_run
        last = total[length - 1 :, :]
        fading = (keys * jnp.exp(last - total)).astype(BF16)
        state = dot(fading, values, ((0,), (0,)))
        spread = jnp.broadcast_to(last, (LANES, LANES)).T
        high = spread.astype(BF16).astype(F32)
        split = jnp.where(lane < LANES // 2, high, spread - high)
        packed = jnp.concatenate(
            [state.reshape(LANES // 8, 8, LANES), split.reshape(LANES // 8, 8, LANES)], axis=1
        )
        state_ref[r * 16 : (r + 1) * 16] = packed.astype(BF16)
        run_ref[r] = running
        leak_ref[r] = leak_run
        keys_ref[r] = keys
        value_ref[r] = values


def anywhere(count):
    return [pl.BlockSpec(memory_space=pl.ANY) for _ in range(count)]


def token_scratch(tok, columns):
    rows, wide = tok.shape
    return [
        pltpu.VMEM((2 * (rows - 8), columns), BF16),
        pltpu.VMEM((8, rows, wide), BF16),
        pltpu.SemaphoreType.DMA((8,)),
    ]


def local_states(toks, w, floor):
    length = 2 * (toks[0].shape[0] - 8)
    block = (4, length, LANES)
    return pl.pallas_call(
        state_kernel,
        out_shape=(
            struct((64, 16, LANES), BF16),
            struct(block, F32),
            struct(block, F32),
            struct(block, F32),
            struct(block, BF16),
        ),
        in_specs=[*anywhere(8), *vmem(2)],
        out_specs=tuple(vmem(5)),
        scratch_shapes=token_scratch(toks[0], 2 * LANES),
        name="states",
    )(*toks, w, floor)


def sequence_block(*dims):
    return pl.BlockSpec((1, *dims), lambda r: (r, 0, 0))


def whole(*dims):
    return pl.BlockSpec(dims, lambda r: (0,) * len(dims))


def scan_kernel(in_ref, o_ref):
    carry = jnp.zeros((8, LANES), F32)
    for k in range(in_ref.shape[0]):
        both = in_ref[k].astype(F32)
        o_ref[k] = carry.astype(BF16)
        coded = both[8:]
        decay = jnp.exp(coded + pltpu.roll(coded, LANES // 2, 1))
        carry = decay * carry + both[:8]


def scan_blocks(states):
    return pl.pallas_call(
        scan_kernel,
        out_shape=struct((states.shape[0], 8, LANES), BF16),
        in_specs=vmem(1),
        out_specs=vmem(1)[0],
        name="scan",
    )(states)


def inside_kernel(*refs):
    tok_refs, rest = refs[:8], refs[8:]
    w_ref, run_ref, leak_ref, keys_ref, value_ref, *rest = rest
    inside_ref, reach_ref, gate_ref, signal_ref, raw, toks, sems = rest
    copies = fetches(tok_refs, toks, sems)
    for copy in copies:
        copy.start()
    length = run_ref.shape[1]
    causal = lower_triangle(length)
    w = w_ref[...]
    for r in range(4):
        copies[2 * r].wait()
        copies[2 * r + 1].wait()
        place_rows(raw, toks, r, w)
        gate_ref[r] = raw[:, LANES : 2 * LANES]
        signal_ref[r] = raw[:, 2 * LANES :]
        running = run_ref[r]
        leak_run = leak_ref[r]
        logits = raw[:, :LANES].astype(F32)
        query = logits * jax.nn.sigmoid(logits)
        middle = 0.5 * running[length - 1 :, :]
        ahead = (query * jnp.exp(running - middle)).astype(BF16)
        behind = (keys_ref[r] * jnp.exp(middle - running)).astype(BF16)
        fade = jnp.exp(jnp.where(causal, leak_run[:, :1] - leak_run.T[:1, :], -jnp.inf))
        scores = dot(ahead, behind, ((1,), (1,))) * fade
        inside_ref[r] = dot(scores.astype(BF16), value_ref[r])
        reach_ref[r] = (query * jnp.exp(running + leak_run)).astype(BF16)


def inside_blocks(toks, w, running, leak_run, keys, values):
    length = running.shape[1]
    block = (4, length, LANES)
    return pl.pallas_call(
        inside_kernel,
        out_shape=(struct(block, F32), struct(block, BF16), struct(block, BF16), struct(block, BF16)),
        in_specs=[*anywhere(8), *vmem(5)],
        out_specs=tuple(vmem(4)),
        scratch_shapes=token_scratch(toks[0], 3 * LANES),
        name="inside",
    )(*toks, w, running, leak_run, keys, values)


def mix_kernel(
    inside_ref, reach_ref, state_ref, gate_ref, signal_ref, rim_ref, taps_ref, gain_ref, o_ref, padded
):
    length = inside_ref.shape[1]
    half = length // 2
    x = lax.axis_index("fs")
    r = pl.program_id(0)
    shift = jnp.where(r == 1, 3, jnp.where(r == 2, 1, jnp.where(r == 3, 2, 0)))
    sequence = (x + shift) % 4
    start = pl.multiple_of(x * LANES, LANES)
    taps = taps_ref[:, pl.ds(start, LANES)]
    padded[0:8, :] = rim_ref[0, 8:, :].astype(F32)
    padded[8:, :] = signal_ref[0].astype(F32)
    filtered = taps[0:1] * padded[6 : 6 + length, :]
    filtered = filtered + taps[1:2] * padded[7 : 7 + length, :]
    filtered = filtered + taps[2:3] * padded[8 : 8 + length, :]
    conv = (gate_ref[0].astype(F32) * filtered).astype(BF16)
    chain = inside_ref[0] + dot(reach_ref[0], state_ref[0])
    scale = lax.rsqrt(jnp.mean(chain * chain, axis=-1, keepdims=True) + 1e-06)
    chain = (chain * scale * gain_ref[...]).astype(BF16)
    for h in range(2):
        rows = slice(h * half, (h + 1) * half)
        o_ref[2 * sequence + h, :, :LANES] = conv[rows]
        o_ref[2 * sequence + h, :, LANES:] = chain[rows]


def mix_blocks(inside, reach, state, gate, signal, rim, taps, gain):
    length = inside.shape[1]
    narrow = sequence_block(length, LANES)
    return pl.pallas_call(
        mix_kernel,
        out_shape=struct((8, length // 2, 2 * LANES), BF16),
        grid=(4,),
        in_specs=[
            narrow,
            narrow,
            sequence_block(LANES, LANES),
            narrow,
            narrow,
            sequence_block(16, LANES),
            whole(*taps.shape),
            whole(1, LANES),
        ],
        out_specs=whole(8, length // 2, 2 * LANES),
        scratch_shapes=[pltpu.VMEM((length + 8, LANES), F32)],
        name="mix",
    )(inside, reach, state, gate, signal, rim, taps, gain)


def out_kernel(mix_ref, near_ref, far_ref, o_ref):
    core = lax.axis_index("tp")
    total = jnp.zeros(o_ref.shape, F32)
    for c, w_ref in ((core, near_ref), (1 - core, far_ref)):
        pieces = [mix_ref[2 * x + c] for x in range(4)]
        lhs = jnp.concatenate(
            [piece[:, :LANES] for piece in pieces] + [piece[:, LANES:] for piece in pieces], axis=1
        )
        total = total + dot(lhs, w_ref[0])
    o_ref[...] = total.astype(BF16)


def out_rows(mix, near, far):
    rows = mix.shape[1]
    pieces, deep, wide = near.shape
    return pl.pallas_call(
        out_kernel,
        out_shape=struct((rows, pieces * wide), BF16),
        grid=(pieces,),
        in_specs=[whole(*mix.shape), sequence_block(deep, wide), sequence_block(deep, wide)],
        out_specs=pl.BlockSpec((rows, wide), lambda j: (0, j)),
        name="out",
    )(mix, near, far)


def ring(array, axis, by):
    count = lax.axis_size(axis)
    return lax.ppermute(array, axis, [(i, (i + by) % count) for i in range(count)])


def exchanged(array, axis):
    return lax.all_to_all(array, axis, split_axis=0, concat_axis=0, tiled=True)


def layer(
    tokens,
    norm_gain,
    conv_gate_w,
    conv_in_w,
    query_w,
    forget_w,
    value_w,
    conv_taps,
    floor_gate,
    leak,
    head_gain,
    conv_out_w,
    chain_out_w,
):
    x = lax.axis_index("fs")
    slabs = weight_slabs((forget_w, value_w, query_w, conv_gate_w, conv_in_w), 8)
    y_rows = exchanged(slabs, "sp_1").reshape(-1, slabs.shape[2])
    early, late = split_columns(y_rows, 8)
    late_w = lax.all_gather(late, "sp_0", axis=0, tiled=True)
    early_w = exchanged(early, "sp_0").reshape(-1, early.shape[2])

    own = norm_rows(tokens[0], norm_gain, leak[0].T)
    near = [own]
    for by in (1, 3, 2):
        near.append(ring(own, "fs", by))
    far = []
    for part in near:
        far.append(ring(part, "tp", 1))
    toks = [part for pair in zip(near, far) for part in pair]

    out_w = jnp.concatenate([conv_out_w, chain_out_w], axis=0)
    out_w, late = lax.optimization_barrier((out_w, late))
    out_near = lax.all_gather(out_w, "fs", axis=0)
    out_far = ring(out_near, "tp", 1)

    floor = lax.dynamic_slice_in_dim(floor_gate, x * LANES, LANES, 0)[None]
    states, running, leak_run, keys, values = local_states(toks, early_w, floor)
    arrived = exchanged(states, SP)
    before = exchanged(scan_blocks(arrived), SP)
    before = before.reshape(4, LANES, LANES)

    inside, reach, gate, signal = inside_blocks(toks, late_w, running, leak_run, keys, values)
    count = 64
    tail = signal[:, -16:, :]
    rim = lax.ppermute(tail, SP, [(i, i + 1) for i in range(count - 1)])
    mix = mix_blocks(inside, reach, before, gate, signal, rim, conv_taps, head_gain[None])
    mix = exchanged(mix, ("fs", "tp"))
    return out_rows(mix, out_near, out_far)[None]


def solution(mesh):
    split = Mesh(
        mesh.devices.reshape(8, 8, mesh.shape["fs"], mesh.shape["tp"]), ("sp_0", "sp_1", "fs", "tp")
    )
    in_specs = (
        P("fs", SP_TP, None),
        P(),
        P(SP, "tp"),
        P(SP, "tp"),
        P(SP, "tp"),
        P(SP, "tp"),
        P(SP, "tp"),
        P(None, "tp"),
        P("tp"),
        P("fs", SP, "tp"),
        P(),
        P("tp", "fs"),
        P("tp", "fs"),
    )
    out_specs = P("fs", SP_TP, None)
    return jax.shard_map(layer, mesh=split, in_specs=in_specs, out_specs=out_specs, check_vma=False)
```

time: 197 us -> 248 us (1.26)
  waiting for transfers between devices: 17.4 us -> 77.8 us
  blocking collectives: 62.3 us -> 45.1 us
  Pallas kernels: 36 us -> 39.2 us
  starting transfers between devices: 59.5 us -> 62.2 us
    all_gather x2, waiting for transfers between devices: 0.02 us -> 56.3 us  [the longest x1 56.3 us: layer(): out_near = lax.all_gather(out_w, 'fs', axis=0)]
    all_to_all x3 -> x2, blocking collectives: 62.3 us -> 45.1 us  [exchanged(): return lax.all_to_all(array, axis, split_axis=0, concat_axis=0, tiled=True)]
    all_to_all x1 -> x3, starting transfers between devices: 4.79 us -> 20.3 us  [exchanged(): return lax.all_to_all(array, axis, split_axis=0, concat_axis=0, tiled=True)]
    ppermute x11 -> x8, starting transfers between devices: 52 us -> 39.1 us  [ring(): lax.ppermute(array, axis, [(i, (i + by) % count) for i in range(count)])]
    all_to_all x1 -> x3, waiting for transfers between devices: 0.01 us -> 7.79 us  [exchanged(): return lax.all_to_all(array, axis, split_axis=0, concat_axis=0, tiled=True)]
    ppermute x11 -> x8, waiting for transfers between devices: 16.5 us -> 12.8 us  [ring(): lax.ppermute(array, axis, [(i, (i + by) % count) for i in range(count)])]
  transfers between devices with their start and end apart: 15 -> 14, of which waited for: 6 -> 5; matrix products, arithmetic and copies ran while one was open for 2% -> 2% of each run, Pallas kernels for 14% -> 12%
where the time goes in v1:
time: 248 us; the launch traced here: 245 us
  waiting for transfers between devices  77.8 us (31%)
  starting transfers between devices  62.2 us (25%)
  blocking collectives  45.1 us (18%)
  Pallas kernels  39.2 us (16%)
  between operations  15 us (6%)
  local copies, waits for them, and re-layouts  3.69 us (1%)
    all_gather x1, waiting for transfers between devices, layer(): out_near = lax.all_gather(out_w, 'fs', axis=0)  56.3 us
    all_to_all x2, blocking collectives, exchanged(): return lax.all_to_all(array, axis, split_axis=0, concat_axis=0, tiled=True)  45.1 us
    ppermute x8, starting transfers between devices, ring(): lax.ppermute(array, axis, [(i, (i + by) % count) for i in range(count)])  39.1 us
    all_to_all x3, starting transfers between devices, exchanged(): return lax.all_to_all(array, axis, split_axis=0, concat_axis=0, tiled=True)  20.3 us
    ppermute x8, waiting for transfers between devices, ring(): lax.ppermute(array, axis, [(i, (i + by) % count) for i in range(count)])  12.8 us
    pallas_call x1, Pallas kernels, local_states(): pl.pallas_call(state_kernel, out_shape=(struct((64, 16, LANES), BF16), st...  10.7 us
    pallas_call x1, Pallas kernels, inside_blocks(): pl.pallas_call(inside_kernel, out_shape=(struct(block, F32), struct(block...  10.2 us
    all_to_all x3, waiting for transfers between devices, exchanged(): return lax.all_to_all(array, axis, split_axis=0, concat_axis=0, tiled=True)  7.79 us
  transfers between devices with their start and end apart: 14, of which 5 were waited for; matrix products, arithmetic and copies ran while one was open for 2% of the time, Pallas kernels for 12%

profile of v1, /device:TPU:1, one launch (start us, length us, event | category | flops | bytes accessed | tf_op | source)
XLA Modules:
  0.0 245.2 jit_solution(16483118211588034975)
XLA Ops:
  9.0 7.6 %all-to-all-start = ((bf16[8,32,640]{2,1,0:T(8,128)(2,1)}), bf16[8,32,640]{2,1,0:T(8,128)(2,1)S(1)}, u32[]{:S(2)}, u32[]{:S(2)}) async-start(bf16[8,32,640]{2,1,0:T(8,128)(2,1)} %slab.1), calls=%async_computation | async-start | bytes 655360 | tf_op jit(solution)/shard_map/all_to_all | solution.py:346
  16.6 2.3 pad_maximum_fusion
  18.9 7.8 %all-to-all-done = bf16[8,32,640]{2,1,0:T(8,128)(2,1)S(1)} async-done(((bf16[8,32,640]{2,1,0:T(8,128)(2,1)}), bf16[8,32,640]{2,1,0:T(8,128)(2,1)S(1)}, u32[]{:S(2)}, u32[]{:S(2)}) %all-to-all-start) | async-done | bytes 327712 | tf_op jit(solution)/shard_map/all_to_all | solution.py:346
  27.4 2.1 relay.1
  29.6 56.3 %all-gather.6.cloned.1.call-done = bf16[4096,512]{1,0:T(8,128)(2,1)} async-done(((bf16[1024,512]{1,0:T(8,128)(2,1)}), bf16[4096,512]{1,0:T(8,128)(2,1)}) %all-gather.6.cloned.1.call-update) | async-done | bytes 4194320 | tf_op jit(solution)/shard_map/all_gather | solution.py:382
  85.9 2.7 %collective-permute-start.8 = (bf16[4,1024,512]{2,1,0:T(8,128)(2,1)}, bf16[4,1024,512]{2,1,0:T(8,128)(2,1)}, u32[]{:S(2)}, u32[]{:S(2)}) collective-permute-start(bf16[4,1024,512]{2,1,0:T(8,128)(2,1)} %bitcast.13), channel_id=1, source_target_pairs={{0,1},{1,0},{2,3},{3,2},{4,5},{5,4},{6,7},{7,6},{8,9},{9,8},{10,11... | collective-permute-start | bytes 12582920 | tf_op jit(solution)/shard_map/ppermute | solution.py:342
  88.7 7.1 %all-to-all-start.1 = ((bf16[8,256,256]{2,1,0:T(8,128)(2,1)}), bf16[8,256,256]{2,1,0:T(8,128)(2,1)S(1)}, u32[]{:S(2)}, u32[]{:S(2)}) async-start(bf16[8,256,256]{2,1,0:T(8,128)(2,1)} %get-tuple-element.18), calls=%async_computation.1 | async-start | bytes 2097152 | tf_op jit(solution)/shard_map/all_to_all | solution.py:346
  95.8 2.6 %norm.1.refs_0_ = bf16[200,2048]{1,0:T(8,128)(2,1)} custom-call(bf16[192,2048]{1,0:T(8,128)(2,1)} %bitcast.17, f32[1,2048]{1,0:T(1,128)} %bitcast.19, f32[4,384]{1,0:T(4,128)} %bitcast.20), custom_call_target="tpu_custom_call" | custom-call | tf_op jit(solution)/shard_map/norm/pallas_call | solution.py:50
  98.4 2.5 %collective-permute-start.1 = (bf16[200,2048]{1,0:T(8,128)(2,1)}, bf16[200,2048]{1,0:T(8,128)(2,1)S(1)}, u32[]{:S(2)}, u32[]{:S(2)}) collective-permute-start(bf16[200,2048]{1,0:T(8,128)(2,1)} %norm.1.refs_0_), channel_id=1, source_target_pairs={{0,2},{2,4},{4,6},{6,0},{1,3},{3,5},{5,7},{7,1},{8,10},{10,12},{12... | collective-permute-start | bytes 2457608 | tf_op jit(solution)/shard_map/ppermute | solution.py:342
  100.8 4.0 %collective-permute-start.3 = (bf16[200,2048]{1,0:T(8,128)(2,1)}, bf16[200,2048]{1,0:T(8,128)(2,1)S(1)}, u32[]{:S(2)}, u32[]{:S(2)}) collective-permute-start(bf16[200,2048]{1,0:T(8,128)(2,1)} %norm.1.refs_0_), channel_id=1, source_target_pairs={{0,6},{2,0},{4,2},{6,4},{1,7},{3,1},{5,3},{7,5},{8,14},{10,8},{12,... | collective-permute-start | bytes 2457608 | tf_op jit(solution)/shard_map/ppermute | solution.py:342
  104.9 2.5 %collective-permute-start.5 = (bf16[200,2048]{1,0:T(8,128)(2,1)}, bf16[200,2048]{1,0:T(8,128)(2,1)S(1)}, u32[]{:S(2)}, u32[]{:S(2)}) collective-permute-start(bf16[200,2048]{1,0:T(8,128)(2,1)} %norm.1.refs_0_), channel_id=1, source_target_pairs={{0,4},{2,6},{4,0},{6,2},{1,5},{3,7},{5,1},{7,3},{8,12},{10,14},{12... | collective-permute-start | bytes 2457608 | tf_op jit(solution)/shard_map/ppermute | solution.py:342
  107.4 3.0 %collective-permute-start = (bf16[200,2048]{1,0:T(8,128)(2,1)}, bf16[200,2048]{1,0:T(8,128)(2,1)}, u32[]{:S(2)}, u32[]{:S(2)}) collective-permute-start(bf16[200,2048]{1,0:T(8,128)(2,1)} %norm.1.refs_0_), channel_id=1, source_target_pairs={{0,1},{1,0},{2,3},{3,2},{4,5},{5,4},{6,7},{7,6},{8,9},{9,8},{10,11... | collective-permute-start | bytes 2457608 | tf_op jit(solution)/shard_map/ppermute | solution.py:342
  110.4 11.4 %collective-permute-done.1.refs_2_ = bf16[200,2048]{1,0:T(8,128)(2,1)S(1)} collective-permute-done((bf16[200,2048]{1,0:T(8,128)(2,1)}, bf16[200,2048]{1,0:T(8,128)(2,1)S(1)}, u32[]{:S(2)}, u32[]{:S(2)}) %collective-permute-start.1) | collective-permute-done | bytes 819232 | tf_op jit(solution)/shard_map/ppermute | solution.py:342
  121.8 20.0 %collective-permute-start.2 = (bf16[200,2048]{1,0:T(8,128)(2,1)S(1)}, bf16[200,2048]{1,0:T(8,128)(2,1)}, u32[]{:S(2)}, u32[]{:S(2)}) collective-permute-start(bf16[200,2048]{1,0:T(8,128)(2,1)S(1)} %collective-permute-done.1.refs_2_), channel_id=1, source_target_pairs={{0,1},{1,0},{2,3},{3,2},{4,5},{5,4},{6,7},{7,6},{8,9},{9,8},{10,11... | collective-permute-start | bytes 2457608 | tf_op jit(solution)/shard_map/ppermute | solution.py:342
  141.8 1.9 collective-permute-start.4
  143.8 2.4 collective-permute-start.6
  149.2 10.7 %states.1 = (bf16[64,16,128]{2,1,0:T(8,128)(2,1)}, f32[4,384,128]{2,1,0:T(8,128)}, f32[4,384,128]{2,1,0:T(8,128)}, f32[4,384,128]{2,1,0:T(8,128)}, bf16[4,384,128]{2,1,0:T(8,128)(2,1)}) custom-call(bf16[200,2048]{1,0:T(8,128)(2,1)} %norm.1.refs_0_, bf16[200,2048]{1,0:T(8,128)(2,1)} %collective-permute-done.refs_1_, bf16[200,2048]{1,0:T(8,128)(2,1)} %copy-done.2, ...), custom_call_target="tpu_custom_call" | custom-call | tf_op jit(solution)/shard_map/states/pallas_call | solution.py:180
  160.0 25.8 %all_to_all.25.in_ref = bf16[64,16,128]{2,1,0:T(8,128)(2,1)} all-to-all(bf16[64,16,128]{2,1,0:T(8,128)(2,1)} %get-tuple-element.25), channel_id=1, replica_groups=mesh['sp_0'=8,'sp_1'=8,'fs'=4,'tp'=2] {'sp_0','sp_1'}, dimensions={0} | all-to-all | bytes 524288 | tf_op jit(solution)/shard_map/all_to_all | solution.py:346
  187.6 5.5 %all-to-all-start.3 = ((bf16[64,8,128]{2,1,0:T(8,128)(2,1)}), bf16[64,8,128]{2,1,0:T(8,128)(2,1)S(1)}, u32[]{:S(2)}, u32[]{:S(2)}) async-start(bf16[64,8,128]{2,1,0:T(8,128)(2,1)} %scan.1), calls=%async_computation.3 | async-start | bytes 262144 | tf_op jit(solution)/shard_map/all_to_all | solution.py:346
  193.2 10.2 %inside.1 = (f32[4,384,128]{2,1,0:T(8,128)}, bf16[4,384,128]{2,1,0:T(8,128)(2,1)}, bf16[4,384,128]{2,1,0:T(8,128)(2,1)}, bf16[4,384,128]{2,1,0:T(8,128)(2,1)}) custom-call(bf16[200,2048]{1,0:T(8,128)(2,1)} %norm.1.refs_0_, bf16[200,2048]{1,0:T(8,128)(2,1)} %collective-permute-done.refs_1_, bf16[200,2048]{1,0:T(8,128)(2,1)} %copy-done.2, ...), custom_call_target="tpu_custom_call" | custom-call | tf_op jit(solution)/shard_map/inside/pallas_call | solution.py:256
  204.1 2.7 %collective-permute-start.7 = (bf16[4,16,128]{2,1,0:T(8,128)(2,1)S(1)}, bf16[4,16,128]{2,1,0:T(8,128)(2,1)S(1)}, u32[]{:S(2)}, u32[]{:S(2)}) collective-permute-start(bf16[4,16,128]{2,1,0:T(8,128)(2,1)S(1)} %slice.3), channel_id=1, source_target_pairs={{0,8},{8,16},{16,24},{24,32},{32,40},{40,48},{48,56},{56,64},{64,7... | collective-permute-start | bytes 49160 | tf_op jit(solution)/shard_map/ppermute | solution.py:394
  208.3 4.1 %mix.1 = bf16[8,192,256]{2,1,0:T(8,128)(2,1)} custom-call(f32[4,384,128]{2,1,0:T(8,128)} %get-tuple-element.23.inside_ref, bf16[4,384,128]{2,1,0:T(8,128)(2,1)} %get-tuple-element.24.reach_ref, bf16[4,128,128]{2,1,0:T(8,128)(2,1)} %bitcast.18, bf16[4,384,128]{2,1,0:T(8,128)(2,1)} %get-tuple-element.26.gate_ref, ...), custom_call_target="tpu_custom_call" | custom-call | tf_op jit(solution)/shard_map/mix/pallas_call | solution.py:295
  212.4 19.3 %all_to_all.26.mix_ref = bf16[8,192,256]{2,1,0:T(8,128)(2,1)} all-to-all(bf16[8,192,256]{2,1,0:T(8,128)(2,1)} %mix.1), channel_id=1, replica_groups=mesh['sp_0'=8,'sp_1'=8,'fs'=4,'tp'=2] {'fs','tp'}, dimensions={0} | all-to-all | bytes 1572864 | tf_op jit(solution)/shard_map/all_to_all | solution.py:346
  231.7 6.1 %out.1 = bf16[192,2048]{1,0:T(8,128)(2,1)} custom-call(bf16[8,192,256]{2,1,0:T(8,128)(2,1)} %all_to_all.26.mix_ref, bf16[4,1024,512]{2,1,0:T(8,128)(2,1)} %bitcast.14, bf16[4,1024,512]{2,1,0:T(8,128)(2,1)} %collective-permute-done.8.far_ref), custom_call_target="tpu_custom_call" | custom-call | tf_op jit(solution)/shard_map/out/pallas_call | solution.py:330
  (35 shorter events, 9.4 us)
Async XLA Ops:
  7.4 138.8 %copy-start = (f32[512]{0:T(512)S(1)}, f32[512]{0:T(512)}, u32[]{:S(2)}) copy-start(f32[512]{0:T(512)} %param.21) | copy-start | bytes 6148
  9.0 17.8 %all-to-all-start = ((bf16[8,32,640]{2,1,0:T(8,128)(2,1)}), bf16[8,32,640]{2,1,0:T(8,128)(2,1)S(1)}, u32[]{:S(2)}, u32[]{:S(2)}) async-start(bf16[8,32,640]{2,1,0:T(8,128)(2,1)} %slab.1), calls=%async_computation | async-start | bytes 655360 | tf_op jit(solution)/shard_map/all_to_all | solution.py:346
  16.6 69.3 %all-gather.6.cloned.1.call-start = ((), (), s32[]{:S(2)}) async-start(), calls=%async_computation.6 | async-start | bytes 5242880 | tf_op jit(solution)/shard_map/all_gather | solution.py:382
  26.7 0.7 copy-start.5
  29.6 163.6 %all-gather.4.cloned.1.call-start = ((), (), s32[]{:S(2)}) async-start(), calls=%async_computation.5 | async-start | bytes 1769472 | tf_op jit(solution)/shard_map/all_gather | solution.py:368
  85.9 145.8 %collective-permute-start.8 = (bf16[4,1024,512]{2,1,0:T(8,128)(2,1)}, bf16[4,1024,512]{2,1,0:T(8,128)(2,1)}, u32[]{:S(2)}, u32[]{:S(2)}) collective-permute-start(bf16[4,1024,512]{2,1,0:T(8,128)(2,1)} %bitcast.13), channel_id=1, source_target_pairs={{0,1},{1,0},{2,3},{3,2},{4,5},{5,4},{6,7},{7,6},{8,9},{9,8},{10,11... | collective-permute-start | bytes 12582920 | tf_op jit(solution)/shard_map/ppermute | solution.py:342
  88.7 59.6 %all-to-all-start.1 = ((bf16[8,256,256]{2,1,0:T(8,128)(2,1)}), bf16[8,256,256]{2,1,0:T(8,128)(2,1)S(1)}, u32[]{:S(2)}, u32[]{:S(2)}) async-start(bf16[8,256,256]{2,1,0:T(8,128)(2,1)} %get-tuple-element.18), calls=%async_computation.1 | async-start | bytes 2097152 | tf_op jit(solution)/shard_map/all_to_all | solution.py:346
  98.4 23.4 %collective-permute-start.1 = (bf16[200,2048]{1,0:T(8,128)(2,1)}, bf16[200,2048]{1,0:T(8,128)(2,1)S(1)}, u32[]{:S(2)}, u32[]{:S(2)}) collective-permute-start(bf16[200,2048]{1,0:T(8,128)(2,1)} %norm.1.refs_0_), channel_id=1, source_target_pairs={{0,2},{2,4},{4,6},{6,0},{1,3},{3,5},{5,7},{7,1},{8,10},{10,12},{12... | collective-permute-start | bytes 2457608 | tf_op jit(solution)/shard_map/ppermute | solution.py:342
  100.8 41.0 %collective-permute-start.3 = (bf16[200,2048]{1,0:T(8,128)(2,1)}, bf16[200,2048]{1,0:T(8,128)(2,1)S(1)}, u32[]{:S(2)}, u32[]{:S(2)}) collective-permute-start(bf16[200,2048]{1,0:T(8,128)(2,1)} %norm.1.refs_0_), channel_id=1, source_target_pairs={{0,6},{2,0},{4,2},{6,4},{1,7},{3,1},{5,3},{7,5},{8,14},{10,8},{12,... | collective-permute-start | bytes 2457608 | tf_op jit(solution)/shard_map/ppermute | solution.py:342
  104.9 38.9 %collective-permute-start.5 = (bf16[200,2048]{1,0:T(8,128)(2,1)}, bf16[200,2048]{1,0:T(8,128)(2,1)S(1)}, u32[]{:S(2)}, u32[]{:S(2)}) collective-permute-start(bf16[200,2048]{1,0:T(8,128)(2,1)} %norm.1.refs_0_), channel_id=1, source_target_pairs={{0,4},{2,6},{4,0},{6,2},{1,5},{3,7},{5,1},{7,3},{8,12},{10,14},{12... | collective-permute-start | bytes 2457608 | tf_op jit(solution)/shard_map/ppermute | solution.py:342
  107.4 39.5 %collective-permute-start = (bf16[200,2048]{1,0:T(8,128)(2,1)}, bf16[200,2048]{1,0:T(8,128)(2,1)}, u32[]{:S(2)}, u32[]{:S(2)}) collective-permute-start(bf16[200,2048]{1,0:T(8,128)(2,1)} %norm.1.refs_0_), channel_id=1, source_target_pairs={{0,1},{1,0},{2,3},{3,2},{4,5},{5,4},{6,7},{7,6},{8,9},{9,8},{10,11... | collective-permute-start | bytes 2457608 | tf_op jit(solution)/shard_map/ppermute | solution.py:342
  121.8 26.5 %copy-start.2 = (bf16[200,2048]{1,0:T(8,128)(2,1)}, bf16[200,2048]{1,0:T(8,128)(2,1)S(1)}, u32[]{:S(2)}) copy-start(bf16[200,2048]{1,0:T(8,128)(2,1)S(1)} %collective-permute-done.1.refs_2_) | copy-start | bytes 2457604
  121.8 25.1 %collective-permute-start.2 = (bf16[200,2048]{1,0:T(8,128)(2,1)S(1)}, bf16[200,2048]{1,0:T(8,128)(2,1)}, u32[]{:S(2)}, u32[]{:S(2)}) collective-permute-start(bf16[200,2048]{1,0:T(8,128)(2,1)S(1)} %collective-permute-done.1.refs_2_), channel_id=1, source_target_pairs={{0,1},{1,0},{2,3},{3,2},{4,5},{5,4},{6,7},{7,6},{8,9},{9,8},{10,11... | collective-permute-start | bytes 2457608 | tf_op jit(solution)/shard_map/ppermute | solution.py:342
  141.8 6.5 %copy-start.3 = (bf16[200,2048]{1,0:T(8,128)(2,1)}, bf16[200,2048]{1,0:T(8,128)(2,1)S(1)}, u32[]{:S(2)}) copy-start(bf16[200,2048]{1,0:T(8,128)(2,1)S(1)} %collective-permute-done.3.refs_4_) | copy-start | bytes 2457604
  141.8 5.1 %collective-permute-start.4 = (bf16[200,2048]{1,0:T(8,128)(2,1)S(1)}, bf16[200,2048]{1,0:T(8,128)(2,1)}, u32[]{:S(2)}, u32[]{:S(2)}) collective-permute-start(bf16[200,2048]{1,0:T(8,128)(2,1)S(1)} %collective-permute-done.3.refs_4_), channel_id=1, source_target_pairs={{0,1},{1,0},{2,3},{3,2},{4,5},{5,4},{6,7},{7,6},{8,9},{9,8},{10,11... | collective-permute-start | bytes 2457608 | tf_op jit(solution)/shard_map/ppermute | solution.py:342
  143.8 4.5 %copy-start.4 = (bf16[200,2048]{1,0:T(8,128)(2,1)}, bf16[200,2048]{1,0:T(8,128)(2,1)S(1)}, u32[]{:S(2)}) copy-start(bf16[200,2048]{1,0:T(8,128)(2,1)S(1)} %collective-permute-done.5.refs_6_) | copy-start | bytes 2457604
  143.8 4.5 %collective-permute-start.6 = (bf16[200,2048]{1,0:T(8,128)(2,1)S(1)}, bf16[200,2048]{1,0:T(8,128)(2,1)}, u32[]{:S(2)}, u32[]{:S(2)}) collective-permute-start(bf16[200,2048]{1,0:T(8,128)(2,1)S(1)} %collective-permute-done.5.refs_6_), channel_id=1, source_target_pairs={{0,1},{1,0},{2,3},{3,2},{4,5},{5,4},{6,7},{7,6},{8,9},{9,8},{10,11... | collective-permute-start | bytes 2457608 | tf_op jit(solution)/shard_map/ppermute | solution.py:342
  148.2 1.0 copy-start.1
  187.6 19.3 %all-to-all-start.3 = ((bf16[64,8,128]{2,1,0:T(8,128)(2,1)}), bf16[64,8,128]{2,1,0:T(8,128)(2,1)S(1)}, u32[]{:S(2)}, u32[]{:S(2)}) async-start(bf16[64,8,128]{2,1,0:T(8,128)(2,1)} %scan.1), calls=%async_computation.3 | async-start | bytes 262144 | tf_op jit(solution)/shard_map/all_to_all | solution.py:346
  204.1 3.6 %collective-permute-start.7 = (bf16[4,16,128]{2,1,0:T(8,128)(2,1)S(1)}, bf16[4,16,128]{2,1,0:T(8,128)(2,1)S(1)}, u32[]{:S(2)}, u32[]{:S(2)}) collective-permute-start(bf16[4,16,128]{2,1,0:T(8,128)(2,1)S(1)} %slice.3), channel_id=1, source_target_pairs={{0,8},{8,16},{16,24},{24,32},{32,40},{40,48},{48,56},{56,64},{64,7... | collective-permute-start | bytes 49160 | tf_op jit(solution)/shard_map/ppermute | solution.py:394
  206.9 0.8 copy-start.6
  207.7 0.6 copy-start.7
Sparse Core Ops, SparseCore 0:
  29.7 56.1 all-gather.5
Sparse Core Ops, SparseCore 1:
  88.8 51.9 all-gather.3

commit v2 on v1

--- a/solution.py
+++ b/solution.py
@@ -11,6 +11,7 @@
 F32 = jnp.float32
 BF16 = jnp.bfloat16
 LANES = 128
+SLOT_SHIFT = (0, 3, 1, 2)
 
 
 def struct(shape, dtype):
@@ -124,7 +125,7 @@
     tok_refs, rest = refs[:8], refs[8:]
     w_ref, floor_ref, state_ref, run_ref, leak_ref, keys_ref, value_ref, raw, toks, sems = rest
     copies = fetches(tok_refs, toks, sems)
-    for copy in copies:
+    for copy in copies[:4]:
         copy.start()
     length = run_ref.shape[1]
     half = length // 2
@@ -136,6 +137,9 @@
     for r in range(4):
         copies[2 * r].wait()
         copies[2 * r + 1].wait()
+        if r < 2:
+            copies[2 * r + 4].start()
+            copies[2 * r + 5].start()
         coded = toks[2 * r, half:, pl.ds(first, length)].astype(F32)
         leaks = jnp.sum(coded, axis=0, keepdims=True)
         leak_rows = jnp.broadcast_to(leaks, (LANES, length))
@@ -222,18 +226,30 @@
 
 
 def inside_kernel(*refs):
-    tok_refs, rest = refs[:8], refs[8:]
-    w_ref, run_ref, leak_ref, keys_ref, value_ref, *rest = rest
-    inside_ref, reach_ref, gate_ref, signal_ref, raw, toks, sems = rest
+    tok_refs, block_refs, rest = refs[:8], refs[8:16], refs[16:]
+    run_ref, leak_ref, keys_ref, value_ref, *rest = rest
+    inside_ref, reach_ref, gate_ref, signal_ref, raw, toks, sems, weights, weight_sems = rest
+    deep = block_refs[0].shape[0]
+    z = lax.axis_index("sp_0")
+    blocks = []
+    for k, ref in enumerate(block_refs):
+        start = pl.multiple_of((z + 8 - k) % 8 * deep, deep)
+        place = weights.at[pl.ds(start, deep), :]
+        blocks.append(pltpu.make_async_copy(ref, place, weight_sems.at[k]))
     copies = fetches(tok_refs, toks, sems)
-    for copy in copies:
+    for copy in blocks + copies[:4]:
         copy.start()
     length = run_ref.shape[1]
     causal = lower_triangle(length)
-    w = w_ref[...]
+    for block in blocks:
+        block.wait()
+    w = weights[...]
     for r in range(4):
         copies[2 * r].wait()
         copies[2 * r + 1].wait()
+        if r < 2:
+            copies[2 * r + 4].start()
+            copies[2 * r + 5].start()
         place_rows(raw, toks, r, w)
         gate_ref[r] = raw[:, LANES : 2 * LANES]
         signal_ref[r] = raw[:, 2 * LANES :]
@@ -250,17 +266,22 @@
         reach_ref[r] = (query * jnp.exp(running + leak_run)).astype(BF16)
 
 
-def inside_blocks(toks, w, running, leak_run, keys, values):
+def inside_blocks(toks, blocks, running, leak_run, keys, values):
     length = running.shape[1]
     block = (4, length, LANES)
+    deep, wide = blocks[0].shape
     return pl.pallas_call(
         inside_kernel,
         out_shape=(struct(block, F32), struct(block, BF16), struct(block, BF16), struct(block, BF16)),
-        in_specs=[*anywhere(8), *vmem(5)],
+        in_specs=[*anywhere(16), *vmem(4)],
         out_specs=tuple(vmem(4)),
-        scratch_shapes=token_scratch(toks[0], 3 * LANES),
+        scratch_shapes=[
+            *token_scratch(toks[0], wide),
+            pltpu.VMEM((8 * deep, wide), BF16),
+            pltpu.SemaphoreType.DMA((8,)),
+        ],
         name="inside",
-    )(*toks, w, running, leak_run, keys, values)
+    )(*toks, *blocks, running, leak_run, keys, values)
 
 
 def mix_kernel(
@@ -312,29 +333,45 @@
     )(inside, reach, state, gate, signal, rim, taps, gain)
 
 
-def out_kernel(mix_ref, near_ref, far_ref, o_ref):
+def out_kernel(mix_ref, *refs):
+    piece_refs, (o_ref, pieces, sems) = refs[:8], refs[8:]
+    copies = [pltpu.make_async_copy(ref, pieces.at[k], sems.at[k]) for k, ref in enumerate(piece_refs)]
+    for copy in copies[:4]:
+        copy.start()
     core = lax.axis_index("tp")
-    total = jnp.zeros(o_ref.shape, F32)
-    for c, w_ref in ((core, near_ref), (1 - core, far_ref)):
-        pieces = [mix_ref[2 * x + c] for x in range(4)]
-        lhs = jnp.concatenate(
-            [piece[:, :LANES] for piece in pieces] + [piece[:, LANES:] for piece in pieces], axis=1
+    x = lax.axis_index("fs")
+    rows = []
+    for c in (core, 1 - core):
+        parts = [mix_ref[2 * k + c] for k in range(4)]
+        rows.append(
+            jnp.concatenate(
+                [part[:, :LANES] for part in parts] + [part[:, LANES:] for part in parts], axis=1
+            )
         )
-        total = total + dot(lhs, w_ref[0])
-    o_ref[...] = total.astype(BF16)
-
-
-def out_rows(mix, near, far):
+    wide = piece_refs[0].shape[1]
+    for k in range(4):
+        copies[2 * k].wait()
+        copies[2 * k + 1].wait()
+        if k < 2:
+            copies[2 * k + 4].start()
+            copies[2 * k + 5].start()
+        start = pl.multiple_of((x + SLOT_SHIFT[k]) % 4 * wide, wide)
+        total = dot(rows[0], pieces[2 * k]) + dot(rows[1], pieces[2 * k + 1])
+        o_ref[:, pl.ds(start, wide)] = total.astype(BF16)
+
+
+def out_rows(mix, nears, fars):
     rows = mix.shape[1]
-    pieces, deep, wide = near.shape
+    deep, wide = nears[0].shape
+    pieces = [piece for pair in zip(nears, fars) for piece in pair]
     return pl.pallas_call(
         out_kernel,
-        out_shape=struct((rows, pieces * wide), BF16),
-        grid=(pieces,),
-        in_specs=[whole(*mix.shape), sequence_block(deep, wide), sequence_block(deep, wide)],
-        out_specs=pl.BlockSpec((rows, wide), lambda j: (0, j)),
+        out_shape=struct((rows, 4 * wide), BF16),
+        in_specs=[*vmem(1), *anywhere(8)],
+        out_specs=vmem(1)[0],
+        scratch_shapes=[pltpu.VMEM((8, deep, wide), BF16), pltpu.SemaphoreType.DMA((8,))],
         name="out",
-    )(mix, near, far)
+    )(mix, *pieces)
 
 
 def ring(array, axis, by):
@@ -365,7 +402,12 @@
     slabs = weight_slabs((forget_w, value_w, query_w, conv_gate_w, conv_in_w), 8)
     y_rows = exchanged(slabs, "sp_1").reshape(-1, slabs.shape[2])
     early, late = split_columns(y_rows, 8)
-    late_w = lax.all_gather(late, "sp_0", axis=0, tiled=True)
+    ahead, behind = [late], [late]
+    for k in range(1, 5):
+        ahead.append(ring(ahead[-1], "sp_0", 1))
+        if k < 4:
+            behind.append(ring(behind[-1], "sp_0", 7))
+    blocks = ahead + behind[:0:-1]
     early_w = exchanged(early, "sp_0").reshape(-1, early.shape[2])
 
     own = norm_rows(tokens[0], norm_gain, leak[0].T)
@@ -378,9 +420,12 @@
     toks = [part for pair in zip(near, far) for part in pair]
 
     out_w = jnp.concatenate([conv_out_w, chain_out_w], axis=0)
-    out_w, late = lax.optimization_barrier((out_w, late))
-    out_near = lax.all_gather(out_w, "fs", axis=0)
-    out_far = ring(out_near, "tp", 1)
+    out_near = [out_w]
+    for by in (1, 3, 2):
+        out_near.append(ring(out_w, "fs", by))
+    out_far = []
+    for part in out_near:
+        out_far.append(ring(part, "tp", 1))
 
     floor = lax.dynamic_slice_in_dim(floor_gate, x * LANES, LANES, 0)[None]
     states, running, leak_run, keys, values = local_states(toks, early_w, floor)
@@ -388,7 +433,7 @@
     before = exchanged(scan_blocks(arrived), SP)
     before = before.reshape(4, LANES, LANES)
 
-    inside, reach, gate, signal = inside_blocks(toks, late_w, running, leak_run, keys, values)
+    inside, reach, gate, signal = inside_blocks(toks, blocks, running, leak_run, keys, values)
     count = 64
     tail = signal[:, -16:, :]
     rim = lax.ppermute(tail, SP, [(i, i + 1) for i in range(count - 1)])

time: 248 us -> 219 us (0.88)
  starting transfers between devices: 62.2 us -> 128 us
  blocking collectives: 45.1 us -> 0 us
  waiting for transfers between devices: 77.8 us -> 40.4 us
  between operations: 15 us -> 0.7 us
  local copies, waits for them, and re-layouts: 3.69 us -> 7.76 us
    all_gather x2 -> x0, waiting for transfers between devices: 56.3 us -> none  [the longest x1 56.3 us: layer(): out_near = lax.all_gather(out_w, 'fs', axis=0)]
    all_to_all x2 -> x0, blocking collectives: 45.1 us -> none  [exchanged(): return lax.all_to_all(array, axis, split_axis=0, concat_axis=0, tiled=True)]
    ppermute x8 -> x21, starting transfers between devices: 39.1 us -> 83.4 us  [ring(): lax.ppermute(array, axis, [(i, (i + by) % count) for i in range(count)])]
    all_to_all x3 -> x5, starting transfers between devices: 20.3 us -> 41.8 us  [exchanged(): return lax.all_to_all(array, axis, split_axis=0, concat_axis=0, tiled=True)]
    ppermute x8 -> x21, waiting for transfers between devices: 12.8 us -> 23 us  [ring(): lax.ppermute(array, axis, [(i, (i + by) % count) for i in range(count)])]
    all_to_all x3 -> x5, waiting for transfers between devices: 7.79 us -> 16.5 us  [exchanged(): return lax.all_to_all(array, axis, split_axis=0, concat_axis=0, tiled=True)]
    unnamed x16 -> x49, local copies, waits for them, and re-layouts: 2.3 us -> 5.6 us
  transfers between devices with their start and end apart: 14 -> 27, of which waited for: 5 -> 6; matrix products, arithmetic and copies ran while one was open for 2% -> 1% of each run, Pallas kernels for 12% -> 15%
where the time goes in v2:
time: 219 us; the launch traced here: 217 us
  starting transfers between devices  128 us (58%)
  Pallas kernels  40.4 us (18%)
  waiting for transfers between devices  40.4 us (18%)
  local copies, waits for them, and re-layouts  7.76 us (4%)
    ppermute x21, starting transfers between devices, ring(): lax.ppermute(array, axis, [(i, (i + by) % count) for i in range(count)])  83.4 us
    all_to_all x5, starting transfers between devices, exchanged(): return lax.all_to_all(array, axis, split_axis=0, concat_axis=0, tiled=True)  41.8 us
    ppermute x21, waiting for transfers between devices, ring(): lax.ppermute(array, axis, [(i, (i + by) % count) for i in range(count)])  23 us
    all_to_all x5, waiting for transfers between devices, exchanged(): return lax.all_to_all(array, axis, split_axis=0, concat_axis=0, tiled=True)  16.5 us
    pallas_call x1, Pallas kernels, inside_blocks(): pl.pallas_call(inside_kernel, out_shape=(struct(block, F32), struct(block...  10.9 us
    pallas_call x1, Pallas kernels, local_states(): pl.pallas_call(state_kernel, out_shape=(struct((64, 16, LANES), BF16), st...  10.7 us
    pallas_call x1, Pallas kernels, out_rows(): pl.pallas_call(out_kernel, out_shape=struct((rows, 4 * wide), BF16), in_s...  6.49 us
    unnamed x49, local copies, waits for them, and re-layouts  5.6 us
  transfers between devices with their start and end apart: 27, of which 6 were waited for; matrix products, arithmetic and copies ran while one was open for 1% of the time, Pallas kernels for 15%

profile of v2, /device:TPU:1, one launch (start us, length us, event | category | flops | bytes accessed | tf_op | source)
XLA Modules:
  0.0 217.3 jit_solution(10626859390189162604)
XLA Ops:
  1.6 7.6 %all-to-all-start = ((bf16[8,32,640]{2,1,0:T(8,128)(2,1)}), bf16[8,32,640]{2,1,0:T(8,128)(2,1)S(1)}, u32[]{:S(2)}, u32[]{:S(2)}) async-start(bf16[8,32,640]{2,1,0:T(8,128)(2,1)} %slab.1), calls=%async_computation | async-start | bytes 655360 | tf_op jit(solution)/shard_map/all_to_all | solution.py:383
  11.9 3.1 %collective-permute-start.1 = (bf16[200,2048]{1,0:T(8,128)(2,1)}, bf16[200,2048]{1,0:T(8,128)(2,1)S(1)}, u32[]{:S(2)}, u32[]{:S(2)}) collective-permute-start(bf16[200,2048]{1,0:T(8,128)(2,1)} %norm.1.refs_0_), channel_id=1, source_target_pairs={{0,2},{2,4},{4,6},{6,0},{1,3},{3,5},{5,7},{7,1},{8,10},{10,12},{12... | collective-permute-start | bytes 2457608 | tf_op jit(solution)/shard_map/ppermute | solution.py:379
  15.0 4.4 %all-to-all-done = bf16[8,32,640]{2,1,0:T(8,128)(2,1)S(1)} async-done(((bf16[8,32,640]{2,1,0:T(8,128)(2,1)}), bf16[8,32,640]{2,1,0:T(8,128)(2,1)S(1)}, u32[]{:S(2)}, u32[]{:S(2)}) %all-to-all-start) | async-done | bytes 327712 | tf_op jit(solution)/shard_map/all_to_all | solution.py:383
  22.2 12.1 %all-to-all-start.1 = ((bf16[8,256,256]{2,1,0:T(8,128)(2,1)}), bf16[8,256,256]{2,1,0:T(8,128)(2,1)S(1)}, u32[]{:S(2)}, u32[]{:S(2)}) async-start(bf16[8,256,256]{2,1,0:T(8,128)(2,1)} %get-tuple-element.17), calls=%async_computation.1 | async-start | bytes 2097152 | tf_op jit(solution)/shard_map/all_to_all | solution.py:383
  34.3 4.5 %collective-permute-start.3 = (bf16[200,2048]{1,0:T(8,128)(2,1)S(1)}, bf16[200,2048]{1,0:T(8,128)(2,1)S(1)}, u32[]{:S(2)}, u32[]{:S(2)}) collective-permute-start(bf16[200,2048]{1,0:T(8,128)(2,1)S(1)} %copy-done.1), channel_id=1, source_target_pairs={{0,6},{2,0},{4,2},{6,4},{1,7},{3,1},{5,3},{7,5},{8,14},{10,8},{12,... | collective-permute-start | bytes 2457608 | tf_op jit(solution)/shard_map/ppermute | solution.py:379
  41.3 4.9 %collective-permute-start = (bf16[200,2048]{1,0:T(8,128)(2,1)S(1)}, bf16[200,2048]{1,0:T(8,128)(2,1)S(1)}, u32[]{:S(2)}, u32[]{:S(2)}) collective-permute-start(bf16[200,2048]{1,0:T(8,128)(2,1)S(1)} %copy-done.1), channel_id=1, source_target_pairs={{0,1},{1,0},{2,3},{3,2},{4,5},{5,4},{6,7},{7,6},{8,9},{9,8},{10,11... | collective-permute-start | bytes 2457608 | tf_op jit(solution)/shard_map/ppermute | solution.py:379
  48.1 6.7 %collective-permute-done.3.refs_4_ = bf16[200,2048]{1,0:T(8,128)(2,1)S(1)} collective-permute-done((bf16[200,2048]{1,0:T(8,128)(2,1)S(1)}, bf16[200,2048]{1,0:T(8,128)(2,1)S(1)}, u32[]{:S(2)}, u32[]{:S(2)}) %collective-permute-start.3) | collective-permute-done | bytes 819232 | tf_op jit(solution)/shard_map/ppermute | solution.py:379
  54.8 22.0 %collective-permute-start.4 = (bf16[200,2048]{1,0:T(8,128)(2,1)S(1)}, bf16[200,2048]{1,0:T(8,128)(2,1)S(1)}, u32[]{:S(2)}, u32[]{:S(2)}) collective-permute-start(bf16[200,2048]{1,0:T(8,128)(2,1)S(1)} %collective-permute-done.3.refs_4_), channel_id=1, source_target_pairs={{0,1},{1,0},{2,3},{3,2},{4,5},{5,4},{6,7},{7,6},{8,9},{9,8},{10,11... | collective-permute-start | bytes 2457608 | tf_op jit(solution)/shard_map/ppermute | solution.py:379
  82.4 5.3 %collective-permute-start.18 = (bf16[1024,512]{1,0:T(8,128)(2,1)}, bf16[1024,512]{1,0:T(8,128)(2,1)S(1)}, u32[]{:S(2)}, u32[]{:S(2)}) collective-permute-start(bf16[1024,512]{1,0:T(8,128)(2,1)} %constant_dynamic-update-slice_fusion.refs_0_), channel_id=1, source_target_pairs={{0,6},{2,0},{4,2},{6,4},{1,7},{3,1},{5,3},{7,5},{8,14},{10,8},{12,... | collective-permute-start | bytes 3145736 | tf_op jit(solution)/shard_map/ppermute | solution.py:379
  90.8 3.4 %collective-permute-start.7 = (bf16[256,384]{1,0:T(8,128)(2,1)S(1)}, bf16[256,384]{1,0:T(8,128)(2,1)S(1)}, u32[]{:S(2)}, u32[]{:S(2)}) collective-permute-start(bf16[256,384]{1,0:T(8,128)(2,1)S(1)} %copy-done.16), channel_id=1, source_target_pairs={{0,64},{64,128},{128,192},{192,256},{256,320},{320,384},{384,448},... | collective-permute-start | bytes 589832 | tf_op jit(solution)/shard_map/ppermute | solution.py:379
  94.2 3.1 %collective-permute-start.11 = (bf16[256,384]{1,0:T(8,128)(2,1)S(1)}, bf16[256,384]{1,0:T(8,128)(2,1)S(1)}, u32[]{:S(2)}, u32[]{:S(2)}) collective-permute-start(bf16[256,384]{1,0:T(8,128)(2,1)S(1)} %copy-done.16), channel_id=1, source_target_pairs={{0,448},{64,0},{128,64},{192,128},{256,192},{320,256},{384,320},{4... | collective-permute-start | bytes 589832 | tf_op jit(solution)/shard_map/ppermute | solution.py:379
  99.0 10.7 %states.1 = (bf16[64,16,128]{2,1,0:T(8,128)(2,1)}, f32[4,384,128]{2,1,0:T(8,128)}, f32[4,384,128]{2,1,0:T(8,128)}, f32[4,384,128]{2,1,0:T(8,128)}, bf16[4,384,128]{2,1,0:T(8,128)(2,1)}) custom-call(bf16[200,2048]{1,0:T(8,128)(2,1)} %norm.1.refs_0_, bf16[200,2048]{1,0:T(8,128)(2,1)} %copy-done.5, bf16[200,2048]{1,0:T(8,128)(2,1)} %copy-done.3, ...), custom_call_target="tpu_custom_call" | custom-call | tf_op jit(solution)/shard_map/states/pallas_call | solution.py:184
  109.7 8.4 %all-to-all-start.2 = ((bf16[64,16,128]{2,1,0:T(8,128)(2,1)}), bf16[64,16,128]{2,1,0:T(8,128)(2,1)S(1)}, u32[]{:S(2)}, u32[]{:S(2)}) async-start(bf16[64,16,128]{2,1,0:T(8,128)(2,1)} %get-tuple-element.24), calls=%async_computation.2 | async-start | bytes 524288 | tf_op jit(solution)/shard_map/all_to_all | solution.py:383
  121.1 3.6 %collective-permute-start.12 = (bf16[256,384]{1,0:T(8,128)(2,1)S(1)}, bf16[256,384]{1,0:T(8,128)(2,1)S(1)}, u32[]{:S(2)}, u32[]{:S(2)}) collective-permute-start(bf16[256,384]{1,0:T(8,128)(2,1)S(1)} %collective-permute-done.11.refs_15_), channel_id=1, source_target_pairs={{0,448},{64,0},{128,64},{192,128},{256,192},{320,256},{384,320},{4... | collective-permute-start | bytes 589832 | tf_op jit(solution)/shard_map/ppermute | solution.py:379
  124.6 7.8 %collective-permute-done.8.refs_10_ = bf16[256,384]{1,0:T(8,128)(2,1)S(1)} collective-permute-done((bf16[256,384]{1,0:T(8,128)(2,1)S(1)}, bf16[256,384]{1,0:T(8,128)(2,1)S(1)}, u32[]{:S(2)}, u32[]{:S(2)}) %collective-permute-start.8) | collective-permute-done | bytes 196640 | tf_op jit(solution)/shard_map/ppermute | solution.py:379
  134.4 4.6 %collective-permute-start.13 = (bf16[256,384]{1,0:T(8,128)(2,1)S(1)}, bf16[256,384]{1,0:T(8,128)(2,1)}, u32[]{:S(2)}, u32[]{:S(2)}) collective-permute-start(bf16[256,384]{1,0:T(8,128)(2,1)S(1)} %collective-permute-done.12.refs_14_), channel_id=1, source_target_pairs={{0,448},{64,0},{128,64},{192,128},{256,192},{320,256},{384,320},{4... | collective-permute-start | bytes 589832 | tf_op jit(solution)/shard_map/ppermute | solution.py:379
  139.0 3.6 %collective-permute-start.15 = (bf16[1024,512]{1,0:T(8,128)(2,1)}, bf16[1024,512]{1,0:T(8,128)(2,1)S(1)}, u32[]{:S(2)}, u32[]{:S(2)}) collective-permute-start(bf16[1024,512]{1,0:T(8,128)(2,1)} %constant_dynamic-update-slice_fusion.refs_0_), channel_id=1, source_target_pairs={{0,1},{1,0},{2,3},{3,2},{4,5},{5,4},{6,7},{7,6},{8,9},{9,8},{10,11... | collective-permute-start | bytes 3145736 | tf_op jit(solution)/shard_map/ppermute | solution.py:379
  151.5 8.2 %all-to-all-start.3 = ((bf16[64,8,128]{2,1,0:T(8,128)(2,1)}), bf16[64,8,128]{2,1,0:T(8,128)(2,1)S(1)}, u32[]{:S(2)}, u32[]{:S(2)}) async-start(bf16[64,8,128]{2,1,0:T(8,128)(2,1)} %scan.1), calls=%async_computation.3 | async-start | bytes 262144 | tf_op jit(solution)/shard_map/all_to_all | solution.py:383
  162.8 8.5 %collective-permute-done.10.refs_12_ = bf16[256,384]{1,0:T(8,128)(2,1)S(1)} collective-permute-done((bf16[256,384]{1,0:T(8,128)(2,1)S(1)}, bf16[256,384]{1,0:T(8,128)(2,1)S(1)}, u32[]{:S(2)}, u32[]{:S(2)}) %collective-permute-start.10) | collective-permute-done | bytes 196640 | tf_op jit(solution)/shard_map/ppermute | solution.py:379
  172.0 10.9 %inside.1 = (f32[4,384,128]{2,1,0:T(8,128)}, bf16[4,384,128]{2,1,0:T(8,128)(2,1)}, bf16[4,384,128]{2,1,0:T(8,128)(2,1)}, bf16[4,384,128]{2,1,0:T(8,128)(2,1)}) custom-call(bf16[200,2048]{1,0:T(8,128)(2,1)} %norm.1.refs_0_, bf16[200,2048]{1,0:T(8,128)(2,1)} %copy-done.5, bf16[200,2048]{1,0:T(8,128)(2,1)} %copy-done.3, bf16[200,2048]{1,0:T(8,128)(2,1)} %copy-done.6, ...), custom_call_target="tpu_custom_call" | custom-call | tf_op jit(solution)/shard_map/inside/pallas_call | solution.py:273
  187.9 4.1 %mix.1 = bf16[8,192,256]{2,1,0:T(8,128)(2,1)} custom-call(f32[4,384,128]{2,1,0:T(8,128)} %get-tuple-element.22.inside_ref, bf16[4,384,128]{2,1,0:T(8,128)(2,1)} %get-tuple-element.23.reach_ref, bf16[4,128,128]{2,1,0:T(8,128)(2,1)} %bitcast.15, bf16[4,384,128]{2,1,0:T(8,128)(2,1)} %get-tuple-element.25.gate_ref, ...), custom_call_target="tpu_custom_call" | custom-call | tf_op jit(solution)/shard_map/mix/pallas_call | solution.py:316
  192.0 5.5 %all-to-all-start.4 = ((bf16[8,192,256]{2,1,0:T(8,128)(2,1)}), bf16[8,192,256]{2,1,0:T(8,128)(2,1)S(1)}, u32[]{:S(2)}, u32[]{:S(2)}) async-start(bf16[8,192,256]{2,1,0:T(8,128)(2,1)} %mix.1), calls=%async_computation.4 | async-start | bytes 1572864 | tf_op jit(solution)/shard_map/all_to_all | solution.py:383
  197.6 12.1 %all-to-all-done.4.mix_ref = bf16[8,192,256]{2,1,0:T(8,128)(2,1)S(1)} async-done(((bf16[8,192,256]{2,1,0:T(8,128)(2,1)}), bf16[8,192,256]{2,1,0:T(8,128)(2,1)S(1)}, u32[]{:S(2)}, u32[]{:S(2)}) %all-to-all-start.4) | async-done | bytes 786464 | tf_op jit(solution)/shard_map/all_to_all | solution.py:383
  210.6 6.5 %out.1 = bf16[192,2048]{1,0:T(8,128)(2,1)} custom-call(bf16[8,192,256]{2,1,0:T(8,128)(2,1)} %copy-done.8, bf16[1024,512]{1,0:T(8,128)(2,1)} %constant_dynamic-update-slice_fusion.refs_0_, bf16[1024,512]{1,0:T(8,128)(2,1)} %copy-done.11, bf16[1024,512]{1,0:T(8,128)(2,1)} %collective-permute-done.16.refs_2_, ...), custom_call_target="tpu_custom_call" | custom-call | tf_op jit(solution)/shard_map/out/pallas_call | solution.py:367
  (90 shorter events, 45.0 us)
Async XLA Ops:
  1.6 17.8 %all-to-all-start = ((bf16[8,32,640]{2,1,0:T(8,128)(2,1)}), bf16[8,32,640]{2,1,0:T(8,128)(2,1)S(1)}, u32[]{:S(2)}, u32[]{:S(2)}) async-start(bf16[8,32,640]{2,1,0:T(8,128)(2,1)} %slab.1), calls=%async_computation | async-start | bytes 655360 | tf_op jit(solution)/shard_map/all_to_all | solution.py:383
  11.9 34.3 %collective-permute-start.1 = (bf16[200,2048]{1,0:T(8,128)(2,1)}, bf16[200,2048]{1,0:T(8,128)(2,1)S(1)}, u32[]{:S(2)}, u32[]{:S(2)}) collective-permute-start(bf16[200,2048]{1,0:T(8,128)(2,1)} %norm.1.refs_0_), channel_id=1, source_target_pairs={{0,2},{2,4},{4,6},{6,0},{1,3},{3,5},{5,7},{7,1},{8,10},{10,12},{12... | collective-permute-start | bytes 2457608 | tf_op jit(solution)/shard_map/ppermute | solution.py:379
  22.2 75.8 %all-to-all-start.1 = ((bf16[8,256,256]{2,1,0:T(8,128)(2,1)}), bf16[8,256,256]{2,1,0:T(8,128)(2,1)S(1)}, u32[]{:S(2)}, u32[]{:S(2)}) async-start(bf16[8,256,256]{2,1,0:T(8,128)(2,1)} %get-tuple-element.17), calls=%async_computation.1 | async-start | bytes 2097152 | tf_op jit(solution)/shard_map/all_to_all | solution.py:383
  34.3 20.5 %collective-permute-start.3 = (bf16[200,2048]{1,0:T(8,128)(2,1)S(1)}, bf16[200,2048]{1,0:T(8,128)(2,1)S(1)}, u32[]{:S(2)}, u32[]{:S(2)}) collective-permute-start(bf16[200,2048]{1,0:T(8,128)(2,1)S(1)} %copy-done.1), channel_id=1, source_target_pairs={{0,6},{2,0},{4,2},{6,4},{1,7},{3,1},{5,3},{7,5},{8,14},{10,8},{12,... | collective-permute-start | bytes 2457608 | tf_op jit(solution)/shard_map/ppermute | solution.py:379
  38.9 37.9 %collective-permute-start.5 = (bf16[200,2048]{1,0:T(8,128)(2,1)S(1)}, bf16[200,2048]{1,0:T(8,128)(2,1)}, u32[]{:S(2)}, u32[]{:S(2)}) collective-permute-start(bf16[200,2048]{1,0:T(8,128)(2,1)S(1)} %copy-done.1), channel_id=1, source_target_pairs={{0,4},{2,6},{4,0},{6,2},{1,5},{3,7},{5,1},{7,3},{8,12},{10,14},{12... | collective-permute-start | bytes 2457608 | tf_op jit(solution)/shard_map/ppermute | solution.py:379
  41.3 41.1 %collective-permute-start = (bf16[200,2048]{1,0:T(8,128)(2,1)S(1)}, bf16[200,2048]{1,0:T(8,128)(2,1)S(1)}, u32[]{:S(2)}, u32[]{:S(2)}) collective-permute-start(bf16[200,2048]{1,0:T(8,128)(2,1)S(1)} %copy-done.1), channel_id=1, source_target_pairs={{0,1},{1,0},{2,3},{3,2},{4,5},{5,4},{6,7},{7,6},{8,9},{9,8},{10,11... | collective-permute-start | bytes 2457608 | tf_op jit(solution)/shard_map/ppermute | solution.py:379
  46.2 41.5 %collective-permute-start.2 = (bf16[200,2048]{1,0:T(8,128)(2,1)S(1)}, bf16[200,2048]{1,0:T(8,128)(2,1)S(1)}, u32[]{:S(2)}, u32[]{:S(2)}) collective-permute-start(bf16[200,2048]{1,0:T(8,128)(2,1)S(1)} %collective-permute-done.1.refs_2_), channel_id=1, source_target_pairs={{0,1},{1,0},{2,3},{3,2},{4,5},{5,4},{6,7},{7,6},{8,9},{9,8},{10,11... | collective-permute-start | bytes 2457608 | tf_op jit(solution)/shard_map/ppermute | solution.py:379
  54.8 36.0 %collective-permute-start.4 = (bf16[200,2048]{1,0:T(8,128)(2,1)S(1)}, bf16[200,2048]{1,0:T(8,128)(2,1)S(1)}, u32[]{:S(2)}, u32[]{:S(2)}) collective-permute-start(bf16[200,2048]{1,0:T(8,128)(2,1)S(1)} %collective-permute-done.3.refs_4_), channel_id=1, source_target_pairs={{0,1},{1,0},{2,3},{3,2},{4,5},{5,4},{6,7},{7,6},{8,9},{9,8},{10,11... | collective-permute-start | bytes 2457608 | tf_op jit(solution)/shard_map/ppermute | solution.py:379
  76.8 17.4 %collective-permute-start.6 = (bf16[200,2048]{1,0:T(8,128)(2,1)}, bf16[200,2048]{1,0:T(8,128)(2,1)}, u32[]{:S(2)}, u32[]{:S(2)}) collective-permute-start(bf16[200,2048]{1,0:T(8,128)(2,1)} %collective-permute-done.5.refs_6_), channel_id=1, source_target_pairs={{0,1},{1,0},{2,3},{3,2},{4,5},{5,4},{6,7},{7,6},{8,9},{9,8},{10,11... | collective-permute-start | bytes 2457608 | tf_op jit(solution)/shard_map/ppermute | solution.py:379
  80.4 58.6 %collective-permute-start.16 = (bf16[1024,512]{1,0:T(8,128)(2,1)}, bf16[1024,512]{1,0:T(8,128)(2,1)}, u32[]{:S(2)}, u32[]{:S(2)}) collective-permute-start(bf16[1024,512]{1,0:T(8,128)(2,1)} %constant_dynamic-update-slice_fusion.refs_0_), channel_id=1, source_target_pairs={{0,2},{2,4},{4,6},{6,0},{1,3},{3,5},{5,7},{7,1},{8,10},{10,12},{12... | collective-permute-start | bytes 3145736 | tf_op jit(solution)/shard_map/ppermute | solution.py:379
  82.4 60.2 %collective-permute-start.18 = (bf16[1024,512]{1,0:T(8,128)(2,1)}, bf16[1024,512]{1,0:T(8,128)(2,1)S(1)}, u32[]{:S(2)}, u32[]{:S(2)}) collective-permute-start(bf16[1024,512]{1,0:T(8,128)(2,1)} %constant_dynamic-update-slice_fusion.refs_0_), channel_id=1, source_target_pairs={{0,6},{2,0},{4,2},{6,4},{1,7},{3,1},{5,3},{7,5},{8,14},{10,8},{12,... | collective-permute-start | bytes 3145736 | tf_op jit(solution)/shard_map/ppermute | solution.py:379
  87.7 56.9 %collective-permute-start.20 = (bf16[1024,512]{1,0:T(8,128)(2,1)}, bf16[1024,512]{1,0:T(8,128)(2,1)}, u32[]{:S(2)}, u32[]{:S(2)}) collective-permute-start(bf16[1024,512]{1,0:T(8,128)(2,1)} %constant_dynamic-update-slice_fusion.refs_0_), channel_id=1, source_target_pairs={{0,4},{2,6},{4,0},{6,2},{1,5},{3,7},{5,1},{7,3},{8,12},{10,14},{12... | collective-permute-start | bytes 3145736 | tf_op jit(solution)/shard_map/ppermute | solution.py:379
  90.8 27.3 %collective-permute-start.7 = (bf16[256,384]{1,0:T(8,128)(2,1)S(1)}, bf16[256,384]{1,0:T(8,128)(2,1)S(1)}, u32[]{:S(2)}, u32[]{:S(2)}) collective-permute-start(bf16[256,384]{1,0:T(8,128)(2,1)S(1)} %copy-done.16), channel_id=1, source_target_pairs={{0,64},{64,128},{128,192},{192,256},{256,320},{320,384},{384,448},... | collective-permute-start | bytes 589832 | tf_op jit(solution)/shard_map/ppermute | solution.py:379
  94.2 26.8 %collective-permute-start.11 = (bf16[256,384]{1,0:T(8,128)(2,1)S(1)}, bf16[256,384]{1,0:T(8,128)(2,1)S(1)}, u32[]{:S(2)}, u32[]{:S(2)}) collective-permute-start(bf16[256,384]{1,0:T(8,128)(2,1)S(1)} %copy-done.16), channel_id=1, source_target_pairs={{0,448},{64,0},{128,64},{192,128},{256,192},{320,256},{384,320},{4... | collective-permute-start | bytes 589832 | tf_op jit(solution)/shard_map/ppermute | solution.py:379
  109.7 39.2 %all-to-all-start.2 = ((bf16[64,16,128]{2,1,0:T(8,128)(2,1)}), bf16[64,16,128]{2,1,0:T(8,128)(2,1)S(1)}, u32[]{:S(2)}, u32[]{:S(2)}) async-start(bf16[64,16,128]{2,1,0:T(8,128)(2,1)} %get-tuple-element.24), calls=%async_computation.2 | async-start | bytes 524288 | tf_op jit(solution)/shard_map/all_to_all | solution.py:383
  118.1 14.4 %collective-permute-start.8 = (bf16[256,384]{1,0:T(8,128)(2,1)S(1)}, bf16[256,384]{1,0:T(8,128)(2,1)S(1)}, u32[]{:S(2)}, u32[]{:S(2)}) collective-permute-start(bf16[256,384]{1,0:T(8,128)(2,1)S(1)} %collective-permute-done.7.refs_9_), channel_id=1, source_target_pairs={{0,64},{64,128},{128,192},{192,256},{256,320},{320,384},{384,448},... | collective-permute-start | bytes 589832 | tf_op jit(solution)/shard_map/ppermute | solution.py:379
  132.5 14.5 %collective-permute-start.9 = (bf16[256,384]{1,0:T(8,128)(2,1)S(1)}, bf16[256,384]{1,0:T(8,128)(2,1)S(1)}, u32[]{:S(2)}, u32[]{:S(2)}) collective-permute-start(bf16[256,384]{1,0:T(8,128)(2,1)S(1)} %collective-permute-done.8.refs_10_), channel_id=1, source_target_pairs={{0,64},{64,128},{128,192},{192,256},{256,320},{320,384},{384,448},... | collective-permute-start | bytes 589832 | tf_op jit(solution)/shard_map/ppermute | solution.py:379
  134.4 25.2 %collective-permute-start.13 = (bf16[256,384]{1,0:T(8,128)(2,1)S(1)}, bf16[256,384]{1,0:T(8,128)(2,1)}, u32[]{:S(2)}, u32[]{:S(2)}) collective-permute-start(bf16[256,384]{1,0:T(8,128)(2,1)S(1)} %collective-permute-done.12.refs_14_), channel_id=1, source_target_pairs={{0,448},{64,0},{128,64},{192,128},{256,192},{320,256},{384,320},{4... | collective-permute-start | bytes 589832 | tf_op jit(solution)/shard_map/ppermute | solution.py:379
  139.0 58.5 %collective-permute-start.15 = (bf16[1024,512]{1,0:T(8,128)(2,1)}, bf16[1024,512]{1,0:T(8,128)(2,1)S(1)}, u32[]{:S(2)}, u32[]{:S(2)}) collective-permute-start(bf16[1024,512]{1,0:T(8,128)(2,1)} %constant_dynamic-update-slice_fusion.refs_0_), channel_id=1, source_target_pairs={{0,1},{1,0},{2,3},{3,2},{4,5},{5,4},{6,7},{7,6},{8,9},{9,8},{10,11... | collective-permute-start | bytes 3145736 | tf_op jit(solution)/shard_map/ppermute | solution.py:379
  142.6 54.9 %collective-permute-start.17 = (bf16[1024,512]{1,0:T(8,128)(2,1)}, bf16[1024,512]{1,0:T(8,128)(2,1)}, u32[]{:S(2)}, u32[]{:S(2)}) collective-permute-start(bf16[1024,512]{1,0:T(8,128)(2,1)} %collective-permute-done.16.refs_2_), channel_id=1, source_target_pairs={{0,1},{1,0},{2,3},{3,2},{4,5},{5,4},{6,7},{7,6},{8,9},{9,8},{10,11... | collective-permute-start | bytes 3145736 | tf_op jit(solution)/shard_map/ppermute | solution.py:379
  144.6 53.0 %collective-permute-start.19 = (bf16[1024,512]{1,0:T(8,128)(2,1)S(1)}, bf16[1024,512]{1,0:T(8,128)(2,1)}, u32[]{:S(2)}, u32[]{:S(2)}) collective-permute-start(bf16[1024,512]{1,0:T(8,128)(2,1)S(1)} %collective-permute-done.18.refs_4_), channel_id=1, source_target_pairs={{0,1},{1,0},{2,3},{3,2},{4,5},{5,4},{6,7},{7,6},{8,9},{9,8},{10,11... | collective-permute-start | bytes 3145736 | tf_op jit(solution)/shard_map/ppermute | solution.py:379
  147.0 50.6 %collective-permute-start.21 = (bf16[1024,512]{1,0:T(8,128)(2,1)}, bf16[1024,512]{1,0:T(8,128)(2,1)}, u32[]{:S(2)}, u32[]{:S(2)}) collective-permute-start(bf16[1024,512]{1,0:T(8,128)(2,1)} %collective-permute-done.20.refs_6_), channel_id=1, source_target_pairs={{0,1},{1,0},{2,3},{3,2},{4,5},{5,4},{6,7},{7,6},{8,9},{9,8},{10,11... | collective-permute-start | bytes 3145736 | tf_op jit(solution)/shard_map/ppermute | solution.py:379
  151.5 35.8 %all-to-all-start.3 = ((bf16[64,8,128]{2,1,0:T(8,128)(2,1)}), bf16[64,8,128]{2,1,0:T(8,128)(2,1)S(1)}, u32[]{:S(2)}, u32[]{:S(2)}) async-start(bf16[64,8,128]{2,1,0:T(8,128)(2,1)} %scan.1), calls=%async_computation.3 | async-start | bytes 262144 | tf_op jit(solution)/shard_map/all_to_all | solution.py:383
  192.0 17.7 %all-to-all-start.4 = ((bf16[8,192,256]{2,1,0:T(8,128)(2,1)}), bf16[8,192,256]{2,1,0:T(8,128)(2,1)S(1)}, u32[]{:S(2)}, u32[]{:S(2)}) async-start(bf16[8,192,256]{2,1,0:T(8,128)(2,1)} %mix.1), calls=%async_computation.4 | async-start | bytes 1572864 | tf_op jit(solution)/shard_map/all_to_all | solution.py:383
  (27 other events, 590.5 us)

commit v3 on v1

--- a/solution.py
+++ b/solution.py
@@ -21,12 +21,12 @@
     return [pl.BlockSpec(memory_space=pltpu.VMEM) for _ in range(count)]
 
 
-def split3(values):
-    high = values.astype(BF16)
-    rest = values - high.astype(F32)
-    middle = rest.astype(BF16)
-    low = (rest - middle.astype(F32)).astype(BF16)
-    return high, middle, low
+def split_parts(values, count):
+    parts = []
+    for _ in range(count):
+        parts.append(values.astype(BF16))
+        values = values - parts[-1].astype(F32)
+    return parts
 
 
 def dot(a, b, dims=((1,), (0,))):
@@ -39,8 +39,15 @@
     center = values - jnp.mean(values, axis=-1, keepdims=True)
     spread = jnp.mean(center * center, axis=-1, keepdims=True)
     o_ref[:rows, :] = (center * lax.rsqrt(spread + 1e-05) * gain_ref[...]).astype(BF16)
-    leaks = jnp.concatenate([leak_ref[h : h + 1, :] for h in range(leak_ref.shape[0])], axis=1)
-    parts = [part.astype(F32) for part in split3(leaks)]
+    heads, length = leak_ref.shape
+    parts = [part.astype(F32) for part in split_parts(leak_ref[...], 3)]
+    both = jnp.concatenate([*parts, jnp.zeros_like(parts[0])], axis=0).astype(BF16)
+    ahead = lax.broadcasted_iota(jnp.int32, (length, length), 0)
+    here = lax.broadcasted_iota(jnp.int32, (length, length), 1)
+    sums = dot(both, (ahead <= here).astype(F32).astype(BF16))
+    total = sums[:heads] + sums[heads : 2 * heads] + sums[2 * heads : 3 * heads]
+    leaks = jnp.concatenate([total[h : h + 1, :] for h in range(heads)], axis=1)
+    parts = [part.astype(F32) for part in split_parts(leaks, 3)]
     tail = jnp.concatenate([*parts, jnp.zeros((8 - len(parts), leaks.shape[1]), F32)], axis=0)
     unused = jnp.zeros((8, o_ref.shape[1] - leaks.shape[1]), F32)
     o_ref[rows:, :] = jnp.concatenate([tail, unused], axis=1).astype(BF16)
@@ -75,23 +82,17 @@
     )(*weights)
 
 
-def relay_kernel(in_ref, early_ref, late_ref):
-    early = in_ref[:, : 2 * LANES]
-    for k in range(early_ref.shape[0]):
-        early_ref[k] = early
-    late_ref[...] = in_ref[:, 2 * LANES :]
-
-
-def split_columns(rows, copies):
-    deep, wide = rows.shape
+def relay_kernel(in_ref, o_ref):
+    o_ref[...] = in_ref[...]
+
+
+def relayed(rows):
     return pl.pallas_call(
         relay_kernel,
-        out_shape=(
-            struct((copies, deep, 2 * LANES), BF16),
-            struct((deep, wide - 2 * LANES), BF16),
-        ),
+        out_shape=struct(rows.shape, rows.dtype),
         in_specs=vmem(1),
-        out_specs=tuple(vmem(2)),
+        out_specs=vmem(1)[0],
+        compiler_params=pltpu.CompilerParams(vmem_limit_bytes=2 << 20),
         name="relay",
     )(rows)
 
@@ -114,40 +115,44 @@
     return row >= col
 
 
-def running_sum(tri, values):
-    width = values.shape[1]
-    parts = dot(tri, jnp.concatenate(split3(values), axis=1))
-    return parts[:, :width] + parts[:, width : 2 * width] + parts[:, 2 * width :]
+def gates(logits, gap, tri):
+    keys = gap * jax.nn.sigmoid(-logits.astype(F32))
+    parts = dot(tri, jnp.concatenate(split_parts(jnp.log1p(-keys), 2), axis=1))
+    return keys, parts[:, :LANES] + parts[:, LANES:]
+
+
+def leak_row(toks, r, length):
+    first = pl.multiple_of(lax.axis_index("fs") * length, LANES)
+    coded = toks[2 * r, length // 2 :, pl.ds(first, length)].astype(F32)
+    return jnp.sum(coded, axis=0, keepdims=True)
 
 
 def state_kernel(*refs):
     tok_refs, rest = refs[:8], refs[8:]
-    w_ref, floor_ref, state_ref, run_ref, leak_ref, keys_ref, value_ref, raw, toks, sems = rest
+    w_ref, floor_ref, state_ref, raw_ref, toks, sems, weights, w_sem = rest
+    w_copy = pltpu.make_async_copy(w_ref.at[:, : 2 * LANES], weights, w_sem)
     copies = fetches(tok_refs, toks, sems)
-    for copy in copies:
+    for copy in [w_copy] + copies[:4]:
         copy.start()
-    length = run_ref.shape[1]
-    half = length // 2
+    length = raw_ref.shape[1]
     tri = lower_triangle(length).astype(F32).astype(BF16)
     gap = 1.0 - floor_ref[...]
     lane = lax.broadcasted_iota(jnp.int32, (LANES, LANES), 1)
-    first = pl.multiple_of(lax.axis_index("fs") * length, LANES)
-    w = w_ref[...]
+    w_copy.wait()
+    w = weights[...]
     for r in range(4):
         copies[2 * r].wait()
         copies[2 * r + 1].wait()
-        coded = toks[2 * r, half:, pl.ds(first, length)].astype(F32)
-        leaks = jnp.sum(coded, axis=0, keepdims=True)
-        leak_rows = jnp.broadcast_to(leaks, (LANES, length))
-        place_rows(raw, toks, r, w)
-        keys = gap * jax.nn.sigmoid(-raw[:, :LANES].astype(F32))
-        values = raw[:, LANES:]
-        both = running_sum(tri, jnp.concatenate([jnp.log1p(-keys), leak_rows.T], axis=1))
-        running, leak_run = both[:, :LANES], both[:, LANES:]
-        total = running + leak_run
+        if r < 2:
+            copies[2 * r + 4].start()
+            copies[2 * r + 5].start()
+        place_rows(raw_ref.at[r], toks, r, w)
+        keys, running = gates(raw_ref[r, :, :LANES], gap, tri)
+        leaks = jnp.broadcast_to(leak_row(toks, r, length), (LANES, length))
+        total = running + leaks.T
         last = total[length - 1 :, :]
         fading = (keys * jnp.exp(last - total)).astype(BF16)
-        state = dot(fading, values, ((0,), (0,)))
+        state = dot(fading, raw_ref[r, :, LANES:], ((0,), (0,)))
         spread = jnp.broadcast_to(last, (LANES, LANES)).T
         high = spread.astype(BF16).astype(F32)
         split = jnp.where(lane < LANES // 2, high, spread - high)
@@ -155,40 +160,29 @@
             [state.reshape(LANES // 8, 8, LANES), split.reshape(LANES // 8, 8, LANES)], axis=1
         )
         state_ref[r * 16 : (r + 1) * 16] = packed.astype(BF16)
-        run_ref[r] = running
-        leak_ref[r] = leak_run
-        keys_ref[r] = keys
-        value_ref[r] = values
 
 
 def anywhere(count):
     return [pl.BlockSpec(memory_space=pl.ANY) for _ in range(count)]
 
 
-def token_scratch(tok, columns):
-    rows, wide = tok.shape
+def token_scratch(tok, deep, columns):
     return [
-        pltpu.VMEM((2 * (rows - 8), columns), BF16),
-        pltpu.VMEM((8, rows, wide), BF16),
+        pltpu.VMEM((8, *tok.shape), BF16),
         pltpu.SemaphoreType.DMA((8,)),
+        pltpu.VMEM((deep, columns), BF16),
+        pltpu.SemaphoreType.DMA,
     ]
 
 
 def local_states(toks, w, floor):
     length = 2 * (toks[0].shape[0] - 8)
-    block = (4, length, LANES)
     return pl.pallas_call(
         state_kernel,
-        out_shape=(
-            struct((64, 16, LANES), BF16),
-            struct(block, F32),
-            struct(block, F32),
-            struct(block, F32),
-            struct(block, BF16),
-        ),
-        in_specs=[*anywhere(8), *vmem(2)],
-        out_specs=tuple(vmem(5)),
-        scratch_shapes=token_scratch(toks[0], 2 * LANES),
+        out_shape=(struct((64, 16, LANES), BF16), struct((4, length, 2 * LANES), BF16)),
+        in_specs=[*anywhere(9), *vmem(1)],
+        out_specs=tuple(vmem(2)),
+        scratch_shapes=token_scratch(toks[0], w.shape[0], 2 * LANES),
         name="states",
     )(*toks, w, floor)
 
@@ -217,50 +211,62 @@
         out_shape=struct((states.shape[0], 8, LANES), BF16),
         in_specs=vmem(1),
         out_specs=vmem(1)[0],
+        compiler_params=pltpu.CompilerParams(vmem_limit_bytes=4 << 20),
         name="scan",
     )(states)
 
 
 def inside_kernel(*refs):
     tok_refs, rest = refs[:8], refs[8:]
-    w_ref, run_ref, leak_ref, keys_ref, value_ref, *rest = rest
-    inside_ref, reach_ref, gate_ref, signal_ref, raw, toks, sems = rest
+    w_ref, floor_ref, early_ref, *rest = rest
+    inside_ref, reach_ref, gate_ref, signal_ref, toks, sems, weights, w_sem, raw = rest
+    w_copy = pltpu.make_async_copy(w_ref.at[:, 2 * LANES :], weights, w_sem)
     copies = fetches(tok_refs, toks, sems)
-    for copy in copies:
+    for copy in [w_copy] + copies[:4]:
         copy.start()
-    length = run_ref.shape[1]
+    length = early_ref.shape[1]
     causal = lower_triangle(length)
-    w = w_ref[...]
+    tri = causal.astype(F32).astype(BF16)
+    gap = 1.0 - floor_ref[...]
+    w_copy.wait()
+    w = weights[...]
     for r in range(4):
+        keys, running = gates(early_ref[r, :, :LANES], gap, tri)
         copies[2 * r].wait()
         copies[2 * r + 1].wait()
+        if r < 2:
+            copies[2 * r + 4].start()
+            copies[2 * r + 5].start()
         place_rows(raw, toks, r, w)
         gate_ref[r] = raw[:, LANES : 2 * LANES]
         signal_ref[r] = raw[:, 2 * LANES :]
-        running = run_ref[r]
-        leak_run = leak_ref[r]
         logits = raw[:, :LANES].astype(F32)
         query = logits * jax.nn.sigmoid(logits)
         middle = 0.5 * running[length - 1 :, :]
         ahead = (query * jnp.exp(running - middle)).astype(BF16)
-        behind = (keys_ref[r] * jnp.exp(middle - running)).astype(BF16)
-        fade = jnp.exp(jnp.where(causal, leak_run[:, :1] - leak_run.T[:1, :], -jnp.inf))
+        behind = (keys * jnp.exp(middle - running)).astype(BF16)
+        leaks = leak_row(toks, r, length)
+        columns = jnp.broadcast_to(leaks, (LANES, length)).T
+        fade = jnp.exp(jnp.where(causal, columns[:, :1] - leaks, -jnp.inf))
         scores = dot(ahead, behind, ((1,), (1,))) * fade
-        inside_ref[r] = dot(scores.astype(BF16), value_ref[r])
-        reach_ref[r] = (query * jnp.exp(running + leak_run)).astype(BF16)
-
-
-def inside_blocks(toks, w, running, leak_run, keys, values):
-    length = running.shape[1]
+        inside_ref[r] = dot(scores.astype(BF16), early_ref[r, :, LANES:])
+        reach_ref[r] = (query * jnp.exp(running + columns)).astype(BF16)
+
+
+def inside_blocks(toks, w, floor, early):
+    length = early.shape[1]
     block = (4, length, LANES)
     return pl.pallas_call(
         inside_kernel,
         out_shape=(struct(block, F32), struct(block, BF16), struct(block, BF16), struct(block, BF16)),
-        in_specs=[*anywhere(8), *vmem(5)],
+        in_specs=[*anywhere(9), *vmem(2)],
         out_specs=tuple(vmem(4)),
-        scratch_shapes=token_scratch(toks[0], 3 * LANES),
+        scratch_shapes=[
+            *token_scratch(toks[0], w.shape[0], 3 * LANES),
+            pltpu.VMEM((length, 3 * LANES), BF16),
+        ],
         name="inside",
-    )(*toks, w, running, leak_run, keys, values)
+    )(*toks, w, floor, early)
 
 
 def mix_kernel(
@@ -364,9 +370,8 @@
     x = lax.axis_index("fs")
     slabs = weight_slabs((forget_w, value_w, query_w, conv_gate_w, conv_in_w), 8)
     y_rows = exchanged(slabs, "sp_1").reshape(-1, slabs.shape[2])
-    early, late = split_columns(y_rows, 8)
-    late_w = lax.all_gather(late, "sp_0", axis=0, tiled=True)
-    early_w = exchanged(early, "sp_0").reshape(-1, early.shape[2])
+    y_rows = relayed(y_rows)
+    weights = lax.all_gather(y_rows, "sp_0", axis=0, tiled=True)
 
     own = norm_rows(tokens[0], norm_gain, leak[0].T)
     near = [own]
@@ -378,17 +383,17 @@
     toks = [part for pair in zip(near, far) for part in pair]
 
     out_w = jnp.concatenate([conv_out_w, chain_out_w], axis=0)
-    out_w, late = lax.optimization_barrier((out_w, late))
+    out_w, y_rows = lax.optimization_barrier((out_w, y_rows))
     out_near = lax.all_gather(out_w, "fs", axis=0)
     out_far = ring(out_near, "tp", 1)
 
     floor = lax.dynamic_slice_in_dim(floor_gate, x * LANES, LANES, 0)[None]
-    states, running, leak_run, keys, values = local_states(toks, early_w, floor)
+    states, early = local_states(toks, weights, floor)
     arrived = exchanged(states, SP)
     before = exchanged(scan_blocks(arrived), SP)
     before = before.reshape(4, LANES, LANES)
 
-    inside, reach, gate, signal = inside_blocks(toks, late_w, running, leak_run, keys, values)
+    inside, reach, gate, signal = inside_blocks(toks, weights, floor, early)
     count = 64
     tail = signal[:, -16:, :]
     rim = lax.ppermute(tail, SP, [(i, i + 1) for i in range(count - 1)])

time: 248 us -> 234 us (0.944)
  starting transfers between devices: 62.2 us -> 37.5 us
  waiting for transfers between devices: 77.8 us -> 95.3 us
  Pallas kernels: 39.2 us -> 35.5 us
    ppermute x8, waiting for transfers between devices: 12.8 us -> 30.3 us  [ring(): lax.ppermute(array, axis, [(i, (i + by) % count) for i in range(count)])]
    ppermute x8, starting transfers between devices: 39.1 us -> 21.6 us  [ring(): lax.ppermute(array, axis, [(i, (i + by) % count) for i in range(count)])]
    all_to_all x3 -> x2, starting transfers between devices: 20.3 us -> 13.1 us  [exchanged(): return lax.all_to_all(array, axis, split_axis=0, concat_axis=0, tiled=True)]
    all_to_all x3 -> x2, waiting for transfers between devices: 7.79 us -> 7.8 us  [exchanged(): return lax.all_to_all(array, axis, split_axis=0, concat_axis=0, tiled=True)]
  transfers between devices with their start and end apart: 14 -> 13, of which waited for: 5 -> 5; matrix products, arithmetic and copies ran while one was open for 2% -> 2% of each run, Pallas kernels for 12% -> 12%
where the time goes in v3:
time: 234 us; the launch traced here: 232 us
  waiting for transfers between devices  95.3 us (41%)
  blocking collectives  45.5 us (19%)
  starting transfers between devices  37.5 us (16%)
  Pallas kernels  35.5 us (15%)
  between operations  13.6 us (6%)
    all_gather x1, waiting for transfers between devices, layer(): out_near = lax.all_gather(out_w, 'fs', axis=0)  55.6 us
    all_to_all x2, blocking collectives, exchanged(): return lax.all_to_all(array, axis, split_axis=0, concat_axis=0, tiled=True)  45.5 us
    ppermute x8, waiting for transfers between devices, ring(): lax.ppermute(array, axis, [(i, (i + by) % count) for i in range(count)])  30.3 us
    ppermute x8, starting transfers between devices, ring(): lax.ppermute(array, axis, [(i, (i + by) % count) for i in range(count)])  21.6 us
    all_to_all x2, starting transfers between devices, exchanged(): return lax.all_to_all(array, axis, split_axis=0, concat_axis=0, tiled=True)  13.1 us
    pallas_call x1, Pallas kernels, inside_blocks(): pl.pallas_call(inside_kernel, out_shape=(struct(block, F32), struct(block...  11 us
    pallas_call x1, Pallas kernels, local_states(): pl.pallas_call(state_kernel, out_shape=(struct((64, 16, LANES), BF16), st...  8.47 us
    all_to_all x2, waiting for transfers between devices, exchanged(): return lax.all_to_all(array, axis, split_axis=0, concat_axis=0, tiled=True)  7.8 us
  transfers between devices with their start and end apart: 13, of which 5 were waited for; matrix products, arithmetic and copies ran while one was open for 2% of the time, Pallas kernels for 12%

profile of v3, /device:TPU:1, one launch (start us, length us, event | category | flops | bytes accessed | tf_op | source)
XLA Modules:
  0.0 231.7 jit_solution(17946265472251800024)
XLA Ops:
  6.5 1.6 slab.1
  8.1 7.6 %all-to-all-start = ((bf16[8,32,640]{2,1,0:T(8,128)(2,1)}), bf16[8,32,640]{2,1,0:T(8,128)(2,1)S(1)}, u32[]{:S(2)}, u32[]{:S(2)}) async-start(bf16[8,32,640]{2,1,0:T(8,128)(2,1)} %slab.1), calls=%async_computation | async-start | bytes 655360 | tf_op jit(solution)/shard_map/all_to_all | solution.py:352
  15.8 2.3 pad_maximum_fusion
  18.1 7.8 %all-to-all-done = bf16[8,32,640]{2,1,0:T(8,128)(2,1)S(1)} async-done(((bf16[8,32,640]{2,1,0:T(8,128)(2,1)}), bf16[8,32,640]{2,1,0:T(8,128)(2,1)S(1)}, u32[]{:S(2)}, u32[]{:S(2)}) %all-to-all-start) | async-done | bytes 327712 | tf_op jit(solution)/shard_map/all_to_all | solution.py:352
  27.4 55.6 %all-gather.6.cloned.1.call-done = bf16[4096,512]{1,0:T(8,128)(2,1)} async-done(((bf16[1024,512]{1,0:T(8,128)(2,1)}), bf16[4096,512]{1,0:T(8,128)(2,1)}) %all-gather.6.cloned.1.call-update) | async-done | bytes 4194320 | tf_op jit(solution)/shard_map/all_gather | solution.py:387
  83.0 2.7 %collective-permute-start.8 = (bf16[4,1024,512]{2,1,0:T(8,128)(2,1)}, bf16[4,1024,512]{2,1,0:T(8,128)(2,1)}, u32[]{:S(2)}, u32[]{:S(2)}) collective-permute-start(bf16[4,1024,512]{2,1,0:T(8,128)(2,1)} %bitcast.13), channel_id=1, source_target_pairs={{0,1},{1,0},{2,3},{3,2},{4,5},{5,4},{6,7},{7,6},{8,9},{9,8},{10,11... | collective-permute-start | bytes 12582920 | tf_op jit(solution)/shard_map/ppermute | solution.py:348
  85.8 2.6 %norm.1.refs_0_ = bf16[200,2048]{1,0:T(8,128)(2,1)} custom-call(bf16[192,2048]{1,0:T(8,128)(2,1)} %bitcast.15, f32[1,2048]{1,0:T(1,128)} %bitcast.17, f32[4,384]{1,0:T(4,128)} %bitcast.18), custom_call_target="tpu_custom_call" | custom-call | tf_op jit(solution)/shard_map/norm/pallas_call | solution.py:57
  88.4 2.5 %collective-permute-start.1 = (bf16[200,2048]{1,0:T(8,128)(2,1)}, bf16[200,2048]{1,0:T(8,128)(2,1)S(1)}, u32[]{:S(2)}, u32[]{:S(2)}) collective-permute-start(bf16[200,2048]{1,0:T(8,128)(2,1)} %norm.1.refs_0_), channel_id=1, source_target_pairs={{0,2},{2,4},{4,6},{6,0},{1,3},{3,5},{5,7},{7,1},{8,10},{10,12},{12... | collective-permute-start | bytes 2457608 | tf_op jit(solution)/shard_map/ppermute | solution.py:348
  90.8 4.0 %collective-permute-start.3 = (bf16[200,2048]{1,0:T(8,128)(2,1)}, bf16[200,2048]{1,0:T(8,128)(2,1)S(1)}, u32[]{:S(2)}, u32[]{:S(2)}) collective-permute-start(bf16[200,2048]{1,0:T(8,128)(2,1)} %norm.1.refs_0_), channel_id=1, source_target_pairs={{0,6},{2,0},{4,2},{6,4},{1,7},{3,1},{5,3},{7,5},{8,14},{10,8},{12,... | collective-permute-start | bytes 2457608 | tf_op jit(solution)/shard_map/ppermute | solution.py:348
  94.9 2.5 %collective-permute-start.5 = (bf16[200,2048]{1,0:T(8,128)(2,1)}, bf16[200,2048]{1,0:T(8,128)(2,1)S(1)}, u32[]{:S(2)}, u32[]{:S(2)}) collective-permute-start(bf16[200,2048]{1,0:T(8,128)(2,1)} %norm.1.refs_0_), channel_id=1, source_target_pairs={{0,4},{2,6},{4,0},{6,2},{1,5},{3,7},{5,1},{7,3},{8,12},{10,14},{12... | collective-permute-start | bytes 2457608 | tf_op jit(solution)/shard_map/ppermute | solution.py:348
  97.3 2.8 %collective-permute-start = (bf16[200,2048]{1,0:T(8,128)(2,1)}, bf16[200,2048]{1,0:T(8,128)(2,1)S(1)}, u32[]{:S(2)}, u32[]{:S(2)}) collective-permute-start(bf16[200,2048]{1,0:T(8,128)(2,1)} %norm.1.refs_0_), channel_id=1, source_target_pairs={{0,1},{1,0},{2,3},{3,2},{4,5},{5,4},{6,7},{7,6},{8,9},{9,8},{10,11... | collective-permute-start | bytes 2457608 | tf_op jit(solution)/shard_map/ppermute | solution.py:348
  100.1 28.9 %collective-permute-done.1.refs_2_ = bf16[200,2048]{1,0:T(8,128)(2,1)S(1)} collective-permute-done((bf16[200,2048]{1,0:T(8,128)(2,1)}, bf16[200,2048]{1,0:T(8,128)(2,1)S(1)}, u32[]{:S(2)}, u32[]{:S(2)}) %collective-permute-start.1) | collective-permute-done | bytes 819232 | tf_op jit(solution)/shard_map/ppermute | solution.py:348
  129.0 2.8 %collective-permute-start.2 = (bf16[200,2048]{1,0:T(8,128)(2,1)S(1)}, bf16[200,2048]{1,0:T(8,128)(2,1)}, u32[]{:S(2)}, u32[]{:S(2)}) collective-permute-start(bf16[200,2048]{1,0:T(8,128)(2,1)S(1)} %collective-permute-done.1.refs_2_), channel_id=1, source_target_pairs={{0,1},{1,0},{2,3},{3,2},{4,5},{5,4},{6,7},{7,6},{8,9},{9,8},{10,11... | collective-permute-start | bytes 2457608 | tf_op jit(solution)/shard_map/ppermute | solution.py:348
  131.8 1.9 collective-permute-start.4
  133.8 2.4 %collective-permute-start.6 = (bf16[200,2048]{1,0:T(8,128)(2,1)S(1)}, bf16[200,2048]{1,0:T(8,128)(2,1)}, u32[]{:S(2)}, u32[]{:S(2)}) collective-permute-start(bf16[200,2048]{1,0:T(8,128)(2,1)S(1)} %collective-permute-done.5.refs_6_), channel_id=1, source_target_pairs={{0,1},{1,0},{2,3},{3,2},{4,5},{5,4},{6,7},{7,6},{8,9},{9,8},{10,11... | collective-permute-start | bytes 2457608 | tf_op jit(solution)/shard_map/ppermute | solution.py:348
  136.8 1.4 collective-permute-done.6.refs_7_
  138.3 8.5 %states.1 = (bf16[64,16,128]{2,1,0:T(8,128)(2,1)}, bf16[4,384,256]{2,1,0:T(8,128)(2,1)}) custom-call(bf16[200,2048]{1,0:T(8,128)(2,1)} %norm.1.refs_0_, bf16[200,2048]{1,0:T(8,128)(2,1)} %copy-done.4, bf16[200,2048]{1,0:T(8,128)(2,1)} %copy-done.1, bf16[200,2048]{1,0:T(8,128)(2,1)} %collective-permute-done.2.refs_3_, bf16[200,2048]{1,0:T(8,128)(2,1)} %copy-done.2, ...), custom_call_target="tpu_custom_call" | custom-call | tf_op jit(solution)/shard_map/states/pallas_call | solution.py:180
  146.7 26.2 %all_to_all.20.in_ref = bf16[64,16,128]{2,1,0:T(8,128)(2,1)S(1)} all-to-all(bf16[64,16,128]{2,1,0:T(8,128)(2,1)} %get-tuple-element.15), channel_id=1, replica_groups=mesh['sp_0'=8,'sp_1'=8,'fs'=4,'tp'=2] {'sp_0','sp_1'}, dimensions={0} | all-to-all | bytes 524288 | tf_op jit(solution)/shard_map/all_to_all | solution.py:352
  173.8 5.5 %all-to-all-start.2 = ((bf16[64,8,128]{2,1,0:T(8,128)(2,1)}), bf16[64,8,128]{2,1,0:T(8,128)(2,1)S(1)}, u32[]{:S(2)}, u32[]{:S(2)}) async-start(bf16[64,8,128]{2,1,0:T(8,128)(2,1)} %scan.1), calls=%async_computation.2 | async-start | bytes 262144 | tf_op jit(solution)/shard_map/all_to_all | solution.py:352
  179.3 11.0 %inside.1 = (f32[4,384,128]{2,1,0:T(8,128)}, bf16[4,384,128]{2,1,0:T(8,128)(2,1)}, bf16[4,384,128]{2,1,0:T(8,128)(2,1)}, bf16[4,384,128]{2,1,0:T(8,128)(2,1)}) custom-call(bf16[200,2048]{1,0:T(8,128)(2,1)} %norm.1.refs_0_, bf16[200,2048]{1,0:T(8,128)(2,1)} %copy-done.4, bf16[200,2048]{1,0:T(8,128)(2,1)} %copy-done.1, ...), custom_call_target="tpu_custom_call" | custom-call | tf_op jit(solution)/shard_map/inside/pallas_call | solution.py:259
  191.1 2.7 %collective-permute-start.7 = (bf16[4,16,128]{2,1,0:T(8,128)(2,1)S(1)}, bf16[4,16,128]{2,1,0:T(8,128)(2,1)S(1)}, u32[]{:S(2)}, u32[]{:S(2)}) collective-permute-start(bf16[4,16,128]{2,1,0:T(8,128)(2,1)S(1)} %slice.3), channel_id=1, source_target_pairs={{0,8},{8,16},{16,24},{24,32},{32,40},{40,48},{48,56},{56,64},{64,7... | collective-permute-start | bytes 49160 | tf_op jit(solution)/shard_map/ppermute | solution.py:399
  195.3 4.1 %mix.1 = bf16[8,192,256]{2,1,0:T(8,128)(2,1)} custom-call(f32[4,384,128]{2,1,0:T(8,128)} %get-tuple-element.13.inside_ref, bf16[4,384,128]{2,1,0:T(8,128)(2,1)} %get-tuple-element.14.reach_ref, bf16[4,128,128]{2,1,0:T(8,128)(2,1)} %bitcast.16, bf16[4,384,128]{2,1,0:T(8,128)(2,1)} %get-tuple-element.16.gate_ref, ...), custom_call_target="tpu_custom_call" | custom-call | tf_op jit(solution)/shard_map/mix/pallas_call | solution.py:301
  199.4 19.3 %all_to_all.21.mix_ref = bf16[8,192,256]{2,1,0:T(8,128)(2,1)} all-to-all(bf16[8,192,256]{2,1,0:T(8,128)(2,1)} %mix.1), channel_id=1, replica_groups=mesh['sp_0'=8,'sp_1'=8,'fs'=4,'tp'=2] {'fs','tp'}, dimensions={0} | all-to-all | bytes 1572864 | tf_op jit(solution)/shard_map/all_to_all | solution.py:352
  218.8 6.1 %out.1 = bf16[192,2048]{1,0:T(8,128)(2,1)} custom-call(bf16[8,192,256]{2,1,0:T(8,128)(2,1)} %all_to_all.21.mix_ref, bf16[4,1024,512]{2,1,0:T(8,128)(2,1)} %bitcast.14, bf16[4,1024,512]{2,1,0:T(8,128)(2,1)} %collective-permute-done.8.far_ref), custom_call_target="tpu_custom_call" | custom-call | tf_op jit(solution)/shard_map/out/pallas_call | solution.py:336
  (31 shorter events, 5.3 us)
Async XLA Ops:
  6.5 129.6 %copy-start = (f32[512]{0:T(512)S(1)}, f32[512]{0:T(512)}, u32[]{:S(2)}) copy-start(f32[512]{0:T(512)} %param.21) | copy-start | bytes 6148
  8.1 17.8 %all-to-all-start = ((bf16[8,32,640]{2,1,0:T(8,128)(2,1)}), bf16[8,32,640]{2,1,0:T(8,128)(2,1)S(1)}, u32[]{:S(2)}, u32[]{:S(2)}) async-start(bf16[8,32,640]{2,1,0:T(8,128)(2,1)} %slab.1), calls=%async_computation | async-start | bytes 655360 | tf_op jit(solution)/shard_map/all_to_all | solution.py:352
  15.8 67.2 %all-gather.6.cloned.1.call-start = ((), (), s32[]{:S(2)}) async-start(), calls=%async_computation.5 | async-start | bytes 5242880 | tf_op jit(solution)/shard_map/all_gather | solution.py:387
  26.7 111.6 %all-gather.4.cloned.1.call-start = ((), (), s32[]{:S(2)}) async-start(), calls=%async_computation.4 | async-start | bytes 2949120 | tf_op jit(solution)/shard_map/all_gather | solution.py:374
  83.0 135.8 %collective-permute-start.8 = (bf16[4,1024,512]{2,1,0:T(8,128)(2,1)}, bf16[4,1024,512]{2,1,0:T(8,128)(2,1)}, u32[]{:S(2)}, u32[]{:S(2)}) collective-permute-start(bf16[4,1024,512]{2,1,0:T(8,128)(2,1)} %bitcast.13), channel_id=1, source_target_pairs={{0,1},{1,0},{2,3},{3,2},{4,5},{5,4},{6,7},{7,6},{8,9},{9,8},{10,11... | collective-permute-start | bytes 12582920 | tf_op jit(solution)/shard_map/ppermute | solution.py:348
  88.4 40.6 %collective-permute-start.1 = (bf16[200,2048]{1,0:T(8,128)(2,1)}, bf16[200,2048]{1,0:T(8,128)(2,1)S(1)}, u32[]{:S(2)}, u32[]{:S(2)}) collective-permute-start(bf16[200,2048]{1,0:T(8,128)(2,1)} %norm.1.refs_0_), channel_id=1, source_target_pairs={{0,2},{2,4},{4,6},{6,0},{1,3},{3,5},{5,7},{7,1},{8,10},{10,12},{12... | collective-permute-start | bytes 2457608 | tf_op jit(solution)/shard_map/ppermute | solution.py:348
  90.8 41.0 %collective-permute-start.3 = (bf16[200,2048]{1,0:T(8,128)(2,1)}, bf16[200,2048]{1,0:T(8,128)(2,1)S(1)}, u32[]{:S(2)}, u32[]{:S(2)}) collective-permute-start(bf16[200,2048]{1,0:T(8,128)(2,1)} %norm.1.refs_0_), channel_id=1, source_target_pairs={{0,6},{2,0},{4,2},{6,4},{1,7},{3,1},{5,3},{7,5},{8,14},{10,8},{12,... | collective-permute-start | bytes 2457608 | tf_op jit(solution)/shard_map/ppermute | solution.py:348
  94.9 38.9 %collective-permute-start.5 = (bf16[200,2048]{1,0:T(8,128)(2,1)}, bf16[200,2048]{1,0:T(8,128)(2,1)S(1)}, u32[]{:S(2)}, u32[]{:S(2)}) collective-permute-start(bf16[200,2048]{1,0:T(8,128)(2,1)} %norm.1.refs_0_), channel_id=1, source_target_pairs={{0,4},{2,6},{4,0},{6,2},{1,5},{3,7},{5,1},{7,3},{8,12},{10,14},{12... | collective-permute-start | bytes 2457608 | tf_op jit(solution)/shard_map/ppermute | solution.py:348
  97.3 39.5 %collective-permute-start = (bf16[200,2048]{1,0:T(8,128)(2,1)}, bf16[200,2048]{1,0:T(8,128)(2,1)S(1)}, u32[]{:S(2)}, u32[]{:S(2)}) collective-permute-start(bf16[200,2048]{1,0:T(8,128)(2,1)} %norm.1.refs_0_), channel_id=1, source_target_pairs={{0,1},{1,0},{2,3},{3,2},{4,5},{5,4},{6,7},{7,6},{8,9},{9,8},{10,11... | collective-permute-start | bytes 2457608 | tf_op jit(solution)/shard_map/ppermute | solution.py:348
  129.0 9.2 %copy-start.1 = (bf16[200,2048]{1,0:T(8,128)(2,1)}, bf16[200,2048]{1,0:T(8,128)(2,1)S(1)}, u32[]{:S(2)}) copy-start(bf16[200,2048]{1,0:T(8,128)(2,1)S(1)} %collective-permute-done.1.refs_2_) | copy-start | bytes 2457604
  129.0 7.8 %collective-permute-start.2 = (bf16[200,2048]{1,0:T(8,128)(2,1)S(1)}, bf16[200,2048]{1,0:T(8,128)(2,1)}, u32[]{:S(2)}, u32[]{:S(2)}) collective-permute-start(bf16[200,2048]{1,0:T(8,128)(2,1)S(1)} %collective-permute-done.1.refs_2_), channel_id=1, source_target_pairs={{0,1},{1,0},{2,3},{3,2},{4,5},{5,4},{6,7},{7,6},{8,9},{9,8},{10,11... | collective-permute-start | bytes 2457608 | tf_op jit(solution)/shard_map/ppermute | solution.py:348
  131.8 6.5 %copy-start.2 = (bf16[200,2048]{1,0:T(8,128)(2,1)}, bf16[200,2048]{1,0:T(8,128)(2,1)S(1)}, u32[]{:S(2)}) copy-start(bf16[200,2048]{1,0:T(8,128)(2,1)S(1)} %collective-permute-done.3.refs_4_) | copy-start | bytes 2457604
  131.8 5.0 %collective-permute-start.4 = (bf16[200,2048]{1,0:T(8,128)(2,1)S(1)}, bf16[200,2048]{1,0:T(8,128)(2,1)}, u32[]{:S(2)}, u32[]{:S(2)}) collective-permute-start(bf16[200,2048]{1,0:T(8,128)(2,1)S(1)} %collective-permute-done.3.refs_4_), channel_id=1, source_target_pairs={{0,1},{1,0},{2,3},{3,2},{4,5},{5,4},{6,7},{7,6},{8,9},{9,8},{10,11... | collective-permute-start | bytes 2457608 | tf_op jit(solution)/shard_map/ppermute | solution.py:348
  133.7 4.5 %copy-start.3 = (bf16[200,2048]{1,0:T(8,128)(2,1)}, bf16[200,2048]{1,0:T(8,128)(2,1)S(1)}, u32[]{:S(2)}) copy-start(bf16[200,2048]{1,0:T(8,128)(2,1)S(1)} %collective-permute-done.5.refs_6_) | copy-start | bytes 2457604
  133.8 4.5 %collective-permute-start.6 = (bf16[200,2048]{1,0:T(8,128)(2,1)S(1)}, bf16[200,2048]{1,0:T(8,128)(2,1)}, u32[]{:S(2)}, u32[]{:S(2)}) collective-permute-start(bf16[200,2048]{1,0:T(8,128)(2,1)S(1)} %collective-permute-done.5.refs_6_), channel_id=1, source_target_pairs={{0,1},{1,0},{2,3},{3,2},{4,5},{5,4},{6,7},{7,6},{8,9},{9,8},{10,11... | collective-permute-start | bytes 2457608 | tf_op jit(solution)/shard_map/ppermute | solution.py:348
  136.8 1.5 copy-start.4
  173.8 20.9 %all-to-all-start.2 = ((bf16[64,8,128]{2,1,0:T(8,128)(2,1)}), bf16[64,8,128]{2,1,0:T(8,128)(2,1)S(1)}, u32[]{:S(2)}, u32[]{:S(2)}) async-start(bf16[64,8,128]{2,1,0:T(8,128)(2,1)} %scan.1), calls=%async_computation.2 | async-start | bytes 262144 | tf_op jit(solution)/shard_map/all_to_all | solution.py:352
  191.1 3.6 %collective-permute-start.7 = (bf16[4,16,128]{2,1,0:T(8,128)(2,1)S(1)}, bf16[4,16,128]{2,1,0:T(8,128)(2,1)S(1)}, u32[]{:S(2)}, u32[]{:S(2)}) collective-permute-start(bf16[4,16,128]{2,1,0:T(8,128)(2,1)S(1)} %slice.3), channel_id=1, source_target_pairs={{0,8},{8,16},{16,24},{24,32},{32,40},{40,48},{48,56},{56,64},{64,7... | collective-permute-start | bytes 49160 | tf_op jit(solution)/shard_map/ppermute | solution.py:399
  194.7 0.6 copy-start.6
  194.7 0.7 copy-start.5
Sparse Core Ops, SparseCore 0:
  26.8 56.1 all-gather.5
  85.1 42.8 all-gather.3

commit v4 on v3

--- a/solution.py
+++ b/solution.py
@@ -97,12 +97,15 @@
     )(rows)
 
 
-def place_rows(scratch, toks, r, w):
+def place_rows(out, toks, r, w):
     core = lax.axis_index("tp")
-    half = scratch.shape[0] // 2
-    for part, place in ((2 * r, core), (2 * r + 1, 1 - core)):
-        start = pl.multiple_of(place * half, half)
-        scratch[pl.ds(start, half), :] = dot(toks[part, :half, :], w).astype(BF16)
+    half = out.shape[0] // 2
+    both = jnp.concatenate([toks[2 * r, :half, :], toks[2 * r + 1, :half, :]], axis=0)
+    result = dot(both, w).astype(BF16)
+    first = pl.multiple_of(core * half, half)
+    second = pl.multiple_of((1 - core) * half, half)
+    out[pl.ds(first, half), :] = result[:half]
+    out[pl.ds(second, half), :] = result[half:]
 
 
 def fetches(refs, toks, sems):
@@ -318,27 +321,38 @@
     )(inside, reach, state, gate, signal, rim, taps, gain)
 
 
-def out_kernel(mix_ref, near_ref, far_ref, o_ref):
+def out_kernel(mix_ref, near_ref, far_ref, o_ref, near, sems):
+    copies = [pltpu.make_async_copy(near_ref.at[x], near.at[x], sems.at[x]) for x in range(4)]
+    for copy in copies:
+        copy.start()
     core = lax.axis_index("tp")
-    total = jnp.zeros(o_ref.shape, F32)
-    for c, w_ref in ((core, near_ref), (1 - core, far_ref)):
+    rows = []
+    for c in (core, 1 - core):
         pieces = [mix_ref[2 * x + c] for x in range(4)]
-        lhs = jnp.concatenate(
-            [piece[:, :LANES] for piece in pieces] + [piece[:, LANES:] for piece in pieces], axis=1
+        rows.append(
+            jnp.concatenate(
+                [piece[:, :LANES] for piece in pieces] + [piece[:, LANES:] for piece in pieces],
+                axis=1,
+            )
         )
-        total = total + dot(lhs, w_ref[0])
-    o_ref[...] = total.astype(BF16)
+    wide = near_ref.shape[2]
+    for x in range(4):
+        total = dot(rows[1], far_ref[x])
+        copies[x].wait()
+        total = total + dot(rows[0], near[x])
+        o_ref[:, x * wide : (x + 1) * wide] = total.astype(BF16)
 
 
 def out_rows(mix, near, far):
     rows = mix.shape[1]
-    pieces, deep, wide = near.shape
+    pieces, _, wide = near.shape
     return pl.pallas_call(
         out_kernel,
         out_shape=struct((rows, pieces * wide), BF16),
-        grid=(pieces,),
-        in_specs=[whole(*mix.shape), sequence_block(deep, wide), sequence_block(deep, wide)],
-        out_specs=pl.BlockSpec((rows, wide), lambda j: (0, j)),
+        in_specs=[*vmem(1), *anywhere(1), *vmem(1)],
+        out_specs=vmem(1)[0],
+        scratch_shapes=[pltpu.VMEM(near.shape, BF16), pltpu.SemaphoreType.DMA((4,))],
+        compiler_params=pltpu.CompilerParams(vmem_limit_bytes=20 << 20),
         name="out",
     )(mix, near, far)
 

time: 234 us -> 238 us (1.017)
  no operation moved by 1% of the time
where the time goes in v4:
time: 238 us; the launch traced here: 235 us
  waiting for transfers between devices  95.2 us (40%)
  blocking collectives  45.4 us (19%)
  starting transfers between devices  37.5 us (16%)
  Pallas kernels  37.2 us (16%)
  between operations  13.6 us (6%)
  local copies, waits for them, and re-layouts  4.26 us (2%)
    all_gather x1, waiting for transfers between devices, layer(): out_near = lax.all_gather(out_w, 'fs', axis=0)  55.6 us
    all_to_all x2, blocking collectives, exchanged(): return lax.all_to_all(array, axis, split_axis=0, concat_axis=0, tiled=True)  45.4 us
    ppermute x8, waiting for transfers between devices, ring(): lax.ppermute(array, axis, [(i, (i + by) % count) for i in range(count)])  30.3 us
    ppermute x8, starting transfers between devices, ring(): lax.ppermute(array, axis, [(i, (i + by) % count) for i in range(count)])  21.6 us
    all_to_all x2, starting transfers between devices, exchanged(): return lax.all_to_all(array, axis, split_axis=0, concat_axis=0, tiled=True)  13.1 us
    pallas_call x1, Pallas kernels, inside_blocks(): pl.pallas_call(inside_kernel, out_shape=(struct(block, F32), struct(block...  11.3 us
    pallas_call x1, Pallas kernels, local_states(): pl.pallas_call(state_kernel, out_shape=(struct((64, 16, LANES), BF16), st...  9.94 us
    all_to_all x2, waiting for transfers between devices, exchanged(): return lax.all_to_all(array, axis, split_axis=0, concat_axis=0, tiled=True)  7.79 us
  transfers between devices with their start and end apart: 13, of which 5 were waited for; matrix products, arithmetic and copies ran while one was open for 2% of the time, Pallas kernels for 12%

profile of v4, /device:TPU:1, one launch (start us, length us, event | category | flops | bytes accessed | tf_op | source)
XLA Modules:
  0.0 235.5 jit_solution(11096482963597601404)
XLA Ops:
  6.5 1.6 slab.1
  8.1 7.6 %all-to-all-start = ((bf16[8,32,640]{2,1,0:T(8,128)(2,1)}), bf16[8,32,640]{2,1,0:T(8,128)(2,1)S(1)}, u32[]{:S(2)}, u32[]{:S(2)}) async-start(bf16[8,32,640]{2,1,0:T(8,128)(2,1)} %slab.1), calls=%async_computation | async-start | bytes 655360 | tf_op jit(solution)/shard_map/all_to_all | solution.py:366
  15.8 2.3 pad_maximum_fusion
  18.1 7.8 %all-to-all-done = bf16[8,32,640]{2,1,0:T(8,128)(2,1)S(1)} async-done(((bf16[8,32,640]{2,1,0:T(8,128)(2,1)}), bf16[8,32,640]{2,1,0:T(8,128)(2,1)S(1)}, u32[]{:S(2)}, u32[]{:S(2)}) %all-to-all-start) | async-done | bytes 327712 | tf_op jit(solution)/shard_map/all_to_all | solution.py:366
  27.4 55.6 %all-gather.6.cloned.1.call-done = bf16[4096,512]{1,0:T(8,128)(2,1)} async-done(((bf16[1024,512]{1,0:T(8,128)(2,1)}), bf16[4096,512]{1,0:T(8,128)(2,1)}) %all-gather.6.cloned.1.call-update) | async-done | bytes 4194320 | tf_op jit(solution)/shard_map/all_gather | solution.py:401
  83.0 2.7 %collective-permute-start.8 = (bf16[4,1024,512]{2,1,0:T(8,128)(2,1)}, bf16[4,1024,512]{2,1,0:T(8,128)(2,1)}, u32[]{:S(2)}, u32[]{:S(2)}) collective-permute-start(bf16[4,1024,512]{2,1,0:T(8,128)(2,1)} %bitcast.12), channel_id=1, source_target_pairs={{0,1},{1,0},{2,3},{3,2},{4,5},{5,4},{6,7},{7,6},{8,9},{9,8},{10,11... | collective-permute-start | bytes 12582920 | tf_op jit(solution)/shard_map/ppermute | solution.py:362
  85.8 2.6 %norm.1.refs_0_ = bf16[200,2048]{1,0:T(8,128)(2,1)} custom-call(bf16[192,2048]{1,0:T(8,128)(2,1)} %bitcast.15, f32[1,2048]{1,0:T(1,128)} %bitcast.17, f32[4,384]{1,0:T(4,128)} %bitcast.18), custom_call_target="tpu_custom_call" | custom-call | tf_op jit(solution)/shard_map/norm/pallas_call | solution.py:57
  88.4 2.5 %collective-permute-start.1 = (bf16[200,2048]{1,0:T(8,128)(2,1)}, bf16[200,2048]{1,0:T(8,128)(2,1)S(1)}, u32[]{:S(2)}, u32[]{:S(2)}) collective-permute-start(bf16[200,2048]{1,0:T(8,128)(2,1)} %norm.1.refs_0_), channel_id=1, source_target_pairs={{0,2},{2,4},{4,6},{6,0},{1,3},{3,5},{5,7},{7,1},{8,10},{10,12},{12... | collective-permute-start | bytes 2457608 | tf_op jit(solution)/shard_map/ppermute | solution.py:362
  90.8 4.0 %collective-permute-start.3 = (bf16[200,2048]{1,0:T(8,128)(2,1)}, bf16[200,2048]{1,0:T(8,128)(2,1)S(1)}, u32[]{:S(2)}, u32[]{:S(2)}) collective-permute-start(bf16[200,2048]{1,0:T(8,128)(2,1)} %norm.1.refs_0_), channel_id=1, source_target_pairs={{0,6},{2,0},{4,2},{6,4},{1,7},{3,1},{5,3},{7,5},{8,14},{10,8},{12,... | collective-permute-start | bytes 2457608 | tf_op jit(solution)/shard_map/ppermute | solution.py:362
  94.9 2.5 %collective-permute-start.5 = (bf16[200,2048]{1,0:T(8,128)(2,1)}, bf16[200,2048]{1,0:T(8,128)(2,1)S(1)}, u32[]{:S(2)}, u32[]{:S(2)}) collective-permute-start(bf16[200,2048]{1,0:T(8,128)(2,1)} %norm.1.refs_0_), channel_id=1, source_target_pairs={{0,4},{2,6},{4,0},{6,2},{1,5},{3,7},{5,1},{7,3},{8,12},{10,14},{12... | collective-permute-start | bytes 2457608 | tf_op jit(solution)/shard_map/ppermute | solution.py:362
  97.3 2.8 %collective-permute-start = (bf16[200,2048]{1,0:T(8,128)(2,1)}, bf16[200,2048]{1,0:T(8,128)(2,1)S(1)}, u32[]{:S(2)}, u32[]{:S(2)}) collective-permute-start(bf16[200,2048]{1,0:T(8,128)(2,1)} %norm.1.refs_0_), channel_id=1, source_target_pairs={{0,1},{1,0},{2,3},{3,2},{4,5},{5,4},{6,7},{7,6},{8,9},{9,8},{10,11... | collective-permute-start | bytes 2457608 | tf_op jit(solution)/shard_map/ppermute | solution.py:362
  100.1 28.9 %collective-permute-done.1.refs_2_ = bf16[200,2048]{1,0:T(8,128)(2,1)S(1)} collective-permute-done((bf16[200,2048]{1,0:T(8,128)(2,1)}, bf16[200,2048]{1,0:T(8,128)(2,1)S(1)}, u32[]{:S(2)}, u32[]{:S(2)}) %collective-permute-start.1) | collective-permute-done | bytes 819232 | tf_op jit(solution)/shard_map/ppermute | solution.py:362
  129.0 2.8 %collective-permute-start.2 = (bf16[200,2048]{1,0:T(8,128)(2,1)S(1)}, bf16[200,2048]{1,0:T(8,128)(2,1)}, u32[]{:S(2)}, u32[]{:S(2)}) collective-permute-start(bf16[200,2048]{1,0:T(8,128)(2,1)S(1)} %collective-permute-done.1.refs_2_), channel_id=1, source_target_pairs={{0,1},{1,0},{2,3},{3,2},{4,5},{5,4},{6,7},{7,6},{8,9},{9,8},{10,11... | collective-permute-start | bytes 2457608 | tf_op jit(solution)/shard_map/ppermute | solution.py:362
  131.8 1.9 collective-permute-start.4
  133.8 2.4 %collective-permute-start.6 = (bf16[200,2048]{1,0:T(8,128)(2,1)S(1)}, bf16[200,2048]{1,0:T(8,128)(2,1)}, u32[]{:S(2)}, u32[]{:S(2)}) collective-permute-start(bf16[200,2048]{1,0:T(8,128)(2,1)S(1)} %collective-permute-done.5.refs_6_), channel_id=1, source_target_pairs={{0,1},{1,0},{2,3},{3,2},{4,5},{5,4},{6,7},{7,6},{8,9},{9,8},{10,11... | collective-permute-start | bytes 2457608 | tf_op jit(solution)/shard_map/ppermute | solution.py:362
  138.3 9.9 %states.1 = (bf16[64,16,128]{2,1,0:T(8,128)(2,1)}, bf16[4,384,256]{2,1,0:T(8,128)(2,1)}) custom-call(bf16[200,2048]{1,0:T(8,128)(2,1)} %norm.1.refs_0_, bf16[200,2048]{1,0:T(8,128)(2,1)} %copy-done.5, bf16[200,2048]{1,0:T(8,128)(2,1)} %copy-done.2, bf16[200,2048]{1,0:T(8,128)(2,1)} %collective-permute-done.2.refs_3_, bf16[200,2048]{1,0:T(8,128)(2,1)} %copy-done.3, ...), custom_call_target="tpu_custom_call" | custom-call | tf_op jit(solution)/shard_map/states/pallas_call | solution.py:183
  148.2 26.2 %all_to_all.20.in_ref = bf16[64,16,128]{2,1,0:T(8,128)(2,1)S(1)} all-to-all(bf16[64,16,128]{2,1,0:T(8,128)(2,1)} %get-tuple-element.15), channel_id=1, replica_groups=mesh['sp_0'=8,'sp_1'=8,'fs'=4,'tp'=2] {'sp_0','sp_1'}, dimensions={0} | all-to-all | bytes 524288 | tf_op jit(solution)/shard_map/all_to_all | solution.py:366
  175.3 5.5 %all-to-all-start.2 = ((bf16[64,8,128]{2,1,0:T(8,128)(2,1)}), bf16[64,8,128]{2,1,0:T(8,128)(2,1)S(1)}, u32[]{:S(2)}, u32[]{:S(2)}) async-start(bf16[64,8,128]{2,1,0:T(8,128)(2,1)} %scan.1), calls=%async_computation.2 | async-start | bytes 262144 | tf_op jit(solution)/shard_map/all_to_all | solution.py:366
  180.8 11.3 %inside.1 = (f32[4,384,128]{2,1,0:T(8,128)}, bf16[4,384,128]{2,1,0:T(8,128)(2,1)}, bf16[4,384,128]{2,1,0:T(8,128)(2,1)}, bf16[4,384,128]{2,1,0:T(8,128)(2,1)}) custom-call(bf16[200,2048]{1,0:T(8,128)(2,1)} %norm.1.refs_0_, bf16[200,2048]{1,0:T(8,128)(2,1)} %copy-done.5, bf16[200,2048]{1,0:T(8,128)(2,1)} %copy-done.2, ...), custom_call_target="tpu_custom_call" | custom-call | tf_op jit(solution)/shard_map/inside/pallas_call | solution.py:262
  192.8 2.7 %collective-permute-start.7 = (bf16[4,16,128]{2,1,0:T(8,128)(2,1)S(1)}, bf16[4,16,128]{2,1,0:T(8,128)(2,1)S(1)}, u32[]{:S(2)}, u32[]{:S(2)}) collective-permute-start(bf16[4,16,128]{2,1,0:T(8,128)(2,1)S(1)} %slice.3), channel_id=1, source_target_pairs={{0,8},{8,16},{16,24},{24,32},{32,40},{40,48},{48,56},{56,64},{64,7... | collective-permute-start | bytes 49160 | tf_op jit(solution)/shard_map/ppermute | solution.py:413
  197.1 4.1 %mix.1 = bf16[8,192,256]{2,1,0:T(8,128)(2,1)} custom-call(f32[4,384,128]{2,1,0:T(8,128)} %get-tuple-element.13.inside_ref, bf16[4,384,128]{2,1,0:T(8,128)(2,1)} %get-tuple-element.14.reach_ref, bf16[4,128,128]{2,1,0:T(8,128)(2,1)} %bitcast.16, bf16[4,384,128]{2,1,0:T(8,128)(2,1)} %get-tuple-element.16.gate_ref, ...), custom_call_target="tpu_custom_call" | custom-call | tf_op jit(solution)/shard_map/mix/pallas_call | solution.py:304
  201.2 19.2 %all_to_all.21.mix_ref = bf16[8,192,256]{2,1,0:T(8,128)(2,1)S(1)} all-to-all(bf16[8,192,256]{2,1,0:T(8,128)(2,1)} %mix.1), channel_id=1, replica_groups=mesh['sp_0'=8,'sp_1'=8,'fs'=4,'tp'=2] {'fs','tp'}, dimensions={0} | all-to-all | bytes 1572864 | tf_op jit(solution)/shard_map/all_to_all | solution.py:366
  220.4 2.2 copy-done.1
  222.6 6.0 %out.1 = bf16[192,2048]{1,0:T(8,128)(2,1)} custom-call(bf16[8,192,256]{2,1,0:T(8,128)(2,1)S(1)} %all_to_all.21.mix_ref, bf16[4,1024,512]{2,1,0:T(8,128)(2,1)S(1)} %bitcast.13, bf16[4,1024,512]{2,1,0:T(8,128)(2,1)} %collective-permute-done.8.far_ref), custom_call_target="tpu_custom_call" | custom-call | tf_op jit(solution)/shard_map/out/pallas_call | solution.py:349
  (33 shorter events, 6.7 us)
Async XLA Ops:
  6.5 129.6 %copy-start = (f32[512]{0:T(512)S(1)}, f32[512]{0:T(512)}, u32[]{:S(2)}) copy-start(f32[512]{0:T(512)} %param.21) | copy-start | bytes 6148
  8.1 17.8 %all-to-all-start = ((bf16[8,32,640]{2,1,0:T(8,128)(2,1)}), bf16[8,32,640]{2,1,0:T(8,128)(2,1)S(1)}, u32[]{:S(2)}, u32[]{:S(2)}) async-start(bf16[8,32,640]{2,1,0:T(8,128)(2,1)} %slab.1), calls=%async_computation | async-start | bytes 655360 | tf_op jit(solution)/shard_map/all_to_all | solution.py:366
  15.8 67.2 %all-gather.6.cloned.1.call-start = ((), (), s32[]{:S(2)}) async-start(), calls=%async_computation.5 | async-start | bytes 5242880 | tf_op jit(solution)/shard_map/all_gather | solution.py:401
  26.7 111.6 %all-gather.4.cloned.1.call-start = ((), (), s32[]{:S(2)}) async-start(), calls=%async_computation.4 | async-start | bytes 2949120 | tf_op jit(solution)/shard_map/all_gather | solution.py:388
  83.0 137.4 %collective-permute-start.8 = (bf16[4,1024,512]{2,1,0:T(8,128)(2,1)}, bf16[4,1024,512]{2,1,0:T(8,128)(2,1)}, u32[]{:S(2)}, u32[]{:S(2)}) collective-permute-start(bf16[4,1024,512]{2,1,0:T(8,128)(2,1)} %bitcast.12), channel_id=1, source_target_pairs={{0,1},{1,0},{2,3},{3,2},{4,5},{5,4},{6,7},{7,6},{8,9},{9,8},{10,11... | collective-permute-start | bytes 12582920 | tf_op jit(solution)/shard_map/ppermute | solution.py:362
  88.4 40.6 %collective-permute-start.1 = (bf16[200,2048]{1,0:T(8,128)(2,1)}, bf16[200,2048]{1,0:T(8,128)(2,1)S(1)}, u32[]{:S(2)}, u32[]{:S(2)}) collective-permute-start(bf16[200,2048]{1,0:T(8,128)(2,1)} %norm.1.refs_0_), channel_id=1, source_target_pairs={{0,2},{2,4},{4,6},{6,0},{1,3},{3,5},{5,7},{7,1},{8,10},{10,12},{12... | collective-permute-start | bytes 2457608 | tf_op jit(solution)/shard_map/ppermute | solution.py:362
  90.8 41.0 %collective-permute-start.3 = (bf16[200,2048]{1,0:T(8,128)(2,1)}, bf16[200,2048]{1,0:T(8,128)(2,1)S(1)}, u32[]{:S(2)}, u32[]{:S(2)}) collective-permute-start(bf16[200,2048]{1,0:T(8,128)(2,1)} %norm.1.refs_0_), channel_id=1, source_target_pairs={{0,6},{2,0},{4,2},{6,4},{1,7},{3,1},{5,3},{7,5},{8,14},{10,8},{12,... | collective-permute-start | bytes 2457608 | tf_op jit(solution)/shard_map/ppermute | solution.py:362
  94.9 38.9 %collective-permute-start.5 = (bf16[200,2048]{1,0:T(8,128)(2,1)}, bf16[200,2048]{1,0:T(8,128)(2,1)S(1)}, u32[]{:S(2)}, u32[]{:S(2)}) collective-permute-start(bf16[200,2048]{1,0:T(8,128)(2,1)} %norm.1.refs_0_), channel_id=1, source_target_pairs={{0,4},{2,6},{4,0},{6,2},{1,5},{3,7},{5,1},{7,3},{8,12},{10,14},{12... | collective-permute-start | bytes 2457608 | tf_op jit(solution)/shard_map/ppermute | solution.py:362
  97.3 39.5 %collective-permute-start = (bf16[200,2048]{1,0:T(8,128)(2,1)}, bf16[200,2048]{1,0:T(8,128)(2,1)S(1)}, u32[]{:S(2)}, u32[]{:S(2)}) collective-permute-start(bf16[200,2048]{1,0:T(8,128)(2,1)} %norm.1.refs_0_), channel_id=1, source_target_pairs={{0,1},{1,0},{2,3},{3,2},{4,5},{5,4},{6,7},{7,6},{8,9},{9,8},{10,11... | collective-permute-start | bytes 2457608 | tf_op jit(solution)/shard_map/ppermute | solution.py:362
  129.0 9.2 %copy-start.2 = (bf16[200,2048]{1,0:T(8,128)(2,1)}, bf16[200,2048]{1,0:T(8,128)(2,1)S(1)}, u32[]{:S(2)}) copy-start(bf16[200,2048]{1,0:T(8,128)(2,1)S(1)} %collective-permute-done.1.refs_2_) | copy-start | bytes 2457604
  129.0 7.8 %collective-permute-start.2 = (bf16[200,2048]{1,0:T(8,128)(2,1)S(1)}, bf16[200,2048]{1,0:T(8,128)(2,1)}, u32[]{:S(2)}, u32[]{:S(2)}) collective-permute-start(bf16[200,2048]{1,0:T(8,128)(2,1)S(1)} %collective-permute-done.1.refs_2_), channel_id=1, source_target_pairs={{0,1},{1,0},{2,3},{3,2},{4,5},{5,4},{6,7},{7,6},{8,9},{9,8},{10,11... | collective-permute-start | bytes 2457608 | tf_op jit(solution)/shard_map/ppermute | solution.py:362
  131.8 6.5 %copy-start.3 = (bf16[200,2048]{1,0:T(8,128)(2,1)}, bf16[200,2048]{1,0:T(8,128)(2,1)S(1)}, u32[]{:S(2)}) copy-start(bf16[200,2048]{1,0:T(8,128)(2,1)S(1)} %collective-permute-done.3.refs_4_) | copy-start | bytes 2457604
  131.8 5.0 %collective-permute-start.4 = (bf16[200,2048]{1,0:T(8,128)(2,1)S(1)}, bf16[200,2048]{1,0:T(8,128)(2,1)}, u32[]{:S(2)}, u32[]{:S(2)}) collective-permute-start(bf16[200,2048]{1,0:T(8,128)(2,1)S(1)} %collective-permute-done.3.refs_4_), channel_id=1, source_target_pairs={{0,1},{1,0},{2,3},{3,2},{4,5},{5,4},{6,7},{7,6},{8,9},{9,8},{10,11... | collective-permute-start | bytes 2457608 | tf_op jit(solution)/shard_map/ppermute | solution.py:362
  133.7 4.5 %copy-start.4 = (bf16[200,2048]{1,0:T(8,128)(2,1)}, bf16[200,2048]{1,0:T(8,128)(2,1)S(1)}, u32[]{:S(2)}) copy-start(bf16[200,2048]{1,0:T(8,128)(2,1)S(1)} %collective-permute-done.5.refs_6_) | copy-start | bytes 2457604
  133.8 4.5 %collective-permute-start.6 = (bf16[200,2048]{1,0:T(8,128)(2,1)S(1)}, bf16[200,2048]{1,0:T(8,128)(2,1)}, u32[]{:S(2)}, u32[]{:S(2)}) collective-permute-start(bf16[200,2048]{1,0:T(8,128)(2,1)S(1)} %collective-permute-done.5.refs_6_), channel_id=1, source_target_pairs={{0,1},{1,0},{2,3},{3,2},{4,5},{5,4},{6,7},{7,6},{8,9},{9,8},{10,11... | collective-permute-start | bytes 2457608 | tf_op jit(solution)/shard_map/ppermute | solution.py:362
  136.8 1.4 copy-start.5
  175.3 21.1 %all-to-all-start.2 = ((bf16[64,8,128]{2,1,0:T(8,128)(2,1)}), bf16[64,8,128]{2,1,0:T(8,128)(2,1)S(1)}, u32[]{:S(2)}, u32[]{:S(2)}) async-start(bf16[64,8,128]{2,1,0:T(8,128)(2,1)} %scan.1), calls=%async_computation.2 | async-start | bytes 262144 | tf_op jit(solution)/shard_map/all_to_all | solution.py:366
  192.8 3.6 %collective-permute-start.7 = (bf16[4,16,128]{2,1,0:T(8,128)(2,1)S(1)}, bf16[4,16,128]{2,1,0:T(8,128)(2,1)S(1)}, u32[]{:S(2)}, u32[]{:S(2)}) collective-permute-start(bf16[4,16,128]{2,1,0:T(8,128)(2,1)S(1)} %slice.3), channel_id=1, source_target_pairs={{0,8},{8,16},{16,24},{24,32},{32,40},{40,48},{48,56},{56,64},{64,7... | collective-permute-start | bytes 49160 | tf_op jit(solution)/shard_map/ppermute | solution.py:413
  196.4 0.6 copy-start.7
  196.4 0.7 copy-start.6
  220.4 2.2 copy-start.1
Sparse Core Ops, SparseCore 0:
  26.8 56.1 all-gather.5
  85.1 42.8 all-gather.3

commit v5 on v3

--- a/solution.py
+++ b/solution.py
@@ -11,6 +11,7 @@
 F32 = jnp.float32
 BF16 = jnp.bfloat16
 LANES = 128
+SLOT_SHIFT = (0, 3, 1, 2)
 
 
 def struct(shape, dtype):
@@ -82,17 +83,24 @@
     )(*weights)
 
 
-def relay_kernel(in_ref, o_ref):
-    o_ref[...] = in_ref[...]
-
-
-def relayed(rows):
+def relay_kernel(in_ref, early_ref, late_ref):
+    early = in_ref[:, : 2 * LANES]
+    for k in range(early_ref.shape[0]):
+        early_ref[k] = early
+    late_ref[...] = in_ref[:, 2 * LANES :]
+
+
+def split_columns(rows, copies):
+    deep, wide = rows.shape
     return pl.pallas_call(
         relay_kernel,
-        out_shape=struct(rows.shape, rows.dtype),
+        out_shape=(
+            struct((copies, deep, 2 * LANES), BF16),
+            struct((deep, wide - 2 * LANES), BF16),
+        ),
         in_specs=vmem(1),
-        out_specs=vmem(1)[0],
-        compiler_params=pltpu.CompilerParams(vmem_limit_bytes=2 << 20),
+        out_specs=tuple(vmem(2)),
+        compiler_params=pltpu.CompilerParams(vmem_limit_bytes=4 << 20),
         name="relay",
     )(rows)
 
@@ -130,7 +138,7 @@
 def state_kernel(*refs):
     tok_refs, rest = refs[:8], refs[8:]
     w_ref, floor_ref, state_ref, raw_ref, toks, sems, weights, w_sem = rest
-    w_copy = pltpu.make_async_copy(w_ref.at[:, : 2 * LANES], weights, w_sem)
+    w_copy = pltpu.make_async_copy(w_ref, weights, w_sem)
     copies = fetches(tok_refs, toks, sems)
     for copy in [w_copy] + copies[:4]:
         copy.start()
@@ -220,7 +228,7 @@
     tok_refs, rest = refs[:8], refs[8:]
     w_ref, floor_ref, early_ref, *rest = rest
     inside_ref, reach_ref, gate_ref, signal_ref, toks, sems, weights, w_sem, raw = rest
-    w_copy = pltpu.make_async_copy(w_ref.at[:, 2 * LANES :], weights, w_sem)
+    w_copy = pltpu.make_async_copy(w_ref, weights, w_sem)
     copies = fetches(tok_refs, toks, sems)
     for copy in [w_copy] + copies[:4]:
         copy.start()
@@ -318,29 +326,45 @@
     )(inside, reach, state, gate, signal, rim, taps, gain)
 
 
-def out_kernel(mix_ref, near_ref, far_ref, o_ref):
+def out_kernel(mix_ref, *refs):
+    piece_refs, (o_ref, pieces, sems) = refs[:8], refs[8:]
+    copies = [pltpu.make_async_copy(ref, pieces.at[k], sems.at[k]) for k, ref in enumerate(piece_refs)]
+    for copy in copies[:4]:
+        copy.start()
     core = lax.axis_index("tp")
-    total = jnp.zeros(o_ref.shape, F32)
-    for c, w_ref in ((core, near_ref), (1 - core, far_ref)):
-        pieces = [mix_ref[2 * x + c] for x in range(4)]
-        lhs = jnp.concatenate(
-            [piece[:, :LANES] for piece in pieces] + [piece[:, LANES:] for piece in pieces], axis=1
+    x = lax.axis_index("fs")
+    rows = []
+    for c in (core, 1 - core):
+        parts = [mix_ref[2 * k + c] for k in range(4)]
+        rows.append(
+            jnp.concatenate(
+                [part[:, :LANES] for part in parts] + [part[:, LANES:] for part in parts], axis=1
+            )
         )
-        total = total + dot(lhs, w_ref[0])
-    o_ref[...] = total.astype(BF16)
-
-
-def out_rows(mix, near, far):
+    wide = piece_refs[0].shape[1]
+    for k in range(4):
+        copies[2 * k].wait()
+        copies[2 * k + 1].wait()
+        if k < 2:
+            copies[2 * k + 4].start()
+            copies[2 * k + 5].start()
+        start = pl.multiple_of((x + SLOT_SHIFT[k]) % 4 * wide, wide)
+        total = dot(rows[0], pieces[2 * k]) + dot(rows[1], pieces[2 * k + 1])
+        o_ref[:, pl.ds(start, wide)] = total.astype(BF16)
+
+
+def out_rows(mix, nears, fars):
     rows = mix.shape[1]
-    pieces, deep, wide = near.shape
+    deep, wide = nears[0].shape
+    pieces = [piece for pair in zip(nears, fars) for piece in pair]
     return pl.pallas_call(
         out_kernel,
-        out_shape=struct((rows, pieces * wide), BF16),
-        grid=(pieces,),
-        in_specs=[whole(*mix.shape), sequence_block(deep, wide), sequence_block(deep, wide)],
-        out_specs=pl.BlockSpec((rows, wide), lambda j: (0, j)),
+        out_shape=struct((rows, 4 * wide), BF16),
+        in_specs=[*vmem(1), *anywhere(8)],
+        out_specs=vmem(1)[0],
+        scratch_shapes=[pltpu.VMEM((8, deep, wide), BF16), pltpu.SemaphoreType.DMA((8,))],
         name="out",
-    )(mix, near, far)
+    )(mix, *pieces)
 
 
 def ring(array, axis, by):
@@ -370,8 +394,9 @@
     x = lax.axis_index("fs")
     slabs = weight_slabs((forget_w, value_w, query_w, conv_gate_w, conv_in_w), 8)
     y_rows = exchanged(slabs, "sp_1").reshape(-1, slabs.shape[2])
-    y_rows = relayed(y_rows)
-    weights = lax.all_gather(y_rows, "sp_0", axis=0, tiled=True)
+    early, late = split_columns(y_rows, 8)
+    early_w = exchanged(early, "sp_0").reshape(-1, early.shape[2])
+    late_w = lax.all_gather(late, "sp_0", axis=0, tiled=True)
 
     own = norm_rows(tokens[0], norm_gain, leak[0].T)
     near = [own]
@@ -383,17 +408,20 @@
     toks = [part for pair in zip(near, far) for part in pair]
 
     out_w = jnp.concatenate([conv_out_w, chain_out_w], axis=0)
-    out_w, y_rows = lax.optimization_barrier((out_w, y_rows))
-    out_near = lax.all_gather(out_w, "fs", axis=0)
-    out_far = ring(out_near, "tp", 1)
+    out_near = [out_w]
+    for by in (1, 3, 2):
+        out_near.append(ring(out_w, "fs", by))
+    out_far = []
+    for part in out_near:
+        out_far.append(ring(part, "tp", 1))
 
     floor = lax.dynamic_slice_in_dim(floor_gate, x * LANES, LANES, 0)[None]
-    states, early = local_states(toks, weights, floor)
+    states, projected = local_states(toks, early_w, floor)
     arrived = exchanged(states, SP)
     before = exchanged(scan_blocks(arrived), SP)
     before = before.reshape(4, LANES, LANES)
 
-    inside, reach, gate, signal = inside_blocks(toks, weights, floor, early)
+    inside, reach, gate, signal = inside_blocks(toks, late_w, floor, projected)
     count = 64
     tail = signal[:, -16:, :]
     rim = lax.ppermute(tail, SP, [(i, i + 1) for i in range(count - 1)])

time: 234 us -> 195 us (0.83)
  starting transfers between devices: 37.5 us -> 101 us
  waiting for transfers between devices: 95.3 us -> 34.6 us
  blocking collectives: 45.5 us -> 0 us
  local copies, waits for them, and re-layouts: 2.01 us -> 6.61 us
    all_gather x2 -> x1, waiting for transfers between devices: 55.6 us -> 0.02 us  [layer(): late_w = lax.all_gather(late, 'sp_0', axis=0, tiled=True)]
    all_to_all x2 -> x0, blocking collectives: 45.5 us -> none  [exchanged(): return lax.all_to_all(array, axis, split_axis=0, concat_axis=0, tiled=True)]
    all_to_all x2 -> x5, starting transfers between devices: 13.1 us -> 52.2 us  [exchanged(): return lax.all_to_all(array, axis, split_axis=0, concat_axis=0, tiled=True)]
    ppermute x8 -> x14, starting transfers between devices: 21.6 us -> 46.1 us  [ring(): lax.ppermute(array, axis, [(i, (i + by) % count) for i in range(count)])]
    ppermute x8 -> x14, waiting for transfers between devices: 30.3 us -> 18.9 us  [ring(): lax.ppermute(array, axis, [(i, (i + by) % count) for i in range(count)])]
    all_to_all x2 -> x5, waiting for transfers between devices: 7.8 us -> 14.8 us  [exchanged(): return lax.all_to_all(array, axis, split_axis=0, concat_axis=0, tiled=True)]
    unnamed x14 -> x25, local copies, waits for them, and re-layouts: 0.68 us -> 3.34 us
  transfers between devices with their start and end apart: 13 -> 21, of which waited for: 5 -> 5; matrix products, arithmetic and copies ran while one was open for 2% -> 2% of each run, Pallas kernels for 12% -> 15%
where the time goes in v5:
time: 195 us; the launch traced here: 192 us
  starting transfers between devices  101 us (52%)
  Pallas kernels  36.2 us (19%)
  waiting for transfers between devices  34.6 us (18%)
  between operations  13.8 us (7%)
  local copies, waits for them, and re-layouts  6.61 us (3%)
    all_to_all x5, starting transfers between devices, exchanged(): return lax.all_to_all(array, axis, split_axis=0, concat_axis=0, tiled=True)  52.2 us
    ppermute x14, starting transfers between devices, ring(): lax.ppermute(array, axis, [(i, (i + by) % count) for i in range(count)])  46.1 us
    ppermute x14, waiting for transfers between devices, ring(): lax.ppermute(array, axis, [(i, (i + by) % count) for i in range(count)])  18.9 us
    all_to_all x5, waiting for transfers between devices, exchanged(): return lax.all_to_all(array, axis, split_axis=0, concat_axis=0, tiled=True)  14.8 us
    pallas_call x1, Pallas kernels, inside_blocks(): pl.pallas_call(inside_kernel, out_shape=(struct(block, F32), struct(block...  11 us
    pallas_call x1, Pallas kernels, local_states(): pl.pallas_call(state_kernel, out_shape=(struct((64, 16, LANES), BF16), st...  8.47 us
    pallas_call x1, Pallas kernels, out_rows(): pl.pallas_call(out_kernel, out_shape=struct((rows, 4 * wide), BF16), in_s...  6.49 us
    pallas_call x1, Pallas kernels, mix_blocks(): pl.pallas_call(mix_kernel, out_shape=struct((8, length // 2, 2 * LANES),...  4.09 us
  transfers between devices with their start and end apart: 21, of which 5 were waited for; matrix products, arithmetic and copies ran while one was open for 2% of the time, Pallas kernels for 15%

profile of v5, /device:TPU:1, one launch (start us, length us, event | category | flops | bytes accessed | tf_op | source)
XLA Modules:
  0.0 192.2 jit_solution(17985410414400683106)
XLA Ops:
  8.1 7.6 %all-to-all-start = ((bf16[8,32,640]{2,1,0:T(8,128)(2,1)}), bf16[8,32,640]{2,1,0:T(8,128)(2,1)S(1)}, u32[]{:S(2)}, u32[]{:S(2)}) async-start(bf16[8,32,640]{2,1,0:T(8,128)(2,1)} %slab.1), calls=%async_computation | async-start | bytes 655360 | tf_op jit(solution)/shard_map/all_to_all | solution.py:376
  15.8 2.6 %norm.1.refs_0_ = bf16[200,2048]{1,0:T(8,128)(2,1)} custom-call(bf16[192,2048]{1,0:T(8,128)(2,1)} %bitcast.14, f32[1,2048]{1,0:T(1,128)} %bitcast.16, f32[4,384]{1,0:T(4,128)} %bitcast.17), custom_call_target="tpu_custom_call" | custom-call | tf_op jit(solution)/shard_map/norm/pallas_call | solution.py:58
  18.4 4.8 %collective-permute-start.5 = (bf16[200,2048]{1,0:T(8,128)(2,1)}, bf16[200,2048]{1,0:T(8,128)(2,1)S(1)}, u32[]{:S(2)}, u32[]{:S(2)}) collective-permute-start(bf16[200,2048]{1,0:T(8,128)(2,1)} %norm.1.refs_0_), channel_id=1, source_target_pairs={{0,4},{2,6},{4,0},{6,2},{1,5},{3,7},{5,1},{7,3},{8,12},{10,14},{12... | collective-permute-start | bytes 2457608 | tf_op jit(solution)/shard_map/ppermute | solution.py:372
  23.2 2.7 %all-to-all-done = bf16[8,32,640]{2,1,0:T(8,128)(2,1)S(1)} async-done(((bf16[8,32,640]{2,1,0:T(8,128)(2,1)}), bf16[8,32,640]{2,1,0:T(8,128)(2,1)S(1)}, u32[]{:S(2)}, u32[]{:S(2)}) %all-to-all-start) | async-done | bytes 327712 | tf_op jit(solution)/shard_map/all_to_all | solution.py:376
  27.0 12.0 %all-to-all-start.1 = ((bf16[8,256,256]{2,1,0:T(8,128)(2,1)}), bf16[8,256,256]{2,1,0:T(8,128)(2,1)S(1)}, u32[]{:S(2)}, u32[]{:S(2)}) async-start(bf16[8,256,256]{2,1,0:T(8,128)(2,1)} %get-tuple-element.14), calls=%async_computation.1 | async-start | bytes 2097152 | tf_op jit(solution)/shard_map/all_to_all | solution.py:376
  39.0 4.4 %collective-permute-start.3 = (bf16[200,2048]{1,0:T(8,128)(2,1)S(1)}, bf16[200,2048]{1,0:T(8,128)(2,1)}, u32[]{:S(2)}, u32[]{:S(2)}) collective-permute-start(bf16[200,2048]{1,0:T(8,128)(2,1)S(1)} %copy-done.1), channel_id=1, source_target_pairs={{0,6},{2,0},{4,2},{6,4},{1,7},{3,1},{5,3},{7,5},{8,14},{10,8},{12,... | collective-permute-start | bytes 2457608 | tf_op jit(solution)/shard_map/ppermute | solution.py:372
  45.4 4.6 %collective-permute-start = (bf16[200,2048]{1,0:T(8,128)(2,1)S(1)}, bf16[200,2048]{1,0:T(8,128)(2,1)S(1)}, u32[]{:S(2)}, u32[]{:S(2)}) collective-permute-start(bf16[200,2048]{1,0:T(8,128)(2,1)S(1)} %copy-done.1), channel_id=1, source_target_pairs={{0,1},{1,0},{2,3},{3,2},{4,5},{5,4},{6,7},{7,6},{8,9},{9,8},{10,11... | collective-permute-start | bytes 2457608 | tf_op jit(solution)/shard_map/ppermute | solution.py:372
  51.9 6.7 %collective-permute-done.3.refs_4_ = bf16[200,2048]{1,0:T(8,128)(2,1)} collective-permute-done((bf16[200,2048]{1,0:T(8,128)(2,1)S(1)}, bf16[200,2048]{1,0:T(8,128)(2,1)}, u32[]{:S(2)}, u32[]{:S(2)}) %collective-permute-start.3) | collective-permute-done | bytes 819232 | tf_op jit(solution)/shard_map/ppermute | solution.py:372
  58.6 5.2 %collective-permute-start.4 = (bf16[200,2048]{1,0:T(8,128)(2,1)}, bf16[200,2048]{1,0:T(8,128)(2,1)}, u32[]{:S(2)}, u32[]{:S(2)}) collective-permute-start(bf16[200,2048]{1,0:T(8,128)(2,1)} %collective-permute-done.3.refs_4_), channel_id=1, source_target_pairs={{0,1},{1,0},{2,3},{3,2},{4,5},{5,4},{6,7},{7,6},{8,9},{9,8},{10,11... | collective-permute-start | bytes 2457608 | tf_op jit(solution)/shard_map/ppermute | solution.py:372
  63.8 5.4 %collective-permute-start.2 = (bf16[200,2048]{1,0:T(8,128)(2,1)}, bf16[200,2048]{1,0:T(8,128)(2,1)}, u32[]{:S(2)}, u32[]{:S(2)}) collective-permute-start(bf16[200,2048]{1,0:T(8,128)(2,1)} %collective-permute-done.1.refs_2_), channel_id=1, source_target_pairs={{0,1},{1,0},{2,3},{3,2},{4,5},{5,4},{6,7},{7,6},{8,9},{9,8},{10,11... | collective-permute-start | bytes 2457608 | tf_op jit(solution)/shard_map/ppermute | solution.py:372
  74.0 3.1 %collective-permute-start.11 = (bf16[1024,512]{1,0:T(8,128)(2,1)}, bf16[1024,512]{1,0:T(8,128)(2,1)S(1)}, u32[]{:S(2)}, u32[]{:S(2)}) collective-permute-start(bf16[1024,512]{1,0:T(8,128)(2,1)} %constant_dynamic-update-slice_fusion.refs_0_), channel_id=1, source_target_pairs={{0,6},{2,0},{4,2},{6,4},{1,7},{3,1},{5,3},{7,5},{8,14},{10,8},{12,... | collective-permute-start | bytes 3145736 | tf_op jit(solution)/shard_map/ppermute | solution.py:372
  80.9 8.5 %states.1 = (bf16[64,16,128]{2,1,0:T(8,128)(2,1)}, bf16[4,384,256]{2,1,0:T(8,128)(2,1)}) custom-call(bf16[200,2048]{1,0:T(8,128)(2,1)} %norm.1.refs_0_, bf16[200,2048]{1,0:T(8,128)(2,1)} %copy-done.4, bf16[200,2048]{1,0:T(8,128)(2,1)} %collective-permute-done.1.refs_2_, bf16[200,2048]{1,0:T(8,128)(2,1)} %collective-permute-done.2.refs_3_, ...), custom_call_target="tpu_custom_call" | custom-call | tf_op jit(solution)/shard_map/states/pallas_call | solution.py:188
  89.4 13.3 %all-to-all-start.2 = ((bf16[64,16,128]{2,1,0:T(8,128)(2,1)}), bf16[64,16,128]{2,1,0:T(8,128)(2,1)S(1)}, u32[]{:S(2)}, u32[]{:S(2)}) async-start(bf16[64,16,128]{2,1,0:T(8,128)(2,1)} %get-tuple-element.18), calls=%async_computation.2 | async-start | bytes 524288 | tf_op jit(solution)/shard_map/all_to_all | solution.py:376
  102.7 3.2 %collective-permute-start.8 = (bf16[1024,512]{1,0:T(8,128)(2,1)}, bf16[1024,512]{1,0:T(8,128)(2,1)S(1)}, u32[]{:S(2)}, u32[]{:S(2)}) collective-permute-start(bf16[1024,512]{1,0:T(8,128)(2,1)} %constant_dynamic-update-slice_fusion.refs_0_), channel_id=1, source_target_pairs={{0,1},{1,0},{2,3},{3,2},{4,5},{5,4},{6,7},{7,6},{8,9},{9,8},{10,11... | collective-permute-start | bytes 3145736 | tf_op jit(solution)/shard_map/ppermute | solution.py:372
  107.9 12.2 %collective-permute-done.11.refs_4_ = bf16[1024,512]{1,0:T(8,128)(2,1)S(1)} collective-permute-done((bf16[1024,512]{1,0:T(8,128)(2,1)}, bf16[1024,512]{1,0:T(8,128)(2,1)S(1)}, u32[]{:S(2)}, u32[]{:S(2)}) %collective-permute-start.11) | collective-permute-done | bytes 1048608 | tf_op jit(solution)/shard_map/ppermute | solution.py:372
  120.1 3.1 %collective-permute-start.12 = (bf16[1024,512]{1,0:T(8,128)(2,1)S(1)}, bf16[1024,512]{1,0:T(8,128)(2,1)}, u32[]{:S(2)}, u32[]{:S(2)}) collective-permute-start(bf16[1024,512]{1,0:T(8,128)(2,1)S(1)} %collective-permute-done.11.refs_4_), channel_id=1, source_target_pairs={{0,1},{1,0},{2,3},{3,2},{4,5},{5,4},{6,7},{7,6},{8,9},{9,8},{10,11... | collective-permute-start | bytes 3145736 | tf_op jit(solution)/shard_map/ppermute | solution.py:372
  123.3 2.4 %collective-permute-start.10 = (bf16[1024,512]{1,0:T(8,128)(2,1)}, bf16[1024,512]{1,0:T(8,128)(2,1)}, u32[]{:S(2)}, u32[]{:S(2)}) collective-permute-start(bf16[1024,512]{1,0:T(8,128)(2,1)} %collective-permute-done.9.refs_2_), channel_id=1, source_target_pairs={{0,1},{1,0},{2,3},{3,2},{4,5},{5,4},{6,7},{7,6},{8,9},{9,8},{10,11... | collective-permute-start | bytes 3145736 | tf_op jit(solution)/shard_map/ppermute | solution.py:372
  126.6 13.3 %all-to-all-start.3 = ((bf16[64,8,128]{2,1,0:T(8,128)(2,1)}), bf16[64,8,128]{2,1,0:T(8,128)(2,1)S(1)}, u32[]{:S(2)}, u32[]{:S(2)}) async-start(bf16[64,8,128]{2,1,0:T(8,128)(2,1)} %scan.1), calls=%async_computation.3 | async-start | bytes 262144 | tf_op jit(solution)/shard_map/all_to_all | solution.py:376
  139.9 11.0 %inside.1 = (f32[4,384,128]{2,1,0:T(8,128)}, bf16[4,384,128]{2,1,0:T(8,128)(2,1)}, bf16[4,384,128]{2,1,0:T(8,128)(2,1)}, bf16[4,384,128]{2,1,0:T(8,128)(2,1)}) custom-call(bf16[200,2048]{1,0:T(8,128)(2,1)} %norm.1.refs_0_, bf16[200,2048]{1,0:T(8,128)(2,1)} %copy-done.4, bf16[200,2048]{1,0:T(8,128)(2,1)} %collective-permute-done.1.refs_2_, ...), custom_call_target="tpu_custom_call" | custom-call | tf_op jit(solution)/shard_map/inside/pallas_call | solution.py:267
  151.7 2.7 %collective-permute-start.7 = (bf16[4,16,128]{2,1,0:T(8,128)(2,1)S(1)}, bf16[4,16,128]{2,1,0:T(8,128)(2,1)S(1)}, u32[]{:S(2)}, u32[]{:S(2)}) collective-permute-start(bf16[4,16,128]{2,1,0:T(8,128)(2,1)S(1)} %slice.3), channel_id=1, source_target_pairs={{0,8},{8,16},{16,24},{24,32},{32,40},{40,48},{48,56},{56,64},{64,7... | collective-permute-start | bytes 49160 | tf_op jit(solution)/shard_map/ppermute | solution.py:427
  155.9 4.1 %mix.1 = bf16[8,192,256]{2,1,0:T(8,128)(2,1)} custom-call(f32[4,384,128]{2,1,0:T(8,128)} %get-tuple-element.16.inside_ref, bf16[4,384,128]{2,1,0:T(8,128)(2,1)} %get-tuple-element.17.reach_ref, bf16[4,128,128]{2,1,0:T(8,128)(2,1)} %bitcast.15, bf16[4,384,128]{2,1,0:T(8,128)(2,1)} %get-tuple-element.19.gate_ref, ...), custom_call_target="tpu_custom_call" | custom-call | tf_op jit(solution)/shard_map/mix/pallas_call | solution.py:309
  160.0 5.8 %all-to-all-start.4 = ((bf16[8,192,256]{2,1,0:T(8,128)(2,1)}), bf16[8,192,256]{2,1,0:T(8,128)(2,1)S(1)}, u32[]{:S(2)}, u32[]{:S(2)}) async-start(bf16[8,192,256]{2,1,0:T(8,128)(2,1)} %mix.1), calls=%async_computation.4 | async-start | bytes 1572864 | tf_op jit(solution)/shard_map/all_to_all | solution.py:376
  165.8 12.1 %all-to-all-done.4.mix_ref = bf16[8,192,256]{2,1,0:T(8,128)(2,1)S(1)} async-done(((bf16[8,192,256]{2,1,0:T(8,128)(2,1)}), bf16[8,192,256]{2,1,0:T(8,128)(2,1)S(1)}, u32[]{:S(2)}, u32[]{:S(2)}) %all-to-all-start.4) | async-done | bytes 786464 | tf_op jit(solution)/shard_map/all_to_all | solution.py:376
  178.8 6.5 %out.1 = bf16[192,2048]{1,0:T(8,128)(2,1)} custom-call(bf16[8,192,256]{2,1,0:T(8,128)(2,1)} %copy-done.6, bf16[1024,512]{1,0:T(8,128)(2,1)} %constant_dynamic-update-slice_fusion.refs_0_, bf16[1024,512]{1,0:T(8,128)(2,1)} %copy-done.8, bf16[1024,512]{1,0:T(8,128)(2,1)} %collective-permute-done.9.refs_2_, bf16[1024,512]{1,0:T(8,128)(2,1)} %collective-permute-done.10.refs_3_, ...), custom_call_target="tpu_custom_call" | custom-call | tf_op jit(solution)/shard_map/out/pallas_call | solution.py:360
  (55 shorter events, 21.0 us)
Async XLA Ops:
  6.5 72.8 %copy-start = (f32[512]{0:T(512)S(1)}, f32[512]{0:T(512)}, u32[]{:S(2)}) copy-start(f32[512]{0:T(512)} %param.21) | copy-start | bytes 6148
  8.1 17.8 %all-to-all-start = ((bf16[8,32,640]{2,1,0:T(8,128)(2,1)}), bf16[8,32,640]{2,1,0:T(8,128)(2,1)S(1)}, u32[]{:S(2)}, u32[]{:S(2)}) async-start(bf16[8,32,640]{2,1,0:T(8,128)(2,1)} %slab.1), calls=%async_computation | async-start | bytes 655360 | tf_op jit(solution)/shard_map/all_to_all | solution.py:376
  15.8 124.2 %all-gather.2.cloned.1.call-start = ((), (), s32[]{:S(2)}) async-start(), calls=%async_computation.5 | async-start | bytes 1769472 | tf_op jit(solution)/shard_map/all_gather | solution.py:399
  18.4 50.8 %copy-start.10 = (bf16[512,512]{1,0:T(8,128)(2,1)S(1)}, bf16[512,512]{1,0:T(8,128)(2,1)}, u32[]{:S(2)}) copy-start(bf16[512,512]{1,0:T(8,128)(2,1)} %param.24) | copy-start | bytes 1572868
  18.4 31.6 %collective-permute-start.5 = (bf16[200,2048]{1,0:T(8,128)(2,1)}, bf16[200,2048]{1,0:T(8,128)(2,1)S(1)}, u32[]{:S(2)}, u32[]{:S(2)}) collective-permute-start(bf16[200,2048]{1,0:T(8,128)(2,1)} %norm.1.refs_0_), channel_id=1, source_target_pairs={{0,4},{2,6},{4,0},{6,2},{1,5},{3,7},{5,1},{7,3},{8,12},{10,14},{12... | collective-permute-start | bytes 2457608 | tf_op jit(solution)/shard_map/ppermute | solution.py:372
  27.0 52.9 %all-to-all-start.1 = ((bf16[8,256,256]{2,1,0:T(8,128)(2,1)}), bf16[8,256,256]{2,1,0:T(8,128)(2,1)S(1)}, u32[]{:S(2)}, u32[]{:S(2)}) async-start(bf16[8,256,256]{2,1,0:T(8,128)(2,1)} %get-tuple-element.14), calls=%async_computation.1 | async-start | bytes 2097152 | tf_op jit(solution)/shard_map/all_to_all | solution.py:376
  39.0 19.6 %collective-permute-start.3 = (bf16[200,2048]{1,0:T(8,128)(2,1)S(1)}, bf16[200,2048]{1,0:T(8,128)(2,1)}, u32[]{:S(2)}, u32[]{:S(2)}) collective-permute-start(bf16[200,2048]{1,0:T(8,128)(2,1)S(1)} %copy-done.1), channel_id=1, source_target_pairs={{0,6},{2,0},{4,2},{6,4},{1,7},{3,1},{5,3},{7,5},{8,14},{10,8},{12,... | collective-permute-start | bytes 2457608 | tf_op jit(solution)/shard_map/ppermute | solution.py:372
  43.4 20.3 %collective-permute-start.1 = (bf16[200,2048]{1,0:T(8,128)(2,1)S(1)}, bf16[200,2048]{1,0:T(8,128)(2,1)}, u32[]{:S(2)}, u32[]{:S(2)}) collective-permute-start(bf16[200,2048]{1,0:T(8,128)(2,1)S(1)} %copy-done.1), channel_id=1, source_target_pairs={{0,2},{2,4},{4,6},{6,0},{1,3},{3,5},{5,7},{7,1},{8,10},{10,12},{12... | collective-permute-start | bytes 2457608 | tf_op jit(solution)/shard_map/ppermute | solution.py:372
  45.4 28.6 %collective-permute-start = (bf16[200,2048]{1,0:T(8,128)(2,1)S(1)}, bf16[200,2048]{1,0:T(8,128)(2,1)S(1)}, u32[]{:S(2)}, u32[]{:S(2)}) collective-permute-start(bf16[200,2048]{1,0:T(8,128)(2,1)S(1)} %copy-done.1), channel_id=1, source_target_pairs={{0,1},{1,0},{2,3},{3,2},{4,5},{5,4},{6,7},{7,6},{8,9},{9,8},{10,11... | collective-permute-start | bytes 2457608 | tf_op jit(solution)/shard_map/ppermute | solution.py:372
  50.0 27.1 %collective-permute-start.6 = (bf16[200,2048]{1,0:T(8,128)(2,1)S(1)}, bf16[200,2048]{1,0:T(8,128)(2,1)S(1)}, u32[]{:S(2)}, u32[]{:S(2)}) collective-permute-start(bf16[200,2048]{1,0:T(8,128)(2,1)S(1)} %collective-permute-done.5.refs_6_), channel_id=1, source_target_pairs={{0,1},{1,0},{2,3},{3,2},{4,5},{5,4},{6,7},{7,6},{8,9},{9,8},{10,11... | collective-permute-start | bytes 2457608 | tf_op jit(solution)/shard_map/ppermute | solution.py:372
  58.6 21.3 %collective-permute-start.4 = (bf16[200,2048]{1,0:T(8,128)(2,1)}, bf16[200,2048]{1,0:T(8,128)(2,1)}, u32[]{:S(2)}, u32[]{:S(2)}) collective-permute-start(bf16[200,2048]{1,0:T(8,128)(2,1)} %collective-permute-done.3.refs_4_), channel_id=1, source_target_pairs={{0,1},{1,0},{2,3},{3,2},{4,5},{5,4},{6,7},{7,6},{8,9},{9,8},{10,11... | collective-permute-start | bytes 2457608 | tf_op jit(solution)/shard_map/ppermute | solution.py:372
  63.8 16.2 %collective-permute-start.2 = (bf16[200,2048]{1,0:T(8,128)(2,1)}, bf16[200,2048]{1,0:T(8,128)(2,1)}, u32[]{:S(2)}, u32[]{:S(2)}) collective-permute-start(bf16[200,2048]{1,0:T(8,128)(2,1)} %collective-permute-done.1.refs_2_), channel_id=1, source_target_pairs={{0,1},{1,0},{2,3},{3,2},{4,5},{5,4},{6,7},{7,6},{8,9},{9,8},{10,11... | collective-permute-start | bytes 2457608 | tf_op jit(solution)/shard_map/ppermute | solution.py:372
  72.0 33.9 %collective-permute-start.13 = (bf16[1024,512]{1,0:T(8,128)(2,1)}, bf16[1024,512]{1,0:T(8,128)(2,1)}, u32[]{:S(2)}, u32[]{:S(2)}) collective-permute-start(bf16[1024,512]{1,0:T(8,128)(2,1)} %constant_dynamic-update-slice_fusion.refs_0_), channel_id=1, source_target_pairs={{0,4},{2,6},{4,0},{6,2},{1,5},{3,7},{5,1},{7,3},{8,12},{10,14},{12... | collective-permute-start | bytes 3145736 | tf_op jit(solution)/shard_map/ppermute | solution.py:372
  74.0 46.1 %collective-permute-start.11 = (bf16[1024,512]{1,0:T(8,128)(2,1)}, bf16[1024,512]{1,0:T(8,128)(2,1)S(1)}, u32[]{:S(2)}, u32[]{:S(2)}) collective-permute-start(bf16[1024,512]{1,0:T(8,128)(2,1)} %constant_dynamic-update-slice_fusion.refs_0_), channel_id=1, source_target_pairs={{0,6},{2,0},{4,2},{6,4},{1,7},{3,1},{5,3},{7,5},{8,14},{10,8},{12,... | collective-permute-start | bytes 3145736 | tf_op jit(solution)/shard_map/ppermute | solution.py:372
  77.1 46.2 %collective-permute-start.9 = (bf16[1024,512]{1,0:T(8,128)(2,1)}, bf16[1024,512]{1,0:T(8,128)(2,1)}, u32[]{:S(2)}, u32[]{:S(2)}) collective-permute-start(bf16[1024,512]{1,0:T(8,128)(2,1)} %constant_dynamic-update-slice_fusion.refs_0_), channel_id=1, source_target_pairs={{0,2},{2,4},{4,6},{6,0},{1,3},{3,5},{5,7},{7,1},{8,10},{10,12},{12... | collective-permute-start | bytes 3145736 | tf_op jit(solution)/shard_map/ppermute | solution.py:372
  89.4 36.3 %all-to-all-start.2 = ((bf16[64,16,128]{2,1,0:T(8,128)(2,1)}), bf16[64,16,128]{2,1,0:T(8,128)(2,1)S(1)}, u32[]{:S(2)}, u32[]{:S(2)}) async-start(bf16[64,16,128]{2,1,0:T(8,128)(2,1)} %get-tuple-element.18), calls=%async_computation.2 | async-start | bytes 524288 | tf_op jit(solution)/shard_map/all_to_all | solution.py:376
  102.7 63.1 %collective-permute-start.8 = (bf16[1024,512]{1,0:T(8,128)(2,1)}, bf16[1024,512]{1,0:T(8,128)(2,1)S(1)}, u32[]{:S(2)}, u32[]{:S(2)}) collective-permute-start(bf16[1024,512]{1,0:T(8,128)(2,1)} %constant_dynamic-update-slice_fusion.refs_0_), channel_id=1, source_target_pairs={{0,1},{1,0},{2,3},{3,2},{4,5},{5,4},{6,7},{7,6},{8,9},{9,8},{10,11... | collective-permute-start | bytes 3145736 | tf_op jit(solution)/shard_map/ppermute | solution.py:372
  106.0 59.8 %collective-permute-start.14 = (bf16[1024,512]{1,0:T(8,128)(2,1)}, bf16[1024,512]{1,0:T(8,128)(2,1)}, u32[]{:S(2)}, u32[]{:S(2)}) collective-permute-start(bf16[1024,512]{1,0:T(8,128)(2,1)} %collective-permute-done.13.refs_6_), channel_id=1, source_target_pairs={{0,1},{1,0},{2,3},{3,2},{4,5},{5,4},{6,7},{7,6},{8,9},{9,8},{10,11... | collective-permute-start | bytes 3145736 | tf_op jit(solution)/shard_map/ppermute | solution.py:372
  120.1 30.9 %copy-start.7 = (bf16[1024,512]{1,0:T(8,128)(2,1)}, bf16[1024,512]{1,0:T(8,128)(2,1)S(1)}, u32[]{:S(2)}) copy-start(bf16[1024,512]{1,0:T(8,128)(2,1)S(1)} %collective-permute-done.11.refs_4_) | copy-start | bytes 3145732
  120.1 45.7 %collective-permute-start.12 = (bf16[1024,512]{1,0:T(8,128)(2,1)S(1)}, bf16[1024,512]{1,0:T(8,128)(2,1)}, u32[]{:S(2)}, u32[]{:S(2)}) collective-permute-start(bf16[1024,512]{1,0:T(8,128)(2,1)S(1)} %collective-permute-done.11.refs_4_), channel_id=1, source_target_pairs={{0,1},{1,0},{2,3},{3,2},{4,5},{5,4},{6,7},{7,6},{8,9},{9,8},{10,11... | collective-permute-start | bytes 3145736 | tf_op jit(solution)/shard_map/ppermute | solution.py:372
  123.3 42.5 %collective-permute-start.10 = (bf16[1024,512]{1,0:T(8,128)(2,1)}, bf16[1024,512]{1,0:T(8,128)(2,1)}, u32[]{:S(2)}, u32[]{:S(2)}) collective-permute-start(bf16[1024,512]{1,0:T(8,128)(2,1)} %collective-permute-done.9.refs_2_), channel_id=1, source_target_pairs={{0,1},{1,0},{2,3},{3,2},{4,5},{5,4},{6,7},{7,6},{8,9},{9,8},{10,11... | collective-permute-start | bytes 3145736 | tf_op jit(solution)/shard_map/ppermute | solution.py:372
  126.6 27.8 %all-to-all-start.3 = ((bf16[64,8,128]{2,1,0:T(8,128)(2,1)}), bf16[64,8,128]{2,1,0:T(8,128)(2,1)S(1)}, u32[]{:S(2)}, u32[]{:S(2)}) async-start(bf16[64,8,128]{2,1,0:T(8,128)(2,1)} %scan.1), calls=%async_computation.3 | async-start | bytes 262144 | tf_op jit(solution)/shard_map/all_to_all | solution.py:376
  151.7 3.6 %collective-permute-start.7 = (bf16[4,16,128]{2,1,0:T(8,128)(2,1)S(1)}, bf16[4,16,128]{2,1,0:T(8,128)(2,1)S(1)}, u32[]{:S(2)}, u32[]{:S(2)}) collective-permute-start(bf16[4,16,128]{2,1,0:T(8,128)(2,1)S(1)} %slice.3), channel_id=1, source_target_pairs={{0,8},{8,16},{16,24},{24,32},{32,40},{40,48},{48,56},{56,64},{64,7... | collective-permute-start | bytes 49160 | tf_op jit(solution)/shard_map/ppermute | solution.py:427
  160.0 18.0 %all-to-all-start.4 = ((bf16[8,192,256]{2,1,0:T(8,128)(2,1)}), bf16[8,192,256]{2,1,0:T(8,128)(2,1)S(1)}, u32[]{:S(2)}, u32[]{:S(2)}) async-start(bf16[8,192,256]{2,1,0:T(8,128)(2,1)} %mix.1), calls=%async_computation.4 | async-start | bytes 1572864 | tf_op jit(solution)/shard_map/all_to_all | solution.py:376
  (9 other events, 71.4 us)
Sparse Core Ops, SparseCore 0:
  27.1 55.6 all-gather.1

commit v6 on v5

--- a/solution.py
+++ b/solution.py
@@ -137,7 +137,7 @@
 
 def state_kernel(*refs):
     tok_refs, rest = refs[:8], refs[8:]
-    w_ref, floor_ref, state_ref, raw_ref, toks, sems, weights, w_sem = rest
+    w_ref, floor_ref, state_ref, raw_ref, tail_ref, toks, sems, weights, w_sem = rest
     w_copy = pltpu.make_async_copy(w_ref, weights, w_sem)
     copies = fetches(tok_refs, toks, sems)
     for copy in [w_copy] + copies[:4]:
@@ -148,6 +148,8 @@
     lane = lax.broadcasted_iota(jnp.int32, (LANES, LANES), 1)
     w_copy.wait()
     w = weights[...]
+    half = length // 2
+    tails = []
     for r in range(4):
         copies[2 * r].wait()
         copies[2 * r + 1].wait()
@@ -155,6 +157,8 @@
             copies[2 * r + 4].start()
             copies[2 * r + 5].start()
         place_rows(raw_ref.at[r], toks, r, w)
+        last_rows = [toks[2 * r + k, half - 16 : half, :].astype(F32)[8:] for k in range(2)]
+        tails.append(jnp.where(lax.axis_index("tp") == 1, last_rows[0], last_rows[1]))
         keys, running = gates(raw_ref[r, :, :LANES], gap, tri)
         leaks = jnp.broadcast_to(leak_row(toks, r, length), (LANES, length))
         total = running + leaks.T
@@ -168,6 +172,7 @@
             [state.reshape(LANES // 8, 8, LANES), split.reshape(LANES // 8, 8, LANES)], axis=1
         )
         state_ref[r * 16 : (r + 1) * 16] = packed.astype(BF16)
+    tail_ref[...] = jnp.concatenate(tails, axis=0).astype(BF16)
 
 
 def anywhere(count):
@@ -187,9 +192,13 @@
     length = 2 * (toks[0].shape[0] - 8)
     return pl.pallas_call(
         state_kernel,
-        out_shape=(struct((64, 16, LANES), BF16), struct((4, length, 2 * LANES), BF16)),
+        out_shape=(
+            struct((64, 16, LANES), BF16),
+            struct((4, length, 2 * LANES), BF16),
+            struct((32, toks[0].shape[1]), BF16),
+        ),
         in_specs=[*anywhere(9), *vmem(1)],
-        out_specs=tuple(vmem(2)),
+        out_specs=tuple(vmem(3)),
         scratch_shapes=token_scratch(toks[0], w.shape[0], 2 * LANES),
         name="states",
     )(*toks, w, floor)
@@ -226,8 +235,8 @@
 
 def inside_kernel(*refs):
     tok_refs, rest = refs[:8], refs[8:]
-    w_ref, floor_ref, early_ref, *rest = rest
-    inside_ref, reach_ref, gate_ref, signal_ref, toks, sems, weights, w_sem, raw = rest
+    w_ref, floor_ref, early_ref, tail_ref, *rest = rest
+    inside_ref, reach_ref, gate_ref, signal_ref, rim_ref, toks, sems, weights, w_sem, raw = rest
     w_copy = pltpu.make_async_copy(w_ref, weights, w_sem)
     copies = fetches(tok_refs, toks, sems)
     for copy in [w_copy] + copies[:4]:
@@ -238,7 +247,9 @@
     gap = 1.0 - floor_ref[...]
     w_copy.wait()
     w = weights[...]
+    rim = dot(tail_ref[...], weights[:, 2 * LANES :]).astype(BF16).astype(F32)
     for r in range(4):
+        rim_ref[r] = rim[8 * r : 8 * r + 8]
         keys, running = gates(early_ref[r, :, :LANES], gap, tri)
         copies[2 * r].wait()
         copies[2 * r + 1].wait()
@@ -261,20 +272,26 @@
         reach_ref[r] = (query * jnp.exp(running + columns)).astype(BF16)
 
 
-def inside_blocks(toks, w, floor, early):
+def inside_blocks(toks, w, floor, early, tail):
     length = early.shape[1]
     block = (4, length, LANES)
     return pl.pallas_call(
         inside_kernel,
-        out_shape=(struct(block, F32), struct(block, BF16), struct(block, BF16), struct(block, BF16)),
-        in_specs=[*anywhere(9), *vmem(2)],
-        out_specs=tuple(vmem(4)),
+        out_shape=(
+            struct(block, F32),
+            struct(block, BF16),
+            struct(block, BF16),
+            struct(block, BF16),
+            struct((4, 8, LANES), F32),
+        ),
+        in_specs=[*anywhere(9), *vmem(3)],
+        out_specs=tuple(vmem(5)),
         scratch_shapes=[
             *token_scratch(toks[0], w.shape[0], 3 * LANES),
             pltpu.VMEM((length, 3 * LANES), BF16),
         ],
         name="inside",
-    )(*toks, w, floor, early)
+    )(*toks, w, floor, early, tail)
 
 
 def mix_kernel(
@@ -288,7 +305,7 @@
     sequence = (x + shift) % 4
     start = pl.multiple_of(x * LANES, LANES)
     taps = taps_ref[:, pl.ds(start, LANES)]
-    padded[0:8, :] = rim_ref[0, 8:, :].astype(F32)
+    padded[0:8, :] = rim_ref[0]
     padded[8:, :] = signal_ref[0].astype(F32)
     filtered = taps[0:1] * padded[6 : 6 + length, :]
     filtered = filtered + taps[1:2] * padded[7 : 7 + length, :]
@@ -316,7 +333,7 @@
             sequence_block(LANES, LANES),
             narrow,
             narrow,
-            sequence_block(16, LANES),
+            sequence_block(8, LANES),
             whole(*taps.shape),
             whole(1, LANES),
         ],
@@ -416,15 +433,14 @@
         out_far.append(ring(part, "tp", 1))
 
     floor = lax.dynamic_slice_in_dim(floor_gate, x * LANES, LANES, 0)[None]
-    states, projected = local_states(toks, early_w, floor)
+    states, projected, tail = local_states(toks, early_w, floor)
     arrived = exchanged(states, SP)
     before = exchanged(scan_blocks(arrived), SP)
     before = before.reshape(4, LANES, LANES)
 
-    inside, reach, gate, signal = inside_blocks(toks, late_w, floor, projected)
     count = 64
-    tail = signal[:, -16:, :]
-    rim = lax.ppermute(tail, SP, [(i, i + 1) for i in range(count - 1)])
+    tail = lax.ppermute(tail, SP, [(i, i + 1) for i in range(count - 1)])
+    inside, reach, gate, signal, rim = inside_blocks(toks, late_w, floor, projected, tail)
     mix = mix_blocks(inside, reach, before, gate, signal, rim, conv_taps, head_gain[None])
     mix = exchanged(mix, ("fs", "tp"))
     return out_rows(mix, out_near, out_far)[None]

time: 195 us -> 197 us (1.010)
  waiting for transfers between devices: 34.6 us -> 37.1 us
    ppermute x1, waiting for transfers between devices: 0.83 us -> 3.48 us  [layer(): tail = lax.ppermute(tail, SP, [(i, i + 1) for i in range(count - 1)])]
where the time goes in v6:
time: 197 us; the launch traced here: 194 us
  starting transfers between devices  100 us (51%)
  waiting for transfers between devices  37.1 us (19%)
  Pallas kernels  36.3 us (18%)
  between operations  13.8 us (7%)
  local copies, waits for them, and re-layouts  6.62 us (3%)
    all_to_all x5, starting transfers between devices, exchanged(): return lax.all_to_all(array, axis, split_axis=0, concat_axis=0, tiled=True)  51.2 us
    ppermute x14, starting transfers between devices, ring(): lax.ppermute(array, axis, [(i, (i + by) % count) for i in range(count)])  46.1 us
    ppermute x14, waiting for transfers between devices, ring(): lax.ppermute(array, axis, [(i, (i + by) % count) for i in range(count)])  18.8 us
    all_to_all x5, waiting for transfers between devices, exchanged(): return lax.all_to_all(array, axis, split_axis=0, concat_axis=0, tiled=True)  14.8 us
    pallas_call x1, Pallas kernels, inside_blocks(): pl.pallas_call(inside_kernel, out_shape=(struct(block, F32), struct(block...  11 us
    pallas_call x1, Pallas kernels, local_states(): pl.pallas_call(state_kernel, out_shape=(struct((64, 16, LANES), BF16), st...  8.54 us
    pallas_call x1, Pallas kernels, out_rows(): pl.pallas_call(out_kernel, out_shape=struct((rows, 4 * wide), BF16), in_s...  6.49 us
    pallas_call x1, Pallas kernels, mix_blocks(): pl.pallas_call(mix_kernel, out_shape=struct((8, length // 2, 2 * LANES),...  4.1 us
  transfers between devices with their start and end apart: 21, of which 5 were waited for; matrix products, arithmetic and copies ran while one was open for 2% of the time, Pallas kernels for 15%

profile of v6, /device:TPU:1, one launch (start us, length us, event | category | flops | bytes accessed | tf_op | source)
XLA Modules:
  0.0 194.2 jit_solution(17591612206060501035)
XLA Ops:
  8.1 7.6 %all-to-all-start = ((bf16[8,32,640]{2,1,0:T(8,128)(2,1)}), bf16[8,32,640]{2,1,0:T(8,128)(2,1)S(1)}, u32[]{:S(2)}, u32[]{:S(2)}) async-start(bf16[8,32,640]{2,1,0:T(8,128)(2,1)} %slab.1), calls=%async_computation | async-start | bytes 655360 | tf_op jit(solution)/shard_map/all_to_all | solution.py:393
  15.8 2.6 %norm.1.refs_0_ = bf16[200,2048]{1,0:T(8,128)(2,1)} custom-call(bf16[192,2048]{1,0:T(8,128)(2,1)} %bitcast.14, f32[1,2048]{1,0:T(1,128)} %bitcast.16, f32[4,384]{1,0:T(4,128)} %bitcast.17), custom_call_target="tpu_custom_call" | custom-call | tf_op jit(solution)/shard_map/norm/pallas_call | solution.py:58
  18.4 4.8 %collective-permute-start.5 = (bf16[200,2048]{1,0:T(8,128)(2,1)}, bf16[200,2048]{1,0:T(8,128)(2,1)S(1)}, u32[]{:S(2)}, u32[]{:S(2)}) collective-permute-start(bf16[200,2048]{1,0:T(8,128)(2,1)} %norm.1.refs_0_), channel_id=1, source_target_pairs={{0,4},{2,6},{4,0},{6,2},{1,5},{3,7},{5,1},{7,3},{8,12},{10,14},{12... | collective-permute-start | bytes 2457608 | tf_op jit(solution)/shard_map/ppermute | solution.py:389
  23.2 2.7 %all-to-all-done = bf16[8,32,640]{2,1,0:T(8,128)(2,1)S(1)} async-done(((bf16[8,32,640]{2,1,0:T(8,128)(2,1)}), bf16[8,32,640]{2,1,0:T(8,128)(2,1)S(1)}, u32[]{:S(2)}, u32[]{:S(2)}) %all-to-all-start) | async-done | bytes 327712 | tf_op jit(solution)/shard_map/all_to_all | solution.py:393
  27.0 12.0 %all-to-all-start.1 = ((bf16[8,256,256]{2,1,0:T(8,128)(2,1)}), bf16[8,256,256]{2,1,0:T(8,128)(2,1)S(1)}, u32[]{:S(2)}, u32[]{:S(2)}) async-start(bf16[8,256,256]{2,1,0:T(8,128)(2,1)} %get-tuple-element.16), calls=%async_computation.1 | async-start | bytes 2097152 | tf_op jit(solution)/shard_map/all_to_all | solution.py:393
  39.0 4.4 %collective-permute-start.3 = (bf16[200,2048]{1,0:T(8,128)(2,1)S(1)}, bf16[200,2048]{1,0:T(8,128)(2,1)}, u32[]{:S(2)}, u32[]{:S(2)}) collective-permute-start(bf16[200,2048]{1,0:T(8,128)(2,1)S(1)} %copy-done.1), channel_id=1, source_target_pairs={{0,6},{2,0},{4,2},{6,4},{1,7},{3,1},{5,3},{7,5},{8,14},{10,8},{12,... | collective-permute-start | bytes 2457608 | tf_op jit(solution)/shard_map/ppermute | solution.py:389
  45.4 4.6 %collective-permute-start = (bf16[200,2048]{1,0:T(8,128)(2,1)S(1)}, bf16[200,2048]{1,0:T(8,128)(2,1)S(1)}, u32[]{:S(2)}, u32[]{:S(2)}) collective-permute-start(bf16[200,2048]{1,0:T(8,128)(2,1)S(1)} %copy-done.1), channel_id=1, source_target_pairs={{0,1},{1,0},{2,3},{3,2},{4,5},{5,4},{6,7},{7,6},{8,9},{9,8},{10,11... | collective-permute-start | bytes 2457608 | tf_op jit(solution)/shard_map/ppermute | solution.py:389
  51.9 6.7 %collective-permute-done.3.refs_4_ = bf16[200,2048]{1,0:T(8,128)(2,1)} collective-permute-done((bf16[200,2048]{1,0:T(8,128)(2,1)S(1)}, bf16[200,2048]{1,0:T(8,128)(2,1)}, u32[]{:S(2)}, u32[]{:S(2)}) %collective-permute-start.3) | collective-permute-done | bytes 819232 | tf_op jit(solution)/shard_map/ppermute | solution.py:389
  58.6 5.2 %collective-permute-start.4 = (bf16[200,2048]{1,0:T(8,128)(2,1)}, bf16[200,2048]{1,0:T(8,128)(2,1)}, u32[]{:S(2)}, u32[]{:S(2)}) collective-permute-start(bf16[200,2048]{1,0:T(8,128)(2,1)} %collective-permute-done.3.refs_4_), channel_id=1, source_target_pairs={{0,1},{1,0},{2,3},{3,2},{4,5},{5,4},{6,7},{7,6},{8,9},{9,8},{10,11... | collective-permute-start | bytes 2457608 | tf_op jit(solution)/shard_map/ppermute | solution.py:389
  63.8 5.4 %collective-permute-start.2 = (bf16[200,2048]{1,0:T(8,128)(2,1)}, bf16[200,2048]{1,0:T(8,128)(2,1)}, u32[]{:S(2)}, u32[]{:S(2)}) collective-permute-start(bf16[200,2048]{1,0:T(8,128)(2,1)} %collective-permute-done.1.refs_2_), channel_id=1, source_target_pairs={{0,1},{1,0},{2,3},{3,2},{4,5},{5,4},{6,7},{7,6},{8,9},{9,8},{10,11... | collective-permute-start | bytes 2457608 | tf_op jit(solution)/shard_map/ppermute | solution.py:389
  74.0 3.1 %collective-permute-start.11 = (bf16[1024,512]{1,0:T(8,128)(2,1)}, bf16[1024,512]{1,0:T(8,128)(2,1)S(1)}, u32[]{:S(2)}, u32[]{:S(2)}) collective-permute-start(bf16[1024,512]{1,0:T(8,128)(2,1)} %constant_dynamic-update-slice_fusion.refs_0_), channel_id=1, source_target_pairs={{0,6},{2,0},{4,2},{6,4},{1,7},{3,1},{5,3},{7,5},{8,14},{10,8},{12,... | collective-permute-start | bytes 3145736 | tf_op jit(solution)/shard_map/ppermute | solution.py:389
  81.0 8.5 %states.1 = (bf16[64,16,128]{2,1,0:T(8,128)(2,1)}, bf16[4,384,256]{2,1,0:T(8,128)(2,1)}, bf16[32,2048]{1,0:T(8,128)(2,1)}) custom-call(bf16[200,2048]{1,0:T(8,128)(2,1)} %norm.1.refs_0_, bf16[200,2048]{1,0:T(8,128)(2,1)} %copy-done.4, bf16[200,2048]{1,0:T(8,128)(2,1)} %collective-permute-done.1.refs_2_, bf16[200,2048]{1,0:T(8,128)(2,1)} %collective-permute-done.2.refs_3_, ...), custom_call_target="tpu_custom_call" | custom-call | tf_op jit(solution)/shard_map/states/pallas_call | solution.py:193
  89.5 13.3 %all-to-all-start.2 = ((bf16[64,16,128]{2,1,0:T(8,128)(2,1)}), bf16[64,16,128]{2,1,0:T(8,128)(2,1)S(1)}, u32[]{:S(2)}, u32[]{:S(2)}) async-start(bf16[64,16,128]{2,1,0:T(8,128)(2,1)} %get-tuple-element.21), calls=%async_computation.2 | async-start | bytes 524288 | tf_op jit(solution)/shard_map/all_to_all | solution.py:393
  102.9 3.2 %collective-permute-start.8 = (bf16[1024,512]{1,0:T(8,128)(2,1)}, bf16[1024,512]{1,0:T(8,128)(2,1)S(1)}, u32[]{:S(2)}, u32[]{:S(2)}) collective-permute-start(bf16[1024,512]{1,0:T(8,128)(2,1)} %constant_dynamic-update-slice_fusion.refs_0_), channel_id=1, source_target_pairs={{0,1},{1,0},{2,3},{3,2},{4,5},{5,4},{6,7},{7,6},{8,9},{9,8},{10,11... | collective-permute-start | bytes 3145736 | tf_op jit(solution)/shard_map/ppermute | solution.py:389
  108.0 12.1 %collective-permute-done.11.refs_4_ = bf16[1024,512]{1,0:T(8,128)(2,1)S(1)} collective-permute-done((bf16[1024,512]{1,0:T(8,128)(2,1)}, bf16[1024,512]{1,0:T(8,128)(2,1)S(1)}, u32[]{:S(2)}, u32[]{:S(2)}) %collective-permute-start.11) | collective-permute-done | bytes 1048608 | tf_op jit(solution)/shard_map/ppermute | solution.py:389
  120.1 3.1 %collective-permute-start.12 = (bf16[1024,512]{1,0:T(8,128)(2,1)S(1)}, bf16[1024,512]{1,0:T(8,128)(2,1)}, u32[]{:S(2)}, u32[]{:S(2)}) collective-permute-start(bf16[1024,512]{1,0:T(8,128)(2,1)S(1)} %collective-permute-done.11.refs_4_), channel_id=1, source_target_pairs={{0,1},{1,0},{2,3},{3,2},{4,5},{5,4},{6,7},{7,6},{8,9},{9,8},{10,11... | collective-permute-start | bytes 3145736 | tf_op jit(solution)/shard_map/ppermute | solution.py:389
  126.6 13.2 %all-to-all-start.3 = ((bf16[64,8,128]{2,1,0:T(8,128)(2,1)}), bf16[64,8,128]{2,1,0:T(8,128)(2,1)S(1)}, u32[]{:S(2)}, u32[]{:S(2)}) async-start(bf16[64,8,128]{2,1,0:T(8,128)(2,1)} %scan.1), calls=%async_computation.3 | async-start | bytes 262144 | tf_op jit(solution)/shard_map/all_to_all | solution.py:393
  139.7 3.1 %collective-permute-start.7 = (bf16[32,2048]{1,0:T(8,128)(2,1)}, bf16[32,2048]{1,0:T(8,128)(2,1)S(1)}, u32[]{:S(2)}, u32[]{:S(2)}) collective-permute-start(bf16[32,2048]{1,0:T(8,128)(2,1)} %get-tuple-element.18), channel_id=1, source_target_pairs={{0,8},{8,16},{16,24},{24,32},{32,40},{40,48},{48,56},{56,64},{64,7... | collective-permute-start | bytes 393224 | tf_op jit(solution)/shard_map/ppermute | solution.py:442
  142.8 3.5 %collective-permute-done.7.refs_11_ = bf16[32,2048]{1,0:T(8,128)(2,1)S(1)} collective-permute-done((bf16[32,2048]{1,0:T(8,128)(2,1)}, bf16[32,2048]{1,0:T(8,128)(2,1)S(1)}, u32[]{:S(2)}, u32[]{:S(2)}) %collective-permute-start.7) | collective-permute-done | bytes 131104 | tf_op jit(solution)/shard_map/ppermute | solution.py:442
  147.0 11.0 %inside.1 = (f32[4,384,128]{2,1,0:T(8,128)}, bf16[4,384,128]{2,1,0:T(8,128)(2,1)}, bf16[4,384,128]{2,1,0:T(8,128)(2,1)}, bf16[4,384,128]{2,1,0:T(8,128)(2,1)}, f32[4,8,128]{2,1,0:T(8,128)}) custom-call(bf16[200,2048]{1,0:T(8,128)(2,1)} %norm.1.refs_0_, bf16[200,2048]{1,0:T(8,128)(2,1)} %copy-done.4, bf16[200,2048]{1,0:T(8,128)(2,1)} %collective-permute-done.1.refs_2_, ...), custom_call_target="tpu_custom_call" | custom-call | tf_op jit(solution)/shard_map/inside/pallas_call | solution.py:278
  158.6 4.1 %mix.1 = bf16[8,192,256]{2,1,0:T(8,128)(2,1)} custom-call(f32[4,384,128]{2,1,0:T(8,128)} %get-tuple-element.19.inside_ref, bf16[4,384,128]{2,1,0:T(8,128)(2,1)} %get-tuple-element.20.reach_ref, bf16[4,128,128]{2,1,0:T(8,128)(2,1)} %bitcast.15, bf16[4,384,128]{2,1,0:T(8,128)(2,1)} %get-tuple-element.22.gate_ref, ...), custom_call_target="tpu_custom_call" | custom-call | tf_op jit(solution)/shard_map/mix/pallas_call | solution.py:326
  162.7 5.1 %all-to-all-start.4 = ((bf16[8,192,256]{2,1,0:T(8,128)(2,1)}), bf16[8,192,256]{2,1,0:T(8,128)(2,1)S(1)}, u32[]{:S(2)}, u32[]{:S(2)}) async-start(bf16[8,192,256]{2,1,0:T(8,128)(2,1)} %mix.1), calls=%async_computation.4 | async-start | bytes 1572864 | tf_op jit(solution)/shard_map/all_to_all | solution.py:393
  167.9 12.1 %all-to-all-done.4.mix_ref = bf16[8,192,256]{2,1,0:T(8,128)(2,1)S(1)} async-done(((bf16[8,192,256]{2,1,0:T(8,128)(2,1)}), bf16[8,192,256]{2,1,0:T(8,128)(2,1)S(1)}, u32[]{:S(2)}, u32[]{:S(2)}) %all-to-all-start.4) | async-done | bytes 786464 | tf_op jit(solution)/shard_map/all_to_all | solution.py:393
  180.9 6.5 %out.1 = bf16[192,2048]{1,0:T(8,128)(2,1)} custom-call(bf16[8,192,256]{2,1,0:T(8,128)(2,1)} %copy-done.6, bf16[1024,512]{1,0:T(8,128)(2,1)} %constant_dynamic-update-slice_fusion.refs_0_, bf16[1024,512]{1,0:T(8,128)(2,1)} %copy-done.8, bf16[1024,512]{1,0:T(8,128)(2,1)} %collective-permute-done.9.refs_2_, bf16[1024,512]{1,0:T(8,128)(2,1)} %collective-permute-done.10.refs_3_, ...), custom_call_target="tpu_custom_call" | custom-call | tf_op jit(solution)/shard_map/out/pallas_call | solution.py:377
  (54 shorter events, 22.6 us)
Async XLA Ops:
  6.5 72.8 %copy-start = (f32[512]{0:T(512)S(1)}, f32[512]{0:T(512)}, u32[]{:S(2)}) copy-start(f32[512]{0:T(512)} %param.21) | copy-start | bytes 6148
  8.1 17.8 %all-to-all-start = ((bf16[8,32,640]{2,1,0:T(8,128)(2,1)}), bf16[8,32,640]{2,1,0:T(8,128)(2,1)S(1)}, u32[]{:S(2)}, u32[]{:S(2)}) async-start(bf16[8,32,640]{2,1,0:T(8,128)(2,1)} %slab.1), calls=%async_computation | async-start | bytes 655360 | tf_op jit(solution)/shard_map/all_to_all | solution.py:393
  15.8 130.6 %all-gather.2.cloned.1.call-start = ((), (), s32[]{:S(2)}) async-start(), calls=%async_computation.5 | async-start | bytes 1769472 | tf_op jit(solution)/shard_map/all_gather | solution.py:416
  18.4 50.8 %copy-start.10 = (bf16[512,512]{1,0:T(8,128)(2,1)S(1)}, bf16[512,512]{1,0:T(8,128)(2,1)}, u32[]{:S(2)}) copy-start(bf16[512,512]{1,0:T(8,128)(2,1)} %param.24) | copy-start | bytes 1572868
  18.4 31.6 %collective-permute-start.5 = (bf16[200,2048]{1,0:T(8,128)(2,1)}, bf16[200,2048]{1,0:T(8,128)(2,1)S(1)}, u32[]{:S(2)}, u32[]{:S(2)}) collective-permute-start(bf16[200,2048]{1,0:T(8,128)(2,1)} %norm.1.refs_0_), channel_id=1, source_target_pairs={{0,4},{2,6},{4,0},{6,2},{1,5},{3,7},{5,1},{7,3},{8,12},{10,14},{12... | collective-permute-start | bytes 2457608 | tf_op jit(solution)/shard_map/ppermute | solution.py:389
  27.0 53.0 %all-to-all-start.1 = ((bf16[8,256,256]{2,1,0:T(8,128)(2,1)}), bf16[8,256,256]{2,1,0:T(8,128)(2,1)S(1)}, u32[]{:S(2)}, u32[]{:S(2)}) async-start(bf16[8,256,256]{2,1,0:T(8,128)(2,1)} %get-tuple-element.16), calls=%async_computation.1 | async-start | bytes 2097152 | tf_op jit(solution)/shard_map/all_to_all | solution.py:393
  39.0 19.6 %collective-permute-start.3 = (bf16[200,2048]{1,0:T(8,128)(2,1)S(1)}, bf16[200,2048]{1,0:T(8,128)(2,1)}, u32[]{:S(2)}, u32[]{:S(2)}) collective-permute-start(bf16[200,2048]{1,0:T(8,128)(2,1)S(1)} %copy-done.1), channel_id=1, source_target_pairs={{0,6},{2,0},{4,2},{6,4},{1,7},{3,1},{5,3},{7,5},{8,14},{10,8},{12,... | collective-permute-start | bytes 2457608 | tf_op jit(solution)/shard_map/ppermute | solution.py:389
  43.4 20.3 %collective-permute-start.1 = (bf16[200,2048]{1,0:T(8,128)(2,1)S(1)}, bf16[200,2048]{1,0:T(8,128)(2,1)}, u32[]{:S(2)}, u32[]{:S(2)}) collective-permute-start(bf16[200,2048]{1,0:T(8,128)(2,1)S(1)} %copy-done.1), channel_id=1, source_target_pairs={{0,2},{2,4},{4,6},{6,0},{1,3},{3,5},{5,7},{7,1},{8,10},{10,12},{12... | collective-permute-start | bytes 2457608 | tf_op jit(solution)/shard_map/ppermute | solution.py:389
  45.4 28.6 %collective-permute-start = (bf16[200,2048]{1,0:T(8,128)(2,1)S(1)}, bf16[200,2048]{1,0:T(8,128)(2,1)S(1)}, u32[]{:S(2)}, u32[]{:S(2)}) collective-permute-start(bf16[200,2048]{1,0:T(8,128)(2,1)S(1)} %copy-done.1), channel_id=1, source_target_pairs={{0,1},{1,0},{2,3},{3,2},{4,5},{5,4},{6,7},{7,6},{8,9},{9,8},{10,11... | collective-permute-start | bytes 2457608 | tf_op jit(solution)/shard_map/ppermute | solution.py:389
  50.0 27.1 %collective-permute-start.6 = (bf16[200,2048]{1,0:T(8,128)(2,1)S(1)}, bf16[200,2048]{1,0:T(8,128)(2,1)S(1)}, u32[]{:S(2)}, u32[]{:S(2)}) collective-permute-start(bf16[200,2048]{1,0:T(8,128)(2,1)S(1)} %collective-permute-done.5.refs_6_), channel_id=1, source_target_pairs={{0,1},{1,0},{2,3},{3,2},{4,5},{5,4},{6,7},{7,6},{8,9},{9,8},{10,11... | collective-permute-start | bytes 2457608 | tf_op jit(solution)/shard_map/ppermute | solution.py:389
  58.6 21.4 %collective-permute-start.4 = (bf16[200,2048]{1,0:T(8,128)(2,1)}, bf16[200,2048]{1,0:T(8,128)(2,1)}, u32[]{:S(2)}, u32[]{:S(2)}) collective-permute-start(bf16[200,2048]{1,0:T(8,128)(2,1)} %collective-permute-done.3.refs_4_), channel_id=1, source_target_pairs={{0,1},{1,0},{2,3},{3,2},{4,5},{5,4},{6,7},{7,6},{8,9},{9,8},{10,11... | collective-permute-start | bytes 2457608 | tf_op jit(solution)/shard_map/ppermute | solution.py:389
  63.8 16.2 %collective-permute-start.2 = (bf16[200,2048]{1,0:T(8,128)(2,1)}, bf16[200,2048]{1,0:T(8,128)(2,1)}, u32[]{:S(2)}, u32[]{:S(2)}) collective-permute-start(bf16[200,2048]{1,0:T(8,128)(2,1)} %collective-permute-done.1.refs_2_), channel_id=1, source_target_pairs={{0,1},{1,0},{2,3},{3,2},{4,5},{5,4},{6,7},{7,6},{8,9},{9,8},{10,11... | collective-permute-start | bytes 2457608 | tf_op jit(solution)/shard_map/ppermute | solution.py:389
  72.0 34.1 %collective-permute-start.13 = (bf16[1024,512]{1,0:T(8,128)(2,1)}, bf16[1024,512]{1,0:T(8,128)(2,1)}, u32[]{:S(2)}, u32[]{:S(2)}) collective-permute-start(bf16[1024,512]{1,0:T(8,128)(2,1)} %constant_dynamic-update-slice_fusion.refs_0_), channel_id=1, source_target_pairs={{0,4},{2,6},{4,0},{6,2},{1,5},{3,7},{5,1},{7,3},{8,12},{10,14},{12... | collective-permute-start | bytes 3145736 | tf_op jit(solution)/shard_map/ppermute | solution.py:389
  74.0 46.1 %collective-permute-start.11 = (bf16[1024,512]{1,0:T(8,128)(2,1)}, bf16[1024,512]{1,0:T(8,128)(2,1)S(1)}, u32[]{:S(2)}, u32[]{:S(2)}) collective-permute-start(bf16[1024,512]{1,0:T(8,128)(2,1)} %constant_dynamic-update-slice_fusion.refs_0_), channel_id=1, source_target_pairs={{0,6},{2,0},{4,2},{6,4},{1,7},{3,1},{5,3},{7,5},{8,14},{10,8},{12,... | collective-permute-start | bytes 3145736 | tf_op jit(solution)/shard_map/ppermute | solution.py:389
  77.1 46.2 %collective-permute-start.9 = (bf16[1024,512]{1,0:T(8,128)(2,1)}, bf16[1024,512]{1,0:T(8,128)(2,1)}, u32[]{:S(2)}, u32[]{:S(2)}) collective-permute-start(bf16[1024,512]{1,0:T(8,128)(2,1)} %constant_dynamic-update-slice_fusion.refs_0_), channel_id=1, source_target_pairs={{0,2},{2,4},{4,6},{6,0},{1,3},{3,5},{5,7},{7,1},{8,10},{10,12},{12... | collective-permute-start | bytes 3145736 | tf_op jit(solution)/shard_map/ppermute | solution.py:389
  89.5 36.2 %all-to-all-start.2 = ((bf16[64,16,128]{2,1,0:T(8,128)(2,1)}), bf16[64,16,128]{2,1,0:T(8,128)(2,1)S(1)}, u32[]{:S(2)}, u32[]{:S(2)}) async-start(bf16[64,16,128]{2,1,0:T(8,128)(2,1)} %get-tuple-element.21), calls=%async_computation.2 | async-start | bytes 524288 | tf_op jit(solution)/shard_map/all_to_all | solution.py:393
  102.9 65.0 %collective-permute-start.8 = (bf16[1024,512]{1,0:T(8,128)(2,1)}, bf16[1024,512]{1,0:T(8,128)(2,1)S(1)}, u32[]{:S(2)}, u32[]{:S(2)}) collective-permute-start(bf16[1024,512]{1,0:T(8,128)(2,1)} %constant_dynamic-update-slice_fusion.refs_0_), channel_id=1, source_target_pairs={{0,1},{1,0},{2,3},{3,2},{4,5},{5,4},{6,7},{7,6},{8,9},{9,8},{10,11... | collective-permute-start | bytes 3145736 | tf_op jit(solution)/shard_map/ppermute | solution.py:389
  106.1 61.7 %collective-permute-start.14 = (bf16[1024,512]{1,0:T(8,128)(2,1)}, bf16[1024,512]{1,0:T(8,128)(2,1)}, u32[]{:S(2)}, u32[]{:S(2)}) collective-permute-start(bf16[1024,512]{1,0:T(8,128)(2,1)} %collective-permute-done.13.refs_6_), channel_id=1, source_target_pairs={{0,1},{1,0},{2,3},{3,2},{4,5},{5,4},{6,7},{7,6},{8,9},{9,8},{10,11... | collective-permute-start | bytes 3145736 | tf_op jit(solution)/shard_map/ppermute | solution.py:389
  120.1 37.9 %copy-start.7 = (bf16[1024,512]{1,0:T(8,128)(2,1)}, bf16[1024,512]{1,0:T(8,128)(2,1)S(1)}, u32[]{:S(2)}) copy-start(bf16[1024,512]{1,0:T(8,128)(2,1)S(1)} %collective-permute-done.11.refs_4_) | copy-start | bytes 3145732
  120.1 47.7 %collective-permute-start.12 = (bf16[1024,512]{1,0:T(8,128)(2,1)S(1)}, bf16[1024,512]{1,0:T(8,128)(2,1)}, u32[]{:S(2)}, u32[]{:S(2)}) collective-permute-start(bf16[1024,512]{1,0:T(8,128)(2,1)S(1)} %collective-permute-done.11.refs_4_), channel_id=1, source_target_pairs={{0,1},{1,0},{2,3},{3,2},{4,5},{5,4},{6,7},{7,6},{8,9},{9,8},{10,11... | collective-permute-start | bytes 3145736 | tf_op jit(solution)/shard_map/ppermute | solution.py:389
  123.3 44.6 %collective-permute-start.10 = (bf16[1024,512]{1,0:T(8,128)(2,1)}, bf16[1024,512]{1,0:T(8,128)(2,1)}, u32[]{:S(2)}, u32[]{:S(2)}) collective-permute-start(bf16[1024,512]{1,0:T(8,128)(2,1)} %collective-permute-done.9.refs_2_), channel_id=1, source_target_pairs={{0,1},{1,0},{2,3},{3,2},{4,5},{5,4},{6,7},{7,6},{8,9},{9,8},{10,11... | collective-permute-start | bytes 3145736 | tf_op jit(solution)/shard_map/ppermute | solution.py:389
  126.6 31.4 %all-to-all-start.3 = ((bf16[64,8,128]{2,1,0:T(8,128)(2,1)}), bf16[64,8,128]{2,1,0:T(8,128)(2,1)S(1)}, u32[]{:S(2)}, u32[]{:S(2)}) async-start(bf16[64,8,128]{2,1,0:T(8,128)(2,1)} %scan.1), calls=%async_computation.3 | async-start | bytes 262144 | tf_op jit(solution)/shard_map/all_to_all | solution.py:393
  139.7 6.6 %collective-permute-start.7 = (bf16[32,2048]{1,0:T(8,128)(2,1)}, bf16[32,2048]{1,0:T(8,128)(2,1)S(1)}, u32[]{:S(2)}, u32[]{:S(2)}) collective-permute-start(bf16[32,2048]{1,0:T(8,128)(2,1)} %get-tuple-element.18), channel_id=1, source_target_pairs={{0,8},{8,16},{16,24},{24,32},{32,40},{40,48},{48,56},{56,64},{64,7... | collective-permute-start | bytes 393224 | tf_op jit(solution)/shard_map/ppermute | solution.py:442
  162.7 17.2 %all-to-all-start.4 = ((bf16[8,192,256]{2,1,0:T(8,128)(2,1)}), bf16[8,192,256]{2,1,0:T(8,128)(2,1)S(1)}, u32[]{:S(2)}, u32[]{:S(2)}) async-start(bf16[8,192,256]{2,1,0:T(8,128)(2,1)} %mix.1), calls=%async_computation.4 | async-start | bytes 1572864 | tf_op jit(solution)/shard_map/all_to_all | solution.py:393
  (9 other events, 71.3 us)
Sparse Core Ops, SparseCore 0:
  27.1 55.6 all-gather.1

commit v7 on v6

--- a/solution.py
+++ b/solution.py
@@ -233,9 +233,32 @@
     )(states)
 
 
+def prepare_kernel(floor_ref, early_ref, run_ref, behind_ref):
+    length = early_ref.shape[1]
+    tri = lower_triangle(length).astype(F32).astype(BF16)
+    keys, running = gates(early_ref[0, :, :LANES], 1.0 - floor_ref[...], tri)
+    middle = 0.5 * running[length - 1 :, :]
+    behind_ref[0] = (keys * jnp.exp(middle - running)).astype(BF16)
+    run_ref[0] = running
+
+
+def prepared(floor, early):
+    length = early.shape[1]
+    block = (4, length, LANES)
+    narrow = sequence_block(length, LANES)
+    return pl.pallas_call(
+        prepare_kernel,
+        out_shape=(struct(block, F32), struct(block, BF16)),
+        grid=(4,),
+        in_specs=[whole(1, LANES), sequence_block(length, 2 * LANES)],
+        out_specs=(narrow, narrow),
+        name="prepare",
+    )(floor, early)
+
+
 def inside_kernel(*refs):
     tok_refs, rest = refs[:8], refs[8:]
-    w_ref, floor_ref, early_ref, tail_ref, *rest = rest
+    w_ref, early_ref, run_ref, behind_ref, tail_ref, *rest = rest
     inside_ref, reach_ref, gate_ref, signal_ref, rim_ref, toks, sems, weights, w_sem, raw = rest
     w_copy = pltpu.make_async_copy(w_ref, weights, w_sem)
     copies = fetches(tok_refs, toks, sems)
@@ -243,14 +266,12 @@
         copy.start()
     length = early_ref.shape[1]
     causal = lower_triangle(length)
-    tri = causal.astype(F32).astype(BF16)
-    gap = 1.0 - floor_ref[...]
     w_copy.wait()
     w = weights[...]
     rim = dot(tail_ref[...], weights[:, 2 * LANES :]).astype(BF16).astype(F32)
     for r in range(4):
         rim_ref[r] = rim[8 * r : 8 * r + 8]
-        keys, running = gates(early_ref[r, :, :LANES], gap, tri)
+        running = run_ref[r]
         copies[2 * r].wait()
         copies[2 * r + 1].wait()
         if r < 2:
@@ -263,16 +284,15 @@
         query = logits * jax.nn.sigmoid(logits)
         middle = 0.5 * running[length - 1 :, :]
         ahead = (query * jnp.exp(running - middle)).astype(BF16)
-        behind = (keys * jnp.exp(middle - running)).astype(BF16)
         leaks = leak_row(toks, r, length)
         columns = jnp.broadcast_to(leaks, (LANES, length)).T
         fade = jnp.exp(jnp.where(causal, columns[:, :1] - leaks, -jnp.inf))
-        scores = dot(ahead, behind, ((1,), (1,))) * fade
+        scores = dot(ahead, behind_ref[r], ((1,), (1,))) * fade
         inside_ref[r] = dot(scores.astype(BF16), early_ref[r, :, LANES:])
         reach_ref[r] = (query * jnp.exp(running + columns)).astype(BF16)
 
 
-def inside_blocks(toks, w, floor, early, tail):
+def inside_blocks(toks, w, early, running, behind, tail):
     length = early.shape[1]
     block = (4, length, LANES)
     return pl.pallas_call(
@@ -284,14 +304,14 @@
             struct(block, BF16),
             struct((4, 8, LANES), F32),
         ),
-        in_specs=[*anywhere(9), *vmem(3)],
+        in_specs=[*anywhere(9), *vmem(4)],
         out_specs=tuple(vmem(5)),
         scratch_shapes=[
             *token_scratch(toks[0], w.shape[0], 3 * LANES),
             pltpu.VMEM((length, 3 * LANES), BF16),
         ],
         name="inside",
-    )(*toks, w, floor, early, tail)
+    )(*toks, w, early, running, behind, tail)
 
 
 def mix_kernel(
@@ -440,7 +460,8 @@
 
     count = 64
     tail = lax.ppermute(tail, SP, [(i, i + 1) for i in range(count - 1)])
-    inside, reach, gate, signal, rim = inside_blocks(toks, late_w, floor, projected, tail)
+    running, behind = prepared(floor, projected)
+    inside, reach, gate, signal, rim = inside_blocks(toks, late_w, projected, running, behind, tail)
     mix = mix_blocks(inside, reach, before, gate, signal, rim, conv_taps, head_gain[None])
     mix = exchanged(mix, ("fs", "tp"))
     return out_rows(mix, out_near, out_far)[None]

time: 197 us -> 210 us (1.066)
  starting transfers between devices: 100 us -> 107 us
  waiting for transfers between devices: 37.1 us -> 41 us
  Pallas kernels: 36.3 us -> 39.2 us
    ppermute x14, starting transfers between devices: 46.1 us -> 61.6 us  [ring(): lax.ppermute(array, axis, [(i, (i + by) % count) for i in range(count)])]
    all_to_all x5, starting transfers between devices: 51.2 us -> 42.6 us  [exchanged(): return lax.all_to_all(array, axis, split_axis=0, concat_axis=0, tiled=True)]
    ppermute x14, waiting for transfers between devices: 18.8 us -> 24.6 us  [ring(): lax.ppermute(array, axis, [(i, (i + by) % count) for i in range(count)])]
    pallas_call x0 -> x1, Pallas kernels: none -> 4 us  [prepared(): pl.pallas_call(prepare_kernel, out_shape=(struct(block, F32), struct(bloc...]
    ppermute x1, waiting for transfers between devices: 3.48 us -> 0.01 us  [layer(): tail = lax.ppermute(tail, SP, [(i, i + 1) for i in range(count - 1)])]
  transfers between devices with their start and end apart: 21 -> 21, of which waited for: 5 -> 4; matrix products, arithmetic and copies ran while one was open for 2% -> 2% of each run, Pallas kernels for 15% -> 15%
where the time goes in v7:
time: 210 us; the launch traced here: 208 us
  starting transfers between devices  107 us (51%)
  waiting for transfers between devices  41 us (20%)
  Pallas kernels  39.2 us (19%)
  between operations  13.8 us (7%)
  local copies, waits for them, and re-layouts  6.46 us (3%)
    ppermute x14, starting transfers between devices, ring(): lax.ppermute(array, axis, [(i, (i + by) % count) for i in range(count)])  61.6 us
    all_to_all x5, starting transfers between devices, exchanged(): return lax.all_to_all(array, axis, split_axis=0, concat_axis=0, tiled=True)  42.6 us
    ppermute x14, waiting for transfers between devices, ring(): lax.ppermute(array, axis, [(i, (i + by) % count) for i in range(count)])  24.6 us
    all_to_all x5, waiting for transfers between devices, exchanged(): return lax.all_to_all(array, axis, split_axis=0, concat_axis=0, tiled=True)  16.3 us
    pallas_call x1, Pallas kernels, inside_blocks(): pl.pallas_call(inside_kernel, out_shape=(struct(block, F32), struct(block...  9.99 us
    pallas_call x1, Pallas kernels, local_states(): pl.pallas_call(state_kernel, out_shape=(struct((64, 16, LANES), BF16), st...  8.46 us
    pallas_call x1, Pallas kernels, out_rows(): pl.pallas_call(out_kernel, out_shape=struct((rows, 4 * wide), BF16), in_s...  6.49 us
  transfers between devices with their start and end apart: 21, of which 4 were waited for; matrix products, arithmetic and copies ran while one was open for 2% of the time, Pallas kernels for 15%

profile of v7, /device:TPU:1, one launch (start us, length us, event | category | flops | bytes accessed | tf_op | source)
XLA Modules:
  0.0 207.8 jit_solution(7620067347248275184)
XLA Ops:
  8.1 7.6 %all-to-all-start = ((bf16[8,32,640]{2,1,0:T(8,128)(2,1)}), bf16[8,32,640]{2,1,0:T(8,128)(2,1)S(1)}, u32[]{:S(2)}, u32[]{:S(2)}) async-start(bf16[8,32,640]{2,1,0:T(8,128)(2,1)} %slab.1), calls=%async_computation | async-start | bytes 655360 | tf_op jit(solution)/shard_map/all_to_all | solution.py:413
  15.8 2.6 %norm.1.refs_0_ = bf16[200,2048]{1,0:T(8,128)(2,1)} custom-call(bf16[192,2048]{1,0:T(8,128)(2,1)} %bitcast.14, f32[1,2048]{1,0:T(1,128)} %bitcast.16, f32[4,384]{1,0:T(4,128)} %bitcast.17), custom_call_target="tpu_custom_call" | custom-call | tf_op jit(solution)/shard_map/norm/pallas_call | solution.py:58
  18.4 3.2 %collective-permute-start.1 = (bf16[200,2048]{1,0:T(8,128)(2,1)}, bf16[200,2048]{1,0:T(8,128)(2,1)S(1)}, u32[]{:S(2)}, u32[]{:S(2)}) collective-permute-start(bf16[200,2048]{1,0:T(8,128)(2,1)} %norm.1.refs_0_), channel_id=1, source_target_pairs={{0,2},{2,4},{4,6},{6,0},{1,3},{3,5},{5,7},{7,1},{8,10},{10,12},{12... | collective-permute-start | bytes 2457608 | tf_op jit(solution)/shard_map/ppermute | solution.py:409
  21.7 4.2 %all-to-all-done = bf16[8,32,640]{2,1,0:T(8,128)(2,1)S(1)} async-done(((bf16[8,32,640]{2,1,0:T(8,128)(2,1)}), bf16[8,32,640]{2,1,0:T(8,128)(2,1)S(1)}, u32[]{:S(2)}, u32[]{:S(2)}) %all-to-all-start) | async-done | bytes 327712 | tf_op jit(solution)/shard_map/all_to_all | solution.py:413
  27.0 12.0 %all-to-all-start.1 = ((bf16[8,256,256]{2,1,0:T(8,128)(2,1)}), bf16[8,256,256]{2,1,0:T(8,128)(2,1)S(1)}, u32[]{:S(2)}, u32[]{:S(2)}) async-start(bf16[8,256,256]{2,1,0:T(8,128)(2,1)} %get-tuple-element.18), calls=%async_computation.1 | async-start | bytes 2097152 | tf_op jit(solution)/shard_map/all_to_all | solution.py:413
  39.1 4.4 %collective-permute-start.3 = (bf16[200,2048]{1,0:T(8,128)(2,1)S(1)}, bf16[200,2048]{1,0:T(8,128)(2,1)}, u32[]{:S(2)}, u32[]{:S(2)}) collective-permute-start(bf16[200,2048]{1,0:T(8,128)(2,1)S(1)} %copy-done.1), channel_id=1, source_target_pairs={{0,6},{2,0},{4,2},{6,4},{1,7},{3,1},{5,3},{7,5},{8,14},{10,8},{12,... | collective-permute-start | bytes 2457608 | tf_op jit(solution)/shard_map/ppermute | solution.py:409
  45.9 4.9 %collective-permute-start = (bf16[200,2048]{1,0:T(8,128)(2,1)S(1)}, bf16[200,2048]{1,0:T(8,128)(2,1)S(1)}, u32[]{:S(2)}, u32[]{:S(2)}) collective-permute-start(bf16[200,2048]{1,0:T(8,128)(2,1)S(1)} %copy-done.1), channel_id=1, source_target_pairs={{0,1},{1,0},{2,3},{3,2},{4,5},{5,4},{6,7},{7,6},{8,9},{9,8},{10,11... | collective-permute-start | bytes 2457608 | tf_op jit(solution)/shard_map/ppermute | solution.py:409
  52.7 6.7 %collective-permute-done.3.refs_4_ = bf16[200,2048]{1,0:T(8,128)(2,1)} collective-permute-done((bf16[200,2048]{1,0:T(8,128)(2,1)S(1)}, bf16[200,2048]{1,0:T(8,128)(2,1)}, u32[]{:S(2)}, u32[]{:S(2)}) %collective-permute-start.3) | collective-permute-done | bytes 819232 | tf_op jit(solution)/shard_map/ppermute | solution.py:409
  59.4 22.0 %collective-permute-start.4 = (bf16[200,2048]{1,0:T(8,128)(2,1)}, bf16[200,2048]{1,0:T(8,128)(2,1)}, u32[]{:S(2)}, u32[]{:S(2)}) collective-permute-start(bf16[200,2048]{1,0:T(8,128)(2,1)} %collective-permute-done.3.refs_4_), channel_id=1, source_target_pairs={{0,1},{1,0},{2,3},{3,2},{4,5},{5,4},{6,7},{7,6},{8,9},{9,8},{10,11... | collective-permute-start | bytes 2457608 | tf_op jit(solution)/shard_map/ppermute | solution.py:409
  88.0 5.4 %collective-permute-start.11 = (bf16[1024,512]{1,0:T(8,128)(2,1)}, bf16[1024,512]{1,0:T(8,128)(2,1)S(1)}, u32[]{:S(2)}, u32[]{:S(2)}) collective-permute-start(bf16[1024,512]{1,0:T(8,128)(2,1)} %constant_dynamic-update-slice_fusion.refs_0_), channel_id=1, source_target_pairs={{0,6},{2,0},{4,2},{6,4},{1,7},{3,1},{5,3},{7,5},{8,14},{10,8},{12,... | collective-permute-start | bytes 3145736 | tf_op jit(solution)/shard_map/ppermute | solution.py:409
  93.5 3.1 %collective-permute-start.13 = (bf16[1024,512]{1,0:T(8,128)(2,1)}, bf16[1024,512]{1,0:T(8,128)(2,1)}, u32[]{:S(2)}, u32[]{:S(2)}) collective-permute-start(bf16[1024,512]{1,0:T(8,128)(2,1)} %constant_dynamic-update-slice_fusion.refs_0_), channel_id=1, source_target_pairs={{0,4},{2,6},{4,0},{6,2},{1,5},{3,7},{5,1},{7,3},{8,12},{10,14},{12... | collective-permute-start | bytes 3145736 | tf_op jit(solution)/shard_map/ppermute | solution.py:409
  98.2 8.5 %states.1 = (bf16[64,16,128]{2,1,0:T(8,128)(2,1)}, bf16[4,384,256]{2,1,0:T(8,128)(2,1)}, bf16[32,2048]{1,0:T(8,128)(2,1)}) custom-call(bf16[200,2048]{1,0:T(8,128)(2,1)} %norm.1.refs_0_, bf16[200,2048]{1,0:T(8,128)(2,1)} %copy-done.4, bf16[200,2048]{1,0:T(8,128)(2,1)} %copy-done.3, bf16[200,2048]{1,0:T(8,128)(2,1)} %copy-done.5, ...), custom_call_target="tpu_custom_call" | custom-call | tf_op jit(solution)/shard_map/states/pallas_call | solution.py:193
  106.6 8.4 %all-to-all-start.2 = ((bf16[64,16,128]{2,1,0:T(8,128)(2,1)}), bf16[64,16,128]{2,1,0:T(8,128)(2,1)S(1)}, u32[]{:S(2)}, u32[]{:S(2)}) async-start(bf16[64,16,128]{2,1,0:T(8,128)(2,1)} %get-tuple-element.25), calls=%async_computation.2 | async-start | bytes 524288 | tf_op jit(solution)/shard_map/all_to_all | solution.py:413
  115.0 3.2 %collective-permute-start.8 = (bf16[1024,512]{1,0:T(8,128)(2,1)}, bf16[1024,512]{1,0:T(8,128)(2,1)S(1)}, u32[]{:S(2)}, u32[]{:S(2)}) collective-permute-start(bf16[1024,512]{1,0:T(8,128)(2,1)} %constant_dynamic-update-slice_fusion.refs_0_), channel_id=1, source_target_pairs={{0,1},{1,0},{2,3},{3,2},{4,5},{5,4},{6,7},{7,6},{8,9},{9,8},{10,11... | collective-permute-start | bytes 3145736 | tf_op jit(solution)/shard_map/ppermute | solution.py:409
  120.2 17.9 %collective-permute-done.11.refs_4_ = bf16[1024,512]{1,0:T(8,128)(2,1)S(1)} collective-permute-done((bf16[1024,512]{1,0:T(8,128)(2,1)}, bf16[1024,512]{1,0:T(8,128)(2,1)S(1)}, u32[]{:S(2)}, u32[]{:S(2)}) %collective-permute-start.11) | collective-permute-done | bytes 1048608 | tf_op jit(solution)/shard_map/ppermute | solution.py:409
  138.1 3.4 %collective-permute-start.12 = (bf16[1024,512]{1,0:T(8,128)(2,1)S(1)}, bf16[1024,512]{1,0:T(8,128)(2,1)}, u32[]{:S(2)}, u32[]{:S(2)}) collective-permute-start(bf16[1024,512]{1,0:T(8,128)(2,1)S(1)} %collective-permute-done.11.refs_4_), channel_id=1, source_target_pairs={{0,1},{1,0},{2,3},{3,2},{4,5},{5,4},{6,7},{7,6},{8,9},{9,8},{10,11... | collective-permute-start | bytes 3145736 | tf_op jit(solution)/shard_map/ppermute | solution.py:409
  144.3 8.4 %all-to-all-start.3 = ((bf16[64,8,128]{2,1,0:T(8,128)(2,1)}), bf16[64,8,128]{2,1,0:T(8,128)(2,1)S(1)}, u32[]{:S(2)}, u32[]{:S(2)}) async-start(bf16[64,8,128]{2,1,0:T(8,128)(2,1)} %scan.1), calls=%async_computation.3 | async-start | bytes 262144 | tf_op jit(solution)/shard_map/all_to_all | solution.py:413
  152.7 3.1 %collective-permute-start.7 = (bf16[32,2048]{1,0:T(8,128)(2,1)}, bf16[32,2048]{1,0:T(8,128)(2,1)S(1)}, u32[]{:S(2)}, u32[]{:S(2)}) collective-permute-start(bf16[32,2048]{1,0:T(8,128)(2,1)} %get-tuple-element.22), channel_id=1, source_target_pairs={{0,8},{8,16},{16,24},{24,32},{32,40},{40,48},{48,56},{56,64},{64,7... | collective-permute-start | bytes 393224 | tf_op jit(solution)/shard_map/ppermute | solution.py:462
  155.8 4.0 %prepare.1 = (f32[4,384,128]{2,1,0:T(8,128)}, bf16[4,384,128]{2,1,0:T(8,128)(2,1)}) custom-call(f32[1,128]{1,0:T(1,128)} %dynamic-slice_bitcast_fusion.refs_9_.floor_ref, bf16[4,384,256]{2,1,0:T(8,128)(2,1)} %get-tuple-element.19.early_ref.refs_9_), custom_call_target="tpu_custom_call" | custom-call | tf_op jit(solution)/shard_map/prepare/pallas_call | solution.py:249
  160.4 10.0 %inside.1 = (f32[4,384,128]{2,1,0:T(8,128)}, bf16[4,384,128]{2,1,0:T(8,128)(2,1)}, bf16[4,384,128]{2,1,0:T(8,128)(2,1)}, bf16[4,384,128]{2,1,0:T(8,128)(2,1)}, f32[4,8,128]{2,1,0:T(8,128)}) custom-call(bf16[200,2048]{1,0:T(8,128)(2,1)} %norm.1.refs_0_, bf16[200,2048]{1,0:T(8,128)(2,1)} %copy-done.4, bf16[200,2048]{1,0:T(8,128)(2,1)} %copy-done.3, ...), custom_call_target="tpu_custom_call" | custom-call | tf_op jit(solution)/shard_map/inside/pallas_call | solution.py:298
  171.1 4.1 %mix.1 = bf16[8,192,256]{2,1,0:T(8,128)(2,1)} custom-call(f32[4,384,128]{2,1,0:T(8,128)} %get-tuple-element.23.inside_ref, bf16[4,384,128]{2,1,0:T(8,128)(2,1)} %get-tuple-element.24.reach_ref, bf16[4,128,128]{2,1,0:T(8,128)(2,1)} %bitcast.15, bf16[4,384,128]{2,1,0:T(8,128)(2,1)} %get-tuple-element.26.gate_ref, ...), custom_call_target="tpu_custom_call" | custom-call | tf_op jit(solution)/shard_map/mix/pallas_call | solution.py:346
  175.2 6.2 %all-to-all-start.4 = ((bf16[8,192,256]{2,1,0:T(8,128)(2,1)}), bf16[8,192,256]{2,1,0:T(8,128)(2,1)S(1)}, u32[]{:S(2)}, u32[]{:S(2)}) async-start(bf16[8,192,256]{2,1,0:T(8,128)(2,1)} %mix.1), calls=%async_computation.4 | async-start | bytes 1572864 | tf_op jit(solution)/shard_map/all_to_all | solution.py:413
  181.4 12.1 %all-to-all-done.4.mix_ref = bf16[8,192,256]{2,1,0:T(8,128)(2,1)S(1)} async-done(((bf16[8,192,256]{2,1,0:T(8,128)(2,1)}), bf16[8,192,256]{2,1,0:T(8,128)(2,1)S(1)}, u32[]{:S(2)}, u32[]{:S(2)}) %all-to-all-start.4) | async-done | bytes 786464 | tf_op jit(solution)/shard_map/all_to_all | solution.py:413
  194.4 6.5 %out.1 = bf16[192,2048]{1,0:T(8,128)(2,1)} custom-call(bf16[8,192,256]{2,1,0:T(8,128)(2,1)} %copy-done.6, bf16[1024,512]{1,0:T(8,128)(2,1)} %constant_dynamic-update-slice_fusion.refs_0_, bf16[1024,512]{1,0:T(8,128)(2,1)} %copy-done.8, bf16[1024,512]{1,0:T(8,128)(2,1)} %collective-permute-done.9.refs_2_, bf16[1024,512]{1,0:T(8,128)(2,1)} %collective-permute-done.10.refs_3_, ...), custom_call_target="tpu_custom_call" | custom-call | tf_op jit(solution)/shard_map/out/pallas_call | solution.py:397
  (55 shorter events, 22.2 us)
Async XLA Ops:
  6.5 90.1 %copy-start = (f32[512]{0:T(512)S(1)}, f32[512]{0:T(512)}, u32[]{:S(2)}) copy-start(f32[512]{0:T(512)} %param.21) | copy-start | bytes 6148
  8.1 17.8 %all-to-all-start = ((bf16[8,32,640]{2,1,0:T(8,128)(2,1)}), bf16[8,32,640]{2,1,0:T(8,128)(2,1)S(1)}, u32[]{:S(2)}, u32[]{:S(2)}) async-start(bf16[8,32,640]{2,1,0:T(8,128)(2,1)} %slab.1), calls=%async_computation | async-start | bytes 655360 | tf_op jit(solution)/shard_map/all_to_all | solution.py:413
  15.8 144.0 %all-gather.2.cloned.1.call-start = ((), (), s32[]{:S(2)}) async-start(), calls=%async_computation.5 | async-start | bytes 1769472 | tf_op jit(solution)/shard_map/all_gather | solution.py:436
  18.4 64.9 %copy-start.10 = (bf16[512,512]{1,0:T(8,128)(2,1)S(1)}, bf16[512,512]{1,0:T(8,128)(2,1)}, u32[]{:S(2)}) copy-start(bf16[512,512]{1,0:T(8,128)(2,1)} %param.24) | copy-start | bytes 1572868
  18.4 32.4 %collective-permute-start.1 = (bf16[200,2048]{1,0:T(8,128)(2,1)}, bf16[200,2048]{1,0:T(8,128)(2,1)S(1)}, u32[]{:S(2)}, u32[]{:S(2)}) collective-permute-start(bf16[200,2048]{1,0:T(8,128)(2,1)} %norm.1.refs_0_), channel_id=1, source_target_pairs={{0,2},{2,4},{4,6},{6,0},{1,3},{3,5},{5,7},{7,1},{8,10},{10,12},{12... | collective-permute-start | bytes 2457608 | tf_op jit(solution)/shard_map/ppermute | solution.py:409
  27.0 70.1 %all-to-all-start.1 = ((bf16[8,256,256]{2,1,0:T(8,128)(2,1)}), bf16[8,256,256]{2,1,0:T(8,128)(2,1)S(1)}, u32[]{:S(2)}, u32[]{:S(2)}) async-start(bf16[8,256,256]{2,1,0:T(8,128)(2,1)} %get-tuple-element.18), calls=%async_computation.1 | async-start | bytes 2097152 | tf_op jit(solution)/shard_map/all_to_all | solution.py:413
  39.1 20.3 %collective-permute-start.3 = (bf16[200,2048]{1,0:T(8,128)(2,1)S(1)}, bf16[200,2048]{1,0:T(8,128)(2,1)}, u32[]{:S(2)}, u32[]{:S(2)}) collective-permute-start(bf16[200,2048]{1,0:T(8,128)(2,1)S(1)} %copy-done.1), channel_id=1, source_target_pairs={{0,6},{2,0},{4,2},{6,4},{1,7},{3,1},{5,3},{7,5},{8,14},{10,8},{12,... | collective-permute-start | bytes 2457608 | tf_op jit(solution)/shard_map/ppermute | solution.py:409
  43.5 37.9 %collective-permute-start.5 = (bf16[200,2048]{1,0:T(8,128)(2,1)S(1)}, bf16[200,2048]{1,0:T(8,128)(2,1)}, u32[]{:S(2)}, u32[]{:S(2)}) collective-permute-start(bf16[200,2048]{1,0:T(8,128)(2,1)S(1)} %copy-done.1), channel_id=1, source_target_pairs={{0,4},{2,6},{4,0},{6,2},{1,5},{3,7},{5,1},{7,3},{8,12},{10,14},{12... | collective-permute-start | bytes 2457608 | tf_op jit(solution)/shard_map/ppermute | solution.py:409
  45.9 42.1 %collective-permute-start = (bf16[200,2048]{1,0:T(8,128)(2,1)S(1)}, bf16[200,2048]{1,0:T(8,128)(2,1)S(1)}, u32[]{:S(2)}, u32[]{:S(2)}) collective-permute-start(bf16[200,2048]{1,0:T(8,128)(2,1)S(1)} %copy-done.1), channel_id=1, source_target_pairs={{0,1},{1,0},{2,3},{3,2},{4,5},{5,4},{6,7},{7,6},{8,9},{9,8},{10,11... | collective-permute-start | bytes 2457608 | tf_op jit(solution)/shard_map/ppermute | solution.py:409
  50.8 46.4 %copy-start.3 = (bf16[200,2048]{1,0:T(8,128)(2,1)}, bf16[200,2048]{1,0:T(8,128)(2,1)S(1)}, u32[]{:S(2)}) copy-start(bf16[200,2048]{1,0:T(8,128)(2,1)S(1)} %collective-permute-done.1.refs_2_) | copy-start | bytes 2457604
  50.8 42.6 %collective-permute-start.2 = (bf16[200,2048]{1,0:T(8,128)(2,1)S(1)}, bf16[200,2048]{1,0:T(8,128)(2,1)S(1)}, u32[]{:S(2)}, u32[]{:S(2)}) collective-permute-start(bf16[200,2048]{1,0:T(8,128)(2,1)S(1)} %collective-permute-done.1.refs_2_), channel_id=1, source_target_pairs={{0,1},{1,0},{2,3},{3,2},{4,5},{5,4},{6,7},{7,6},{8,9},{9,8},{10,11... | collective-permute-start | bytes 2457608 | tf_op jit(solution)/shard_map/ppermute | solution.py:409
  59.4 37.8 %collective-permute-start.4 = (bf16[200,2048]{1,0:T(8,128)(2,1)}, bf16[200,2048]{1,0:T(8,128)(2,1)}, u32[]{:S(2)}, u32[]{:S(2)}) collective-permute-start(bf16[200,2048]{1,0:T(8,128)(2,1)} %collective-permute-done.3.refs_4_), channel_id=1, source_target_pairs={{0,1},{1,0},{2,3},{3,2},{4,5},{5,4},{6,7},{7,6},{8,9},{9,8},{10,11... | collective-permute-start | bytes 2457608 | tf_op jit(solution)/shard_map/ppermute | solution.py:409
  81.4 15.8 %collective-permute-start.6 = (bf16[200,2048]{1,0:T(8,128)(2,1)}, bf16[200,2048]{1,0:T(8,128)(2,1)}, u32[]{:S(2)}, u32[]{:S(2)}) collective-permute-start(bf16[200,2048]{1,0:T(8,128)(2,1)} %collective-permute-done.5.refs_6_), channel_id=1, source_target_pairs={{0,1},{1,0},{2,3},{3,2},{4,5},{5,4},{6,7},{7,6},{8,9},{9,8},{10,11... | collective-permute-start | bytes 2457608 | tf_op jit(solution)/shard_map/ppermute | solution.py:409
  86.1 32.2 %collective-permute-start.9 = (bf16[1024,512]{1,0:T(8,128)(2,1)}, bf16[1024,512]{1,0:T(8,128)(2,1)}, u32[]{:S(2)}, u32[]{:S(2)}) collective-permute-start(bf16[1024,512]{1,0:T(8,128)(2,1)} %constant_dynamic-update-slice_fusion.refs_0_), channel_id=1, source_target_pairs={{0,2},{2,4},{4,6},{6,0},{1,3},{3,5},{5,7},{7,1},{8,10},{10,12},{12... | collective-permute-start | bytes 3145736 | tf_op jit(solution)/shard_map/ppermute | solution.py:409
  88.0 50.0 %collective-permute-start.11 = (bf16[1024,512]{1,0:T(8,128)(2,1)}, bf16[1024,512]{1,0:T(8,128)(2,1)S(1)}, u32[]{:S(2)}, u32[]{:S(2)}) collective-permute-start(bf16[1024,512]{1,0:T(8,128)(2,1)} %constant_dynamic-update-slice_fusion.refs_0_), channel_id=1, source_target_pairs={{0,6},{2,0},{4,2},{6,4},{1,7},{3,1},{5,3},{7,5},{8,14},{10,8},{12,... | collective-permute-start | bytes 3145736 | tf_op jit(solution)/shard_map/ppermute | solution.py:409
  93.5 48.0 %collective-permute-start.13 = (bf16[1024,512]{1,0:T(8,128)(2,1)}, bf16[1024,512]{1,0:T(8,128)(2,1)}, u32[]{:S(2)}, u32[]{:S(2)}) collective-permute-start(bf16[1024,512]{1,0:T(8,128)(2,1)} %constant_dynamic-update-slice_fusion.refs_0_), channel_id=1, source_target_pairs={{0,4},{2,6},{4,0},{6,2},{1,5},{3,7},{5,1},{7,3},{8,12},{10,14},{12... | collective-permute-start | bytes 3145736 | tf_op jit(solution)/shard_map/ppermute | solution.py:409
  106.6 36.8 %all-to-all-start.2 = ((bf16[64,16,128]{2,1,0:T(8,128)(2,1)}), bf16[64,16,128]{2,1,0:T(8,128)(2,1)S(1)}, u32[]{:S(2)}, u32[]{:S(2)}) async-start(bf16[64,16,128]{2,1,0:T(8,128)(2,1)} %get-tuple-element.25), calls=%async_computation.2 | async-start | bytes 524288 | tf_op jit(solution)/shard_map/all_to_all | solution.py:413
  115.0 66.4 %collective-permute-start.8 = (bf16[1024,512]{1,0:T(8,128)(2,1)}, bf16[1024,512]{1,0:T(8,128)(2,1)S(1)}, u32[]{:S(2)}, u32[]{:S(2)}) collective-permute-start(bf16[1024,512]{1,0:T(8,128)(2,1)} %constant_dynamic-update-slice_fusion.refs_0_), channel_id=1, source_target_pairs={{0,1},{1,0},{2,3},{3,2},{4,5},{5,4},{6,7},{7,6},{8,9},{9,8},{10,11... | collective-permute-start | bytes 3145736 | tf_op jit(solution)/shard_map/ppermute | solution.py:409
  118.3 63.1 %collective-permute-start.10 = (bf16[1024,512]{1,0:T(8,128)(2,1)}, bf16[1024,512]{1,0:T(8,128)(2,1)}, u32[]{:S(2)}, u32[]{:S(2)}) collective-permute-start(bf16[1024,512]{1,0:T(8,128)(2,1)} %collective-permute-done.9.refs_2_), channel_id=1, source_target_pairs={{0,1},{1,0},{2,3},{3,2},{4,5},{5,4},{6,7},{7,6},{8,9},{9,8},{10,11... | collective-permute-start | bytes 3145736 | tf_op jit(solution)/shard_map/ppermute | solution.py:409
  138.1 43.3 %collective-permute-start.12 = (bf16[1024,512]{1,0:T(8,128)(2,1)S(1)}, bf16[1024,512]{1,0:T(8,128)(2,1)}, u32[]{:S(2)}, u32[]{:S(2)}) collective-permute-start(bf16[1024,512]{1,0:T(8,128)(2,1)S(1)} %collective-permute-done.11.refs_4_), channel_id=1, source_target_pairs={{0,1},{1,0},{2,3},{3,2},{4,5},{5,4},{6,7},{7,6},{8,9},{9,8},{10,11... | collective-permute-start | bytes 3145736 | tf_op jit(solution)/shard_map/ppermute | solution.py:409
  141.5 39.9 %collective-permute-start.14 = (bf16[1024,512]{1,0:T(8,128)(2,1)}, bf16[1024,512]{1,0:T(8,128)(2,1)}, u32[]{:S(2)}, u32[]{:S(2)}) collective-permute-start(bf16[1024,512]{1,0:T(8,128)(2,1)} %collective-permute-done.13.refs_6_), channel_id=1, source_target_pairs={{0,1},{1,0},{2,3},{3,2},{4,5},{5,4},{6,7},{7,6},{8,9},{9,8},{10,11... | collective-permute-start | bytes 3145736 | tf_op jit(solution)/shard_map/ppermute | solution.py:409
  144.3 26.2 %all-to-all-start.3 = ((bf16[64,8,128]{2,1,0:T(8,128)(2,1)}), bf16[64,8,128]{2,1,0:T(8,128)(2,1)S(1)}, u32[]{:S(2)}, u32[]{:S(2)}) async-start(bf16[64,8,128]{2,1,0:T(8,128)(2,1)} %scan.1), calls=%async_computation.3 | async-start | bytes 262144 | tf_op jit(solution)/shard_map/all_to_all | solution.py:413
  152.7 7.1 %collective-permute-start.7 = (bf16[32,2048]{1,0:T(8,128)(2,1)}, bf16[32,2048]{1,0:T(8,128)(2,1)S(1)}, u32[]{:S(2)}, u32[]{:S(2)}) collective-permute-start(bf16[32,2048]{1,0:T(8,128)(2,1)} %get-tuple-element.22), channel_id=1, source_target_pairs={{0,8},{8,16},{16,24},{24,32},{32,40},{40,48},{48,56},{56,64},{64,7... | collective-permute-start | bytes 393224 | tf_op jit(solution)/shard_map/ppermute | solution.py:462
  175.2 18.4 %all-to-all-start.4 = ((bf16[8,192,256]{2,1,0:T(8,128)(2,1)}), bf16[8,192,256]{2,1,0:T(8,128)(2,1)S(1)}, u32[]{:S(2)}, u32[]{:S(2)}) async-start(bf16[8,192,256]{2,1,0:T(8,128)(2,1)} %mix.1), calls=%async_computation.4 | async-start | bytes 1572864 | tf_op jit(solution)/shard_map/all_to_all | solution.py:413
  (9 other events, 76.8 us)
Sparse Core Ops, SparseCore 0:
  27.2 55.6 all-gather.1
